TPU v7x, 128 devices: a whole 4x4x4 slice. The times are simulated.
128 devices in a mesh: sp: 16 (over z, x), tp: 8 (over y, core).
Axes of the slice: x: 4, y: 4, z: 4, core: 2. Of those that a mesh axis runs over, the one named last changes fastest.
Arguments:
- token_values: bfloat16 [4096, 2048], P('sp', 'tp'), may hold values from -6 to 6
- write_keys: bfloat16 [4096, 1024], P('sp', 'tp'), may hold values from -0.3125 to 0.3125
- read_keys: bfloat16 [4096, 1024], P('sp', 'tp'), may hold values from -0.3125 to 0.3125
- log_decay: float32 [32, 4096], P('tp', 'sp'), may hold values from -0.7 to 0, as said below
- out_gate: bfloat16 [4096, 2048], P('sp', 'tp'), may hold values from -6 to 6
- out_proj: bfloat16 [4096, 2048], P(None, 'tp'), may hold values from -0.125 to 0.125
- mixed: bfloat16 [4096, 4096], P('sp'), may hold values from -6 to 6
- cotangent: bfloat16 [4096, 4096], P('sp'), may hold values from -8 to 8
- route_ids: int32 [4096, 2], P('sp'), may hold values from 0 to 15, all different within a row; in each aligned block of 256 rows (0 to 255, 256 to 511, ...) at most 48 rows name the same one
- route_weights: float32 [4096, 2], P('sp'), may hold values from 0.25 to 1
- w_gate: bfloat16 [16, 4096, 2048], P('sp', None, 'tp'), may hold values from -0.09375 to 0.09375
- w_up: bfloat16 [16, 4096, 2048], P('sp', None, 'tp'), may hold values from -0.09375 to 0.09375
- w_down: bfloat16 [16, 2048, 4096], P('sp', 'tp'), may hold values from -0.125 to 0.125
Outputs:
- value_grad: bfloat16 [4096, 2048], P('sp', 'tp')
- write_grad: bfloat16 [4096, 1024], P('sp', 'tp')
- read_grad: bfloat16 [4096, 1024], P('sp', 'tp')
- gate_grad: bfloat16 [4096, 2048], P('sp', 'tp')
- proj_grad: float32 [4096, 2048], P('sp', 'tp')
- gate_weight_grad: bfloat16 [16, 4096, 2048], P('sp', None, 'tp')
- up_weight_grad: bfloat16 [16, 4096, 2048], P('sp', None, 'tp')
- down_weight_grad: bfloat16 [16, 2048, 4096], P('sp', 'tp')
Inputs may be any that keep to these rules, and one draw needn't show every extreme that they name: `route_ids`: each row names 2 different experts. Within the rows of one device no expert is named more than 48 times, and in every draw some expert is named exactly 48 times by the rows of some device. `log_decay`: every entry is negative.
All inputs are finite; a program needn't handle non-finite values.
Results may differ from a plain program's by a relative error of at most 0.019.
Values may be sent and summed in bfloat16 or wider, within the bound.
A program may use at most 128 MiB of HBM per device.

v0:
```python
import jax
import jax.numpy as jnp
from jax import lax
from jax.sharding import Mesh
from jax.sharding import PartitionSpec as P

HEAD_DIM = 64
STATE = 128
BLOCK = 64
SP = ("sp_0", "sp_1")


highest = lax.Precision.HIGHEST


def sent_together(arrays, axis, split_dim, concat_dim, along):
    both = jnp.concatenate(arrays, axis=along)
    whole, at, finished = (
        lax.all_to_all(both, axis, split_axis=split_dim, concat_axis=concat_dim, tiled=True),
        0,
        [],
    )
    for a in arrays:
        finished.append(lax.slice_in_dim(whole, at, at + a.shape[along], axis=along))
        at += a.shape[along]
    return tuple(finished)


def side_by_side(arrays, axis, dim, along):
    both = jnp.concatenate(arrays, axis=along)
    whole, at, finished = (lax.all_gather(both, axis, axis=dim, tiled=True), 0, [])
    for a in arrays:
        finished.append(lax.slice_in_dim(whole, at, at + a.shape[along], axis=along))
        at += a.shape[along]
    return tuple(finished)


def nothing_yet(array, identity):
    return jax.tree.map(
        lambda a, e: jnp.broadcast_to(jnp.asarray(e, a.dtype), a.shape), array, identity
    )


def prefix_by_axis(array, axes, combine, identity, reverse):
    before = start = nothing_yet(array, identity)
    so_far = array
    for axis in reversed(axes):
        length, position = (lax.axis_size(axis), lax.axis_index(axis))
        pieces = jax.tree.map(
            lambda part, kind: lax.all_gather(part.astype(kind), axis),
            so_far,
            (jnp.bfloat16, jnp.bfloat16),
        )
        inside, so_far = (start, start)
        for k in reversed(range(length)) if reverse else range(length):
            passed = k > position if reverse else k < position
            so_far = combine(
                so_far, jax.tree.map(lambda part, own: part[k].astype(own.dtype), pieces, array)
            )
            inside = jax.tree.map(lambda new, old: jnp.where(passed, new, old), so_far, inside)
        before = combine(inside, before)
    return before


def in_blocks(array, dim, length):
    before, after = (array.shape[:dim], array.shape[dim + 1 :])
    return jnp.moveaxis(array.reshape(*before, length, -1, *after), dim, 0)


def sent_and_summed(array, axis, dim):
    parts = in_blocks(array, dim, lax.axis_size(axis))
    arrived = lax.all_to_all(parts, axis, split_axis=0, concat_axis=0, tiled=True)
    return arrived.astype(jnp.float32).sum(axis=0)


def mix_blocks(token_values, write_keys, read_keys, log_decay, entering):
    length = token_values.shape[0]
    heads = log_decay.shape[0]
    groups = write_keys.shape[1] // STATE
    per_group = heads // groups
    blocks = length // BLOCK
    inputs = token_values.reshape(blocks, BLOCK, groups, per_group, HEAD_DIM)
    writes = write_keys.reshape(blocks, BLOCK, groups, STATE)
    reads = read_keys.reshape(blocks, BLOCK, groups, STATE)
    decay = log_decay.reshape(groups, per_group, blocks, BLOCK).transpose(2, 3, 0, 1)
    cumul = jnp.cumsum(decay, axis=1)
    spans = cumul[:, :, None] - cumul[:, None, :]
    position = jnp.arange(BLOCK, dtype=jnp.int32)
    lower = (position[:, None] >= position[None, :])[None, :, :, None, None]
    weights = jnp.exp(jnp.where(lower, spans, -jnp.inf))
    scores = jnp.einsum("clgn,csgn->clsg", reads, writes, precision=highest)
    inner = jnp.einsum("clsgr,csgrp->clgrp", scores[..., None] * weights, inputs, precision=highest)
    tails = jnp.exp(cumul[:, -1:] - cumul)
    block_states = jnp.einsum(
        "clgn,clgrp->cgrpn", writes, inputs * tails[..., None], precision=highest
    )
    block_decay = jnp.exp(cumul[:, -1])

    def advance(state, pieces):
        factor, added = pieces
        return (factor[..., None, None] * state + added, state)

    final, before = lax.scan(
        advance, entering.reshape(groups, per_group, HEAD_DIM, STATE), (block_decay, block_states)
    )
    carried = (
        jnp.einsum("clgn,cgrpn->clgrp", reads, before, precision=highest)
        * jnp.exp(cumul)[..., None]
    )
    return (
        (inner + carried).reshape(length, heads * HEAD_DIM),
        final.reshape(heads, HEAD_DIM, STATE),
    )


def expert_backward(rows, scaled, gate_weight, up_weight, down_weight):
    gate_pre = jnp.dot(rows, gate_weight, preferred_element_type=jnp.float32)
    up_pre = jnp.dot(rows, up_weight, preferred_element_type=jnp.float32)
    sigma = jax.nn.sigmoid(gate_pre)
    hidden = (jax.nn.silu(gate_pre) * up_pre).astype(jnp.bfloat16)
    over_rows = (((0,), (0,)), ((), ()))
    over_units = (((1,), (1,)), ((), ()))
    grad_down = lax.dot_general(hidden, scaled, over_rows, preferred_element_type=jnp.float32)
    d_hidden = lax.dot_general(scaled, down_weight, over_units, preferred_element_type=jnp.float32)
    d_gate = (d_hidden * up_pre * sigma * (1.0 + gate_pre * (1.0 - sigma))).astype(jnp.bfloat16)
    d_up = (d_hidden * jax.nn.silu(gate_pre)).astype(jnp.bfloat16)
    grad_gate = lax.dot_general(rows, d_gate, over_rows, preferred_element_type=jnp.float32)
    grad_up = lax.dot_general(rows, d_up, over_rows, preferred_element_type=jnp.float32)
    value_portion = lax.dot_general(
        d_gate, gate_weight, over_units, preferred_element_type=jnp.float32
    )
    value_portion = value_portion + lax.dot_general(
        d_up, up_weight, over_units, preferred_element_type=jnp.float32
    )
    return (
        grad_gate.astype(jnp.bfloat16),
        grad_up.astype(jnp.bfloat16),
        grad_down.astype(jnp.bfloat16),
        value_portion,
    )


def forward_join(earlier, later):
    return (earlier[0] + later[0], jnp.exp(later[0])[..., None, None] * earlier[1] + later[1])


def backward_join(earlier, later):
    return (earlier[0] + later[0], later[1] + jnp.exp(later[0])[..., None, None] * earlier[1])


def body(
    token_values,
    write_keys,
    read_keys,
    log_decay,
    out_gate,
    out_proj,
    mixed,
    cotangent,
    route_ids,
    route_weights,
    w_gate,
    w_up,
    w_down,
):
    tok_rows, width = mixed.shape
    experts = lax.axis_size(SP)
    expert_capacity = 3 * tok_rows // experts
    flat_ids = route_ids.reshape(-1)
    pairs = flat_ids.shape[0]
    member = (flat_ids[:, None] == jnp.arange(experts, dtype=jnp.int32)[None, :]).astype(jnp.int32)
    earlier = jnp.cumsum(member, axis=0) - member
    slot_index = jnp.sum(earlier * member, axis=1)
    target = flat_ids * expert_capacity + slot_index
    copies = jnp.repeat(mixed, 2, axis=0)
    scaled = (cotangent.astype(jnp.float32)[:, None, :] * route_weights[:, :, None]).reshape(
        pairs, width
    )
    scaled = scaled.astype(jnp.bfloat16)
    places = experts * expert_capacity
    share = width // lax.axis_size("tp")
    offset = lax.axis_index("tp") * share
    part_rows = lax.dynamic_slice_in_dim(copies, offset, share, 1)
    part_scaled = lax.dynamic_slice_in_dim(scaled, offset, share, 1)
    send_rows = jnp.zeros((places, share), jnp.bfloat16).at[target].set(part_rows)
    send_scaled = jnp.zeros((places, share), jnp.bfloat16).at[target].set(part_scaled)
    got_pieces = sent_together(
        (
            send_rows.reshape(experts, expert_capacity, share),
            send_scaled.reshape(experts, expert_capacity, share),
        ),
        SP,
        0,
        0,
        1,
    )
    got_rows, got_scaled = side_by_side((got_pieces[0], got_pieces[1]), "tp", 2, 0)
    grads = expert_backward(
        got_rows.reshape(places, width),
        got_scaled.reshape(places, width),
        w_gate[0],
        w_up[0],
        w_down[0],
    )
    summed = lax.psum_scatter(
        grads[3].reshape(experts, expert_capacity, width).astype(jnp.bfloat16),
        "tp",
        scatter_dimension=2,
        tiled=True,
    )
    came = lax.all_to_all(summed, SP, split_axis=0, concat_axis=0, tiled=True)
    returned = lax.all_gather(came, "tp", axis=2, tiled=True).reshape(places, width)
    picked = jnp.take(returned, target, axis=0).astype(jnp.float32).reshape(tok_rows, 2, width)
    grad_mixed = (cotangent.astype(jnp.float32) + jnp.sum(picked, axis=1)).astype(jnp.bfloat16)
    out_grad = jnp.dot(grad_mixed, out_proj, preferred_element_type=jnp.float32)
    values_float = token_values.astype(jnp.float32)
    writes_float = write_keys.astype(jnp.float32)
    reads_float = read_keys.astype(jnp.float32)
    gate_float = out_gate.astype(jnp.float32)
    heads = log_decay.shape[0]
    groups = write_keys.shape[1] // STATE
    per_group = heads // groups
    cumul = jnp.cumsum(log_decay, axis=1)
    total = cumul[:, -1]
    tails = jnp.exp(total[:, None] - cumul).T.reshape(tok_rows, groups, per_group)
    leads = jnp.exp(cumul).T.reshape(tok_rows, groups, per_group)
    inputs = values_float.reshape(tok_rows, groups, per_group, HEAD_DIM)
    outer_grad = (out_grad * jax.nn.silu(gate_float)).reshape(tok_rows, groups, per_group, HEAD_DIM)
    writes = writes_float.reshape(tok_rows, groups, STATE)
    reads = reads_float.reshape(tok_rows, groups, STATE)
    local_end = jnp.einsum("tgrp,tgn->grpn", inputs * tails[..., None], writes, precision=highest)
    local_back = jnp.einsum(
        "tgrp,tgn->grpn", outer_grad * leads[..., None], reads, precision=highest
    )
    shaped_total = total.reshape(groups, per_group)
    zero_total = jnp.zeros_like(shaped_total)
    zero_state = jnp.zeros_like(local_end)
    entering = prefix_by_axis(
        (shaped_total, local_end), SP, forward_join, (zero_total, zero_state), False
    )[1].reshape(heads, HEAD_DIM, STATE)
    leaving = prefix_by_axis(
        (shaped_total, local_back), SP, backward_join, (zero_total, zero_state), True
    )[1].reshape(heads, HEAD_DIM, STATE)

    def local_mix(values_in, writes_in, reads_in, gate_in):
        mixed_heads, final = mix_blocks(values_in, writes_in, reads_in, log_decay, entering)
        return (mixed_heads * jax.nn.silu(gate_in), final)

    outputs, pullback = jax.vjp(local_mix, values_float, writes_float, reads_float, gate_float)
    d_values, d_writes, d_reads, d_gate = pullback((out_grad, leaving))
    gated_b = outputs[0].astype(jnp.bfloat16)
    proj_grad = sent_and_summed(
        lax.dot_general(
            grad_mixed, gated_b, (((0,), (0,)), ((), ())), preferred_element_type=jnp.float32
        ).astype(jnp.bfloat16),
        SP,
        0,
    )
    return (
        d_values.astype(jnp.bfloat16),
        d_writes.astype(jnp.bfloat16),
        d_reads.astype(jnp.bfloat16),
        d_gate.astype(jnp.bfloat16),
        proj_grad,
        grads[0][None],
        grads[1][None],
        grads[2][None],
    )


def solution(mesh):
    finer = Mesh(mesh.devices.reshape(4, 4, mesh.shape["tp"]), ("sp_0", "sp_1", "tp"))
    return jax.shard_map(
        body,
        mesh=finer,
        in_specs=(
            P(SP, "tp"),
            P(SP, "tp"),
            P(SP, "tp"),
            P("tp", SP),
            P(SP, "tp"),
            P(None, "tp"),
            P(SP, None),
            P(SP, None),
            P(SP, None),
            P(SP, None),
            P(SP, None, "tp"),
            P(SP, None, "tp"),
            P(SP, "tp", None),
        ),
        out_specs=(
            P(SP, "tp"),
            P(SP, "tp"),
            P(SP, "tp"),
            P(SP, "tp"),
            P(SP, "tp"),
            P(SP, None, "tp"),
            P(SP, None, "tp"),
            P(SP, "tp", None),
        ),
        check_vma=False,
    )
```

profile of v0, /device:TPU:0, one launch (start us, length us, event | category | flops | bytes accessed | tf_op | source)
XLA Modules:
  0.0 423.6 jit_solution(7333332821910809468)
XLA Ops:
  10.9 8.2 %mul.536 = f32[256,2,4096]{2,1,0:T(2,128)} broadcast(bf16[256,4096]{1,0:T(8,128)(2,1)} %param.24), dimensions={0,2} | broadcast | bytes 10485760 | tf_op jit(solution)/shard_map/mul | solution.py:176
  19.1 11.0 %mul.537 = f32[512,4096]{1,0:T(8,128)} reshape(f32[256,2,4096]{2,1,0:T(2,128)} %mul.536) | data formatting | bytes 16777216 | tf_op jit(solution)/shard_map/mul | solution.py:176
  30.4 6.1 %broadcast_in_dim.98 = bf16[256,2,4096]{2,1,0:T(2,128)(2,1)} broadcast(bf16[256,4096]{1,0:T(8,128)(2,1)} %param.23), dimensions={0,2} | broadcast | bytes 6291456 | tf_op jit(solution)/shard_map/broadcast_in_dim | solution.py:175
  36.4 7.2 %reshape.1055 = bf16[512,4096]{1,0:T(8,128)(2,1)} reshape(bf16[256,2,4096]{2,1,0:T(2,128)(2,1)} %broadcast_in_dim.98) | data formatting | bytes 8388608 | tf_op jit(solution)/shard_map/reshape | solution.py:175
  52.2 30.6 %all_to_all.15 = bf16[16,96,512]{2,1,0:T(8,128)(2,1)S(1)} all-to-all(bf16[16,96,512]{2,1,0:T(8,128)(2,1)S(1)} %pad_maximum_fusion), channel_id=1, replica_groups=mesh['sp_0'=4,'sp_1'=4,'tp'=8] {'sp_0','sp_1'}, dimensions={0} | all-to-all | bytes 3145728 | tf_op jit(solution)/shard_map/all_to_all | solution.py:19
  84.4 64.9 %all-gather.6.cloned.1.call-done = bf16[32,48,4096]{2,1,0:T(8,128)(2,1)} async-done(((bf16[32,48,512]{2,1,0:T(8,128)(2,1)}), bf16[32,48,4096]{2,1,0:T(8,128)(2,1)}) %all-gather.6.cloned.1.call-update) | async-done | bytes 12582928 | tf_op jit(solution)/shard_map/all_gather | solution.py:31
  149.3 5.7 %fusion.158 = (bf16[16,48,4096]{2,1,0:T(8,128)(2,1)S(1)}, bf16[16,48,4096]{2,1,0:T(8,128)(2,1)S(1)}) fusion(bf16[32,48,4096]{2,1,0:T(8,128)(2,1)} %all-gather.6.cloned.1.call-done), kind=kLoop, calls=%fused_computation.282 | loop fusion | bytes 25165824 | tf_op jit(solution)/shard_map/slice | solution.py:33
  168.4 43.0 %reduce-scatter.2.cloned.1.call-done = bf16[16,48,512]{2,1,0:T(8,128)(2,1)} async-done(((bf16[16,48,4096]{2,1,0:T(8,128)(2,1)}), bf16[16,48,512]{2,1,0:T(8,128)(2,1)}) %reduce-scatter.2.cloned.1.call-update) | async-done | bytes 786448 | tf_op jit(solution)/shard_map/reduce_scatter | solution.py:205
  211.4 20.8 %all_to_all.16 = bf16[16,48,512]{2,1,0:T(8,128)(2,1)} all-to-all(bf16[16,48,512]{2,1,0:T(8,128)(2,1)} %reduce-scatter.2.cloned.1.call-done), channel_id=1, replica_groups=mesh['sp_0'=4,'sp_1'=4,'tp'=8] {'sp_0','sp_1'}, dimensions={0} | all-to-all | bytes 1572864 | tf_op jit(solution)/shard_map/all_to_all | solution.py:211
  235.6 8.5 %all-reduce = bf16[16]{0:T(256)(128)(2,1)S(1)} all-reduce(bf16[16]{0:T(256)(128)(2,1)S(1)} %dynamic-update-slice), channel_id=3, replica_groups=mesh['sp_0'=4,'sp_1'=4,'tp'=8] {'sp_1'}, use_global_device_ids=true, to_apply=%add | all-reduce | flops 16 | bytes 64
  244.1 8.0 %all_gather.47 = bf16[4,1,4]{2,1,0:T(2,128)(2,1)S(1)} all-gather(bf16[1,1,4]{2,1,0:T(2,128)(2,1)S(1)} %get-tuple-element.273), channel_id=1, replica_groups=mesh['sp_0'=4,'sp_1'=4,'tp'=8] {'sp_0'}, dimensions={0}, use_global_device_ids=true | all-gather | bytes 40 | tf_op jit(solution)/shard_map/all_gather | solution.py:50
  252.2 7.9 %all_gather.46 = bf16[4,1,4]{2,1,0:T(2,128)(2,1)S(1)} all-gather(bf16[1,1,4]{2,1,0:T(2,128)(2,1)S(1)} %get-tuple-element.274), channel_id=1, replica_groups=mesh['sp_0'=4,'sp_1'=4,'tp'=8] {'sp_0'}, dimensions={0}, use_global_device_ids=true | all-gather | bytes 40 | tf_op jit(solution)/shard_map/all_gather | solution.py:50
  262.9 12.3 %all-gather.2 = bf16[16,64,128]{2,1,0:T(8,128)(2,1)S(1)} all-gather(bf16[4,64,128]{2,1,0:T(8,128)(2,1)S(1)} %convolution_convert_fusion.4), channel_id=4, replica_groups=mesh['sp_0'=4,'sp_1'=4,'tp'=8] {'sp_1'}, dimensions={0}, use_global_device_ids=true | all-gather | bytes 327680 | tf_op jit(solution)/shard_map/all_gather | solution.py:50
  276.5 12.3 %all_gather.50 = bf16[4,1,4,64,128]{4,3,2,1,0:T(8,128)(2,1)S(1)} all-gather(bf16[1,1,4,64,128]{4,3,2,1,0:T(8,128)(2,1)S(1)} %fusion.75), channel_id=1, replica_groups=mesh['sp_0'=4,'sp_1'=4,'tp'=8] {'sp_0'}, dimensions={0}, use_global_device_ids=true | all-gather | bytes 327680 | tf_op jit(solution)/shard_map/all_gather | solution.py:50
  295.7 6.1 %fusion.3 = bf16[1,4096,256]{2,1,0:T(8,128)(2,1)} fusion(bf16[768,4096]{1,0:T(8,128)(2,1)} %bitcast.491, bf16[768,256]{1,0:T(8,128)(2,1)} %copy-done.19), kind=kOutput, calls=%fused_computation.20 | convolution fusion | flops 1611661312 | bytes 8781824 | tf_op jit(solution)/shard_map/dot_general | solution.py:128
  301.9 6.1 %fusion.2 = bf16[1,4096,256]{2,1,0:T(8,128)(2,1)} fusion(bf16[768,4096]{1,0:T(8,128)(2,1)} %bitcast.492, bf16[768,256]{1,0:T(8,128)(2,1)S(1)} %copy-done.18), kind=kOutput, calls=%fused_computation.19 | convolution fusion | flops 1611661312 | bytes 8781824 | tf_op jit(solution)/shard_map/dot_general | solution.py:127
  311.2 12.2 %gather_fusion = bf16[512,4096]{1,0:T(8,128)(2,1)} fusion(bf16[768,4096]{1,0:T(8,128)(2,1)} %bitcast.482, s32[1024]{0:T(1024)S(1)} %pad_clamp_fusion), kind=kCustom, calls=%fused_computation | custom fusion | bytes 8390656 | tf_op jit(solution)/shard_map/jit(_take)/gather | solution.py:213
  323.4 7.7 %gather.7 = bf16[256,2,4096]{2,1,0:T(2,128)(2,1)} reshape(bf16[512,4096]{1,0:T(8,128)(2,1)} %gather_fusion) | data formatting | bytes 8388608 | tf_op jit(solution)/shard_map/jit(_take)/gather | solution.py:213
  331.1 14.4 %convert_reduce_fusion = f32[256,4096]{1,0:T(8,128)S(1)} fusion(bf16[256,2,4096]{2,1,0:T(2,128)(2,1)} %gather.7, pred[256,2]{1,0:T(8,128)(4,1)S(1)} %copy.126), kind=kLoop, calls=%fused_computation.13 | loop fusion | flops 5242880 | bytes 8389120 | tf_op jit(solution)/shard_map/reduce_sum | solution.py:214
  348.1 4.6 %all-to-all-start.2 = ((bf16[16,256,256]{2,1,0:T(8,128)(2,1)}), bf16[16,256,256]{2,1,0:T(8,128)(2,1)}, u32[]{:S(2)}, u32[]{:S(2)}) async-start(bf16[16,256,256]{2,1,0:T(8,128)(2,1)} %bitcast.488), calls=%async_computation.3 | async-start | bytes 4194304 | tf_op jit(solution)/shard_map/all_to_all | solution.py:72
  352.7 4.6 %bitcast_multiply_fusion.1 = (f32[256,256]{0,1:T(8,128)}, f32[256,256]{0,1:T(8,128)S(1)}, bf16[256,256]{0,1:T(8,128)(2,1)}) fusion(f32[256,4]{0,1:T(4,128)S(1)} %copy-done.27, bf16[256,256]{0,1:T(8,128)(2,1)S(1)} %copy.129, f32[256,256]{0,1:T(8,128)S(1)} %reshape.1074, bf16[4096,256]{1,0:T(8,128)(2,1)} %param.22, f32[256,4096]{1,0:T(8,128)} %copy-done.3, ...), kind=kOutput, calls=%fused_computation.96 | convolution fusion | flops 540999680 | bytes 9441280 | tf_op jit(solution)/shard_map/dot_general | solution.py:215
  359.1 21.1 %all-gather = bf16[16,64,128]{2,1,0:T(8,128)(2,1)S(1)} all-gather(bf16[4,64,128]{2,1,0:T(8,128)(2,1)S(1)} %convolution_convert_fusion.5), channel_id=2, replica_groups=mesh['sp_0'=4,'sp_1'=4,'tp'=8] {'sp_1'}, dimensions={0}, use_global_device_ids=true | all-gather | bytes 327680 | tf_op jit(solution)/shard_map/all_gather | solution.py:50
  381.0 12.3 %all_gather.45 = bf16[4,1,4,64,128]{4,3,2,1,0:T(8,128)(2,1)S(1)} all-gather(bf16[1,1,4,64,128]{4,3,2,1,0:T(8,128)(2,1)S(1)} %fusion.87), channel_id=1, replica_groups=mesh['sp_0'=4,'sp_1'=4,'tp'=8] {'sp_0'}, dimensions={0}, use_global_device_ids=true | all-gather | bytes 327680 | tf_op jit(solution)/shard_map/all_gather | solution.py:50
  395.2 5.6 %while.31 = (s32[]{:T(128)}, f32[1,4,64,128]{3,2,1,0:T(8,128)S(1)}, f32[4,1,4,64,128]{4,3,2,1,0:T(8,128)}, f32[4,1,4,64,128]{4,3,2,1,0:T(8,128)S(1)}, f32[4,1,4,1,1]{2,4,3,1,0:T(1,128)}, /*index=5*/s32[]{:T(128)}, s32[]{:T(128)}) while((s32[]{:T(128)}, f32[1,4,64,128]{3,2,1,0:T(8,128)S(1)}, f32[4,1,4,64,128]{4,3,2,1,0:T(8,128)}, ...), condition=%wide.region_13.14_spmd, body=%wide.region_12.13_spmd.sunk | while | flops 65539 | bytes 655509 | solution.py:103
  (226 shorter events, 75.3 us)
Async XLA Ops:
  7.2 149.7 %copy-start = (bf16[1,4096,256]{2,1,0:T(8,128)(2,1)S(1)}, bf16[1,4096,256]{2,1,0:T(8,128)(2,1)}, u32[]{:S(2)}) copy-start(bf16[1,4096,256]{2,1,0:T(8,128)(2,1)} %param.27) | copy-start | bytes 6291460
  7.2 142.1 %all-gather.6.cloned.1.call-start = ((), (), s32[]{:S(2)}) async-start(), calls=%async_computation.4 | async-start | bytes 14155776 | tf_op jit(solution)/shard_map/all_gather | solution.py:31
  84.2 127.2 %reduce-scatter.2.cloned.1.call-start = ((), (), s32[]{:S(2)}) async-start(), calls=%async_computation.5 | async-start | bytes 7077888 | tf_op jit(solution)/shard_map/reduce_scatter | solution.py:205
  168.3 63.9 %copy-start.28 = (f32[4,256]{1,0:T(4,128)S(1)}, f32[4,256]{1,0:T(4,128)}, u32[]{:S(2)}) copy-start(f32[4,256]{1,0:T(4,128)} %param.20) | copy-start | bytes 12292
  168.3 65.8 %copy-start.43 = (u32[128]{0:T(128)S(1)}, u32[128]{0:T(128)}, u32[]{:S(2)}) copy-start(u32[128]{0:T(128)} %constant.128) | copy-start | bytes 1540
  168.3 92.1 %copy-start.14 = (bf16[256,256]{1,0:T(8,128)(2,1)S(1)}, bf16[256,256]{1,0:T(8,128)(2,1)}, u32[]{:S(2)}) copy-start(bf16[256,256]{1,0:T(8,128)(2,1)} %param.17) | copy-start | bytes 393220
  168.3 92.5 %copy-start.26 = (s32[256,2]{0,1:T(2,128)S(1)}, s32[256,2]{0,1:T(2,128)}, u32[]{:S(2)}) copy-start(s32[256,2]{0,1:T(2,128)} %param.25) | copy-start | bytes 6148
  168.3 94.0 %copy-start.12 = (bf16[256,128]{1,0:T(8,128)(2,1)S(1)}, bf16[256,128]{1,0:T(8,128)(2,1)}, u32[]{:S(2)}) copy-start(bf16[256,128]{1,0:T(8,128)(2,1)} %param.19) | copy-start | bytes 196612
  168.3 94.0 %copy-start.13 = (bf16[256,128]{1,0:T(8,128)(2,1)S(1)}, bf16[256,128]{1,0:T(8,128)(2,1)}, u32[]{:S(2)}) copy-start(bf16[256,128]{1,0:T(8,128)(2,1)} %param.18) | copy-start | bytes 196612
  168.4 142.9 %all-gather.8.cloned.1.call-start = ((), (), s32[]{:S(2)}) async-start(), calls=%async_computation.6 | async-start | bytes 7077888 | tf_op jit(solution)/shard_map/all_gather | solution.py:212
  260.7 29.9 %copy-start.20 = (bf16[4,64,4,64]{3,2,1,0:T(4,128)(2,1)}, bf16[4,64,4,64]{3,2,1,0:T(4,128)(2,1)S(1)}, u32[]{:S(2)}) copy-start(bf16[4,64,4,64]{3,2,1,0:T(4,128)(2,1)S(1)} %reshape.1071) | copy-start | bytes 393220
  348.1 66.2 %all-to-all-start.2 = ((bf16[16,256,256]{2,1,0:T(8,128)(2,1)}), bf16[16,256,256]{2,1,0:T(8,128)(2,1)}, u32[]{:S(2)}, u32[]{:S(2)}) async-start(bf16[16,256,256]{2,1,0:T(8,128)(2,1)} %bitcast.488), calls=%async_computation.3 | async-start | bytes 4194304 | tf_op jit(solution)/shard_map/all_to_all | solution.py:72
  357.3 36.7 %copy-start.30 = (f32[4]{0:T(128)S(1)}, f32[4]{0:T(128)}, u32[]{:S(2)}) copy-start(f32[4]{0:T(128)} %copy-done.29) | copy-start | bytes 52
  357.3 36.7 %copy-start.32 = (f32[4]{0:T(128)S(1)}, f32[4]{0:T(128)}, u32[]{:S(2)}) copy-start(f32[4]{0:T(128)} %copy-done.31) | copy-start | bytes 52
  357.3 36.7 %copy-start.34 = (f32[4]{0:T(128)S(1)}, f32[4]{0:T(128)}, u32[]{:S(2)}) copy-start(f32[4]{0:T(128)} %get-tuple-element.270) | copy-start | bytes 52
  357.3 36.7 %copy-start.35 = (f32[4]{0:T(128)S(1)}, f32[4]{0:T(128)}, u32[]{:S(2)}) copy-start(f32[4]{0:T(128)} %get-tuple-element.277) | copy-start | bytes 52
  357.3 36.7 %copy-start.37 = (f32[4]{0:T(128)S(1)}, f32[4]{0:T(128)}, u32[]{:S(2)}) copy-start(f32[4]{0:T(128)} %get-tuple-element.271) | copy-start | bytes 52
  357.3 36.7 %copy-start.38 = (f32[4]{0:T(128)S(1)}, f32[4]{0:T(128)}, u32[]{:S(2)}) copy-start(f32[4]{0:T(128)} %get-tuple-element.264) | copy-start | bytes 52
  357.3 36.7 %copy-start.39 = (f32[4]{0:T(128)S(1)}, f32[4]{0:T(128)}, u32[]{:S(2)}) copy-start(f32[4]{0:T(128)} %get-tuple-element.265) | copy-start | bytes 52
  357.3 36.7 %copy-start.40 = (f32[4]{0:T(128)S(1)}, f32[4]{0:T(128)}, u32[]{:S(2)}) copy-start(f32[4]{0:T(128)} %get-tuple-element.266) | copy-start | bytes 52
  357.4 36.7 %copy-start.41 = (f32[4]{0:T(128)S(1)}, f32[4]{0:T(128)}, u32[]{:S(2)}) copy-start(f32[4]{0:T(128)} %get-tuple-element.267) | copy-start | bytes 52
  357.6 43.2 %copy-start.16 = (f32[4,64,64]{2,1,0:T(8,128)S(1)}, f32[4,64,64]{2,1,0:T(8,128)}, u32[]{:S(2)}) copy-start(f32[4,64,64]{2,1,0:T(8,128)} %copy-done.15) | copy-start | bytes 196612
  357.6 43.2 %copy-start.22 = (f32[4,64,1,4]{1,3,0,2:T(4,128)S(1)}, f32[4,64,1,4]{1,3,0,2:T(4,128)}, u32[]{:S(2)}) copy-start(f32[4,64,1,4]{1,3,0,2:T(4,128)} %copy-done.21) | copy-start | bytes 12292
  357.6 43.2 %copy-start.25 = (pred[64,64]{1,0:T(8,128)(4,1)S(1)}, pred[64,64]{1,0:T(8,128)(4,1)}, u32[]{:S(2)}) copy-start(pred[64,64]{1,0:T(8,128)(4,1)} %copy-done.24) | copy-start | bytes 12292
  (27 other events, 251.6 us)
Sparse Core Ops, SparseCore 0:
  84.3 64.9 all-gather.5
  168.5 42.8 reduce-scatter.1
  232.4 37.9 all-gather.7
where the time goes:
time: 431 us; the launch traced here: 424 us
  blocking collectives  134 us (31%)
  waiting for transfers between devices  108 us (25%)
  local copies, waits for them, and re-layouts  81.3 us (19%)
  matrix products  48.9 us (11%)
  other arithmetic  31.2 us (7%)
  between operations  15.5 us (4%)
  starting transfers between devices  4.85 us (1%)
    all_gather x6, blocking collectives, prefix_by_axis(): lax.all_gather(part.astype(kind), axis)  73.8 us
    all_gather x1, waiting for transfers between devices, side_by_side(): lax.all_gather(both, axis, axis=dim, tiled=True)  64.9 us
    reduce_scatter x1, waiting for transfers between devices, body(): lax.psum_scatter(grads[3].reshape(experts, expert_capacity, width).astype...  43 us
    all_to_all x1, blocking collectives, sent_together(): lax.all_to_all(both, axis, split_axis=split_dim, concat_axis=concat_dim,...  30.6 us
    all_to_all x1, blocking collectives, body(): came = lax.all_to_all(summed, SP, split_axis=0, concat_axis=0, tiled=True)  20.8 us
    gather x2, local copies, waits for them, and re-layouts, body(): jnp.take(returned, target, axis=0).astype(jnp.float32)  19.9 us
    mul x3, local copies, waits for them, and re-layouts, body(): cotangent.astype(jnp.float32)[:, None, :] * route_weights[:, :, None]  19.3 us
    reduce_sum x1, other arithmetic, body(): jnp.sum(picked, axis=1)  14.4 us
  transfers between devices with their start and end apart: 4, of which 2 were waited for; matrix products, arithmetic and copies ran while one was open for 13% of the time, Pallas kernels for 0%

commit v1 on v0

v1 whole, which is shorter than its diff:
```python
import jax
import jax.numpy as jnp
from jax import lax
from jax.experimental import pallas as pl
from jax.experimental.pallas import tpu as pltpu
from jax.sharding import Mesh
from jax.sharding import PartitionSpec as P

HEAD_DIM = 64
STATE = 128
SP = ("sp_0", "sp_1")
F32 = jnp.float32
BF16 = jnp.bfloat16
highest = lax.Precision.HIGHEST


def nn(a, b):
    return lax.dot_general(a, b, (((1,), (0,)), ((), ())), preferred_element_type=F32)


def nt(a, b):
    return lax.dot_general(a, b, (((1,), (1,)), ((), ())), preferred_element_type=F32)


def tn(a, b):
    return lax.dot_general(a, b, (((0,), (0,)), ((), ())), preferred_element_type=F32)


def iota(shape, dim):
    return lax.broadcasted_iota(jnp.int32, shape, dim)


def slots(ids_t, experts):
    tokens = ids_t.shape[1]
    e = iota((experts, tokens), 0)
    member = (ids_t[0:1, :] == e) | (ids_t[1:2, :] == e)
    before = (iota((tokens, tokens), 0) < iota((tokens, tokens), 1)).astype(BF16)
    slot = nn(member.astype(BF16), before)
    return jnp.where(member, slot.astype(jnp.int32), -1)


def weight_rows(ids_t, w_t, experts):
    e = iota((experts, ids_t.shape[1]), 0)
    return jnp.where(ids_t[0:1, :] == e, w_t[0:1, :], 0.0) + jnp.where(
        ids_t[1:2, :] == e, w_t[1:2, :], 0.0
    )


def decays(ld):
    heads, tokens = ld.shape
    ld8 = jnp.concatenate([ld, jnp.zeros((8 - heads, tokens), F32)], axis=0)
    upto = (iota((tokens, tokens), 0) <= iota((tokens, tokens), 1)).astype(F32)
    row = lax.dot_general(
        ld8, upto, (((1,), (0,)), ((), ())), precision=highest, preferred_element_type=F32
    )
    col = lax.dot_general(
        upto, ld8, (((0,), (1,)), ((), ())), precision=highest, preferred_element_type=F32
    )
    return row, col


def by_lane(col, tokens, heads):
    lane = iota((tokens, 2 * HEAD_DIM), 1)
    return jnp.concatenate(
        [
            jnp.where(lane < HEAD_DIM, col[:, 2 * p : 2 * p + 1], col[:, 2 * p + 1 : 2 * p + 2])
            for p in range(heads // 2)
        ],
        axis=1,
    )


def span_weights(row, col, h, tokens):
    lower = iota((tokens, tokens), 0) >= iota((tokens, tokens), 1)
    return jnp.exp(jnp.where(lower, col[:, h : h + 1] - row[h : h + 1, :], -1e30))


def mix_local(x, b, c, row, col, heads):
    tokens = x.shape[0]
    scores = nt(c, b)
    first = iota((tokens, 2 * HEAD_DIM), 1) < HEAD_DIM
    ys = []
    for p in range(heads // 2):
        xp = x[:, 128 * p : 128 * p + 128]
        pair = [
            nn((scores * span_weights(row, col, 2 * p + i, tokens)).astype(BF16), xp)
            for i in range(2)
        ]
        ys.append(jnp.where(first, pair[0], pair[1]))
    tails = by_lane(jnp.exp(col[tokens - 1 : tokens, :] - col), tokens, heads)
    end = tn((x.astype(F32) * tails).astype(BF16), b)
    return jnp.concatenate(ys, axis=1), end


def mix_backward(x, b, c, gate, out_grad, y, row, col, entering, leaving, heads):
    tokens = x.shape[0]
    sigma = jax.nn.sigmoid(gate)
    g = out_grad * (gate * sigma)
    d_gate = out_grad * y * sigma * (1.0 + gate * (1.0 - sigma))
    gb = g.astype(BF16)
    scores = nt(c, b)
    first = iota((tokens, 2 * HEAD_DIM), 1) < HEAD_DIM
    d_scores = jnp.zeros((tokens, tokens), F32)
    dxs = []
    for p in range(heads // 2):
        xp = x[:, 128 * p : 128 * p + 128]
        gp = gb[:, 128 * p : 128 * p + 128]
        pair = []
        for i in range(2):
            w = span_weights(row, col, 2 * p + i, tokens)
            mine = first if i == 0 else jnp.logical_not(first)
            d_scores = d_scores + w * nt(jnp.where(mine, gp, jnp.zeros_like(gp)), xp)
            pair.append(tn((scores * w).astype(BF16), gp))
        dxs.append(jnp.where(first, pair[0], pair[1]))
    tails = by_lane(jnp.exp(col[tokens - 1 : tokens, :] - col), tokens, heads)
    leads = by_lane(jnp.exp(col), tokens, heads)
    d_x = jnp.concatenate(dxs, axis=1) + tails * nt(b, leaving)
    ds = d_scores.astype(BF16)
    d_c = nn(ds, b) + nn((g * leads).astype(BF16), entering)
    d_b = tn(ds, c) + nn((x.astype(F32) * tails).astype(BF16), leaving)
    return d_x, d_b, d_c, d_gate


def prep_kernel(experts, cap, heads, ids, wts, mixed, cot, ld, x, b, c, send, hot, y, end):
    slot = slots(ids[...], experts)
    weights = weight_rows(ids[...], wts[...], experts)
    tokens = slot.shape[1]
    place = iota((cap, tokens), 0)
    for e in range(experts):
        mine = place == slot[e : e + 1, :]
        one = mine.astype(BF16)
        hot[e * cap : (e + 1) * cap, :] = one
        send[e, 0:cap, :] = nn(one, mixed[...]).astype(BF16)
        w = jnp.sum(jnp.where(mine, weights[e : e + 1, :], 0.0), axis=1, keepdims=True)
        send[e, cap : 2 * cap, :] = (nn(one, cot[...]) * w).astype(BF16)
    row, col = decays(ld[...])
    inner, last = mix_local(x[...], b[...], c[...], row, col, heads)
    y[...] = inner
    end[...] = last


def combine_kernel(hot, came, cot, out):
    out[...] = (cot[...].astype(F32) + tn(hot[...], came[...])).astype(BF16)


def carried_kernel(heads, ld, c, gate, y_inner, entering, out_grad, y, gated, back):
    row, col = decays(ld[...])
    tokens = y_inner.shape[0]
    leads = by_lane(jnp.exp(col), tokens, heads)
    whole = y_inner[...] + leads * nt(c[...], entering[...])
    g = gate[...].astype(F32)
    silu = g * jax.nn.sigmoid(g)
    y[...] = whole
    gated[...] = (whole * silu).astype(BF16)
    back[...] = tn((out_grad[...] * silu * leads).astype(BF16), c[...])


def backward_kernel(heads, ld, x, b, c, gate, og, y, entering, leaving, dx, db, dc, dg):
    row, col = decays(ld[...])
    d_x, d_b, d_c, d_g = mix_backward(
        x[...],
        b[...],
        c[...],
        gate[...].astype(F32),
        og[...],
        y[...],
        row,
        col,
        entering[...],
        leaving[...],
        heads,
    )
    dx[...] = d_x.astype(BF16)
    db[...] = d_b.astype(BF16)
    dc[...] = d_c.astype(BF16)
    dg[...] = d_g.astype(BF16)


def call(kernel, outs, *args, name):
    vmem = pl.BlockSpec(memory_space=pltpu.VMEM)
    return pl.pallas_call(
        kernel,
        out_shape=[jax.ShapeDtypeStruct(s, d) for s, d in outs],
        in_specs=[vmem] * len(args),
        out_specs=[vmem] * len(outs),
        compiler_params=pltpu.CompilerParams(vmem_limit_bytes=24 * 2**20),
        name=name,
    )(*args)


def nothing_yet(array, identity):
    return jax.tree.map(
        lambda a, e: jnp.broadcast_to(jnp.asarray(e, a.dtype), a.shape), array, identity
    )


def prefix_by_axis(array, axes, combine, identity, reverse):
    before = start = nothing_yet(array, identity)
    so_far = array
    for axis in reversed(axes):
        length, position = (lax.axis_size(axis), lax.axis_index(axis))
        pieces = jax.tree.map(
            lambda part, kind: lax.all_gather(part.astype(kind), axis),
            so_far,
            (BF16, BF16),
        )
        inside, so_far = (start, start)
        for k in reversed(range(length)) if reverse else range(length):
            passed = k > position if reverse else k < position
            so_far = combine(
                so_far, jax.tree.map(lambda part, own: part[k].astype(own.dtype), pieces, array)
            )
            inside = jax.tree.map(lambda new, old: jnp.where(passed, new, old), so_far, inside)
        before = combine(inside, before)
    return before


def forward_join(earlier, later):
    return (earlier[0] + later[0], jnp.exp(later[0])[..., None, None] * earlier[1] + later[1])


def backward_join(earlier, later):
    return (earlier[0] + later[0], later[1] + jnp.exp(later[0])[..., None, None] * earlier[1])


def expert_backward(rows, scaled, gate_weight, up_weight, down_weight):
    gate_pre = nn(rows, gate_weight)
    up_pre = nn(rows, up_weight)
    sigma = jax.nn.sigmoid(gate_pre)
    hidden = (gate_pre * sigma * up_pre).astype(BF16)
    d_hidden = nt(scaled, down_weight)
    d_gate = (d_hidden * up_pre * sigma * (1.0 + gate_pre * (1.0 - sigma))).astype(BF16)
    d_up = (d_hidden * (gate_pre * sigma)).astype(BF16)
    portion = nt(d_gate, gate_weight) + nt(d_up, up_weight)
    return (
        tn(rows, d_gate).astype(BF16),
        tn(rows, d_up).astype(BF16),
        tn(hidden, scaled).astype(BF16),
        portion.astype(BF16),
    )


def body(
    token_values,
    write_keys,
    read_keys,
    log_decay,
    out_gate,
    out_proj,
    mixed,
    cotangent,
    route_ids,
    route_weights,
    w_gate,
    w_up,
    w_down,
):
    tokens, width = mixed.shape
    experts = lax.axis_size(SP)
    cap = 3 * tokens // experts
    places = experts * cap
    heads = log_decay.shape[0]
    channels = token_values.shape[1]
    share = width // lax.axis_size("tp")
    offset = lax.axis_index("tp") * share
    mixed_part = lax.dynamic_slice_in_dim(mixed, offset, share, 1)
    cot_part = lax.dynamic_slice_in_dim(cotangent, offset, share, 1)

    def prep(*refs):
        prep_kernel(experts, cap, heads, *refs)

    send, hot, y_inner, local_end = call(
        prep,
        [
            ((experts, 2 * cap, share), BF16),
            ((places, tokens), BF16),
            ((tokens, channels), F32),
            ((channels, STATE), F32),
        ],
        route_ids.T,
        route_weights.T,
        mixed_part,
        cot_part,
        log_decay,
        token_values,
        write_keys,
        read_keys,
        name="prep",
    )
    got = lax.all_to_all(send, SP, split_axis=0, concat_axis=0, tiled=True)
    rows = lax.all_gather(got, "tp", axis=2, tiled=True)
    grads = expert_backward(
        rows[:, :cap].reshape(places, width),
        rows[:, cap:].reshape(places, width),
        w_gate[0],
        w_up[0],
        w_down[0],
    )
    summed = lax.psum_scatter(
        grads[3].reshape(experts, cap, width), "tp", scatter_dimension=2, tiled=True
    )
    came = lax.all_to_all(summed, SP, split_axis=0, concat_axis=0, tiled=True)
    (grad_part,) = call(
        combine_kernel,
        [((tokens, share), BF16)],
        hot,
        came.reshape(places, share),
        cot_part,
        name="combine",
    )
    grad_mixed = lax.all_gather(grad_part, "tp", axis=1, tiled=True)
    out_grad = nn(grad_mixed, out_proj)

    total = jnp.sum(log_decay, axis=1)
    zero_total = jnp.zeros_like(total)
    zero_state = jnp.zeros((heads, HEAD_DIM, STATE), F32)
    shape = (heads, HEAD_DIM, STATE)
    entering = prefix_by_axis(
        (total, local_end.reshape(shape)), SP, forward_join, (zero_total, zero_state), False
    )[1]
    entering = entering.reshape(channels, STATE).astype(BF16)

    def carried(*refs):
        carried_kernel(heads, *refs)

    y, gated, local_back = call(
        carried,
        [((tokens, channels), F32), ((tokens, channels), BF16), ((channels, STATE), F32)],
        log_decay,
        read_keys,
        out_gate,
        y_inner,
        entering,
        out_grad,
        name="carried",
    )
    proj_part = tn(grad_mixed, gated).astype(BF16).reshape(experts, -1, channels)
    proj_came = lax.all_to_all(proj_part, SP, split_axis=0, concat_axis=0, tiled=True)
    proj_grad = proj_came.astype(F32).sum(axis=0)
    leaving = prefix_by_axis(
        (total, local_back.reshape(shape)), SP, backward_join, (zero_total, zero_state), True
    )[1]
    leaving = leaving.reshape(channels, STATE).astype(BF16)

    def backward(*refs):
        backward_kernel(heads, *refs)

    d_values, d_writes, d_reads, d_gate = call(
        backward,
        [(a.shape, BF16) for a in (token_values, write_keys, read_keys, out_gate)],
        log_decay,
        token_values,
        write_keys,
        read_keys,
        out_gate,
        out_grad,
        y,
        entering,
        leaving,
        name="backward",
    )
    return (
        d_values,
        d_writes,
        d_reads,
        d_gate,
        proj_grad,
        grads[0][None],
        grads[1][None],
        grads[2][None],
    )


def solution(mesh):
    finer = Mesh(mesh.devices.reshape(4, 4, mesh.shape["tp"]), ("sp_0", "sp_1", "tp"))
    return jax.shard_map(
        body,
        mesh=finer,
        in_specs=(
            P(SP, "tp"),
            P(SP, "tp"),
            P(SP, "tp"),
            P("tp", SP),
            P(SP, "tp"),
            P(None, "tp"),
            P(SP, None),
            P(SP, None),
            P(SP, None),
            P(SP, None),
            P(SP, None, "tp"),
            P(SP, None, "tp"),
            P(SP, "tp", None),
        ),
        out_specs=(
            P(SP, "tp"),
            P(SP, "tp"),
            P(SP, "tp"),
            P(SP, "tp"),
            P(SP, "tp"),
            P(SP, None, "tp"),
            P(SP, None, "tp"),
            P(SP, "tp", None),
        ),
        check_vma=False,
    )
```

time: 431 us -> 324 us (0.75); the launches traced: 424 us -> 324 us
  local copies, waits for them, and re-layouts: 81.3 us -> 21.5 us
  other arithmetic: 31.2 us -> 4.1 us
  matrix products: 48.9 us -> 36.3 us
  Pallas kernels: 0 us -> 7.02 us
  blocking collectives: 134 us -> 127 us
    gather x2 -> x0, local copies, waits for them, and re-layouts: 19.9 us -> none  [body(): jnp.take(returned, target, axis=0).astype(jnp.float32)]
    mul x14 -> x32, local copies, waits for them, and re-layouts: 22.3 us -> 6.45 us  [the longest x10 3.6 us: backward_join(): jnp.exp(later[0])[..., None, None] * earlier[1]]
    reduce_sum x3 -> x2, other arithmetic: 17 us -> 2.72 us  [the longest x1 2.6 us: body(): proj_grad = proj_came.astype(F32).sum(axis=0)]
    dot_general x24 -> x10, matrix products: 48.9 us -> 36.3 us  [the longest x4 20.3 us: tn(): lax.dot_general(a, b, (((0,), (0,)), ((), ())), preferred_element_type=F32)]
    reshape x8 -> x0, local copies, waits for them, and re-layouts: 8.75 us -> none  [the longest x1 7.2 us: body(): copies = jnp.repeat(mixed, 2, axis=0)]
    pallas_call x0 -> x4, Pallas kernels: none -> 7.02 us  [call(): pl.pallas_call(kernel, out_shape=[jax.ShapeDtypeStruct(s, d) for s, d in...]
    all_gather x6, blocking collectives: 73.8 us -> 67.3 us  [prefix_by_axis(): lax.all_gather(part.astype(kind), axis)]
    broadcast_in_dim x1 -> x0, local copies, waits for them, and re-layouts: 6.06 us -> none  [body(): copies = jnp.repeat(mixed, 2, axis=0)]
  transfers between devices with their start and end apart: 4 -> 4, of which waited for: 2 -> 2; matrix products, arithmetic and copies ran while one was open for 13% -> 8% of each run, Pallas kernels for 0% -> 1%
where the time goes in v1:
time: 324 us
  blocking collectives  127 us (39%)
  waiting for transfers between devices  108 us (33%)
  matrix products  36.3 us (11%)
  local copies, waits for them, and re-layouts  21.5 us (7%)
  between operations  14.9 us (5%)
  Pallas kernels  7.02 us (2%)
  starting transfers between devices  4.55 us (1%)
  other arithmetic  4.1 us (1%)
    all_gather x6, blocking collectives, prefix_by_axis(): lax.all_gather(part.astype(kind), axis)  67.3 us
    all_gather x1, waiting for transfers between devices, body(): rows = lax.all_gather(got, 'tp', axis=2, tiled=True)  65 us
    reduce_scatter x1, waiting for transfers between devices, body(): lax.psum_scatter(grads[3].reshape(experts, cap, width), 'tp', scatter_dim...  43 us
    all_to_all x1, blocking collectives, body(): got = lax.all_to_all(send, SP, split_axis=0, concat_axis=0, tiled=True)  30.7 us
    all_to_all x1, blocking collectives, body(): came = lax.all_to_all(summed, SP, split_axis=0, concat_axis=0, tiled=True)  20.7 us
    dot_general x4, matrix products, tn(): lax.dot_general(a, b, (((0,), (0,)), ((), ())), preferred_element_type=F32)  20.3 us
    dot_general x3, matrix products, nt(): lax.dot_general(a, b, (((1,), (1,)), ((), ())), preferred_element_type=F32)  9.92 us
    unnamed x1, blocking collectives  8.47 us
  transfers between devices with their start and end apart: 4, of which 2 were waited for; matrix products, arithmetic and copies ran while one was open for 8% of the time, Pallas kernels for 1%

profile of v1, /device:TPU:0, one launch (start us, length us, event | category | flops | bytes accessed | tf_op | source)
XLA Modules:
  0.0 323.6 jit_solution(10961667423038261246)
XLA Ops:
  13.1 2.8 prep.1
  15.9 30.7 %all_to_all.15 = bf16[16,96,512]{2,1,0:T(8,128)(2,1)} all-to-all(bf16[16,96,512]{2,1,0:T(8,128)(2,1)S(1)} %get-tuple-element.20), channel_id=1, replica_groups=mesh['sp_0'=4,'sp_1'=4,'tp'=8] {'sp_0','sp_1'}, dimensions={0} | all-to-all | bytes 3145728 | tf_op jit(solution)/shard_map/all_to_all | solution.py:290
  46.6 65.0 %all-gather.6.cloned.1.call-done = bf16[16,96,4096]{2,1,0:T(8,128)(2,1)} async-done(((bf16[16,96,512]{2,1,0:T(8,128)(2,1)}), bf16[16,96,4096]{2,1,0:T(8,128)(2,1)}) %all-gather.6.cloned.1.call-update) | async-done | bytes 12582928 | tf_op jit(solution)/shard_map/all_gather | solution.py:291
  111.7 5.6 %fusion.60 = (bf16[16,48,4096]{2,1,0:T(8,128)(2,1)S(1)}, bf16[16,48,4096]{2,1,0:T(8,128)(2,1)S(1)}) fusion(bf16[16,96,4096]{2,1,0:T(8,128)(2,1)} %all-gather.6.cloned.1.call-done), kind=kLoop, calls=%fused_computation.126 | loop fusion | bytes 25165824 | tf_op jit(solution)/shard_map/slice | solution.py:294
  123.5 2.0 multiply_convert_fusion.1
  125.5 1.8 fusion.3
  127.4 6.1 %add_convert_fusion = bf16[768,4096]{1,0:T(8,128)(2,1)} fusion(f32[768,4096]{1,0:T(8,128)S(1)} %fusion.3, bf16[768,256]{1,0:T(8,128)(2,1)S(1)} %get-tuple-element.32, bf16[1,4096,256]{2,1,0:T(8,128)(2,1)} %param.24), kind=kOutput, calls=%fused_computation | convolution fusion | flops 1616904192 | bytes 21364736 | tf_op jit(solution)/shard_map/dot_general | solution.py:22
  133.6 43.0 %reduce-scatter.2.cloned.1.call-done = bf16[16,48,512]{2,1,0:T(8,128)(2,1)} async-done(((bf16[16,48,4096]{2,1,0:T(8,128)(2,1)}), bf16[16,48,512]{2,1,0:T(8,128)(2,1)}) %reduce-scatter.2.cloned.1.call-update) | async-done | bytes 786448 | tf_op jit(solution)/shard_map/reduce_scatter | solution.py:299
  176.5 20.7 %all_to_all.16 = bf16[16,48,512]{2,1,0:T(8,128)(2,1)S(1)} all-to-all(bf16[16,48,512]{2,1,0:T(8,128)(2,1)} %reduce-scatter.2.cloned.1.call-done), channel_id=1, replica_groups=mesh['sp_0'=4,'sp_1'=4,'tp'=8] {'sp_0','sp_1'}, dimensions={0} | all-to-all | bytes 1572864 | tf_op jit(solution)/shard_map/all_to_all | solution.py:302
  200.0 8.5 %all-reduce = bf16[16]{0:T(256)(128)(2,1)S(1)} all-reduce(bf16[16]{0:T(256)(128)(2,1)S(1)} %dynamic-update-slice), channel_id=2, replica_groups=mesh['sp_0'=4,'sp_1'=4,'tp'=8] {'sp_1'}, use_global_device_ids=true, to_apply=%add | all-reduce | flops 16 | bytes 64
  208.6 8.0 %all-gather.2 = bf16[4,1,4]{2,1,0:T(2,128)(2,1)S(1)} all-gather(bf16[1,1,4]{2,1,0:T(2,128)(2,1)S(1)} %get-tuple-element.63), channel_id=1, replica_groups=mesh['sp_0'=4,'sp_1'=4,'tp'=8] {'sp_0'}, dimensions={0}, use_global_device_ids=true | all-gather | bytes 40 | tf_op jit(solution)/shard_map/all_gather | solution.py:203
  216.6 7.9 %all-gather.1 = bf16[4,1,4]{2,1,0:T(2,128)(2,1)S(1)} all-gather(bf16[1,1,4]{2,1,0:T(2,128)(2,1)S(1)} %get-tuple-element.64), channel_id=1, replica_groups=mesh['sp_0'=4,'sp_1'=4,'tp'=8] {'sp_0'}, dimensions={0}, use_global_device_ids=true | all-gather | bytes 40 | tf_op jit(solution)/shard_map/all_gather | solution.py:203
  231.2 12.3 %all_gather.40 = bf16[4,4,64,128]{3,2,1,0:T(8,128)(2,1)S(1)} all-gather(bf16[1,4,64,128]{3,2,1,0:T(8,128)(2,1)S(1)} %bitcast.167), channel_id=1, replica_groups=mesh['sp_0'=4,'sp_1'=4,'tp'=8] {'sp_1'}, dimensions={0}, use_global_device_ids=true | all-gather | bytes 327680 | tf_op jit(solution)/shard_map/all_gather | solution.py:203
  243.6 12.3 %all_gather.41 = bf16[4,4,64,128]{3,2,1,0:T(8,128)(2,1)S(1)} all-gather(bf16[1,4,64,128]{3,2,1,0:T(8,128)(2,1)S(1)} %add_convert_fusion.2), channel_id=1, replica_groups=mesh['sp_0'=4,'sp_1'=4,'tp'=8] {'sp_0'}, dimensions={0}, use_global_device_ids=true | all-gather | bytes 327680 | tf_op jit(solution)/shard_map/all_gather | solution.py:203
  256.4 6.1 %fusion.1 = bf16[1,4096,256]{2,1,0:T(8,128)(2,1)} fusion(bf16[768,4096]{1,0:T(8,128)(2,1)} %bitcast.165, bf16[768,256]{1,0:T(8,128)(2,1)S(1)} %copy-done.23), kind=kOutput, calls=%fused_computation.6 | convolution fusion | flops 1611661312 | bytes 8781824 | tf_op jit(solution)/shard_map/dot_general | solution.py:26
  262.5 2.4 fusion.63.refs_5_
  265.9 2.1 convolution_convert_fusion
  268.0 4.4 %all-to-all-start.2 = ((bf16[16,256,256]{2,1,0:T(8,128)(2,1)}), bf16[16,256,256]{2,1,0:T(8,128)(2,1)}, u32[]{:S(2)}, u32[]{:S(2)}) async-start(bf16[16,256,256]{2,1,0:T(8,128)(2,1)} %bitcast.42), calls=%async_computation.3 | async-start | bytes 4194304 | tf_op jit(solution)/shard_map/all_to_all | solution.py:338
  272.4 6.1 %fusion = bf16[1,4096,256]{2,1,0:T(8,128)(2,1)} fusion(bf16[768,4096]{1,0:T(8,128)(2,1)} %bitcast.166, bf16[768,256]{1,0:T(8,128)(2,1)S(1)} %get-tuple-element.33), kind=kOutput, calls=%fused_computation.5 | convolution fusion | flops 1611661312 | bytes 8781824 | tf_op jit(solution)/shard_map/dot_general | solution.py:26
  278.6 6.0 %fusion.2 = bf16[1,256,4096]{2,1,0:T(8,128)(2,1)} fusion(bf16[768,4096]{1,0:T(8,128)(2,1)} %bitcast.161, f32[768,256]{1,0:T(8,128)S(1)} %copy-done.19, f32[768,256]{1,0:T(8,128)S(1)} %copy-done.17), kind=kOutput, calls=%fused_computation.7 | convolution fusion | flops 1612840960 | bytes 9961472 | tf_op jit(solution)/shard_map/dot_general | solution.py:26
  284.6 14.4 %all_gather.42 = bf16[4,4,64,128]{3,2,1,0:T(8,128)(2,1)S(1)} all-gather(bf16[1,4,64,128]{3,2,1,0:T(8,128)(2,1)S(1)} %bitcast.168), channel_id=1, replica_groups=mesh['sp_0'=4,'sp_1'=4,'tp'=8] {'sp_1'}, dimensions={0}, use_global_device_ids=true | all-gather | bytes 327680 | tf_op jit(solution)/shard_map/all_gather | solution.py:203
  299.2 12.5 %all_gather.43 = bf16[4,4,64,128]{3,2,1,0:T(8,128)(2,1)S(1)} all-gather(bf16[1,4,64,128]{3,2,1,0:T(8,128)(2,1)S(1)} %add_convert_fusion.1), channel_id=1, replica_groups=mesh['sp_0'=4,'sp_1'=4,'tp'=8] {'sp_0'}, dimensions={0}, use_global_device_ids=true | all-gather | bytes 327680 | tf_op jit(solution)/shard_map/all_gather | solution.py:203
  312.2 2.2 backward.1
  314.4 2.6 convert_reduce_fusion
  (142 shorter events, 23.2 us)
Async XLA Ops:
  7.2 110.1 %copy-start = (bf16[1,4096,256]{2,1,0:T(8,128)(2,1)S(1)}, bf16[1,4096,256]{2,1,0:T(8,128)(2,1)}, u32[]{:S(2)}) copy-start(bf16[1,4096,256]{2,1,0:T(8,128)(2,1)} %param.23) | copy-start | bytes 6291460
  7.2 104.5 %all-gather.6.cloned.1.call-start = ((), (), s32[]{:S(2)}) async-start(), calls=%async_computation.4 | async-start | bytes 14155776 | tf_op jit(solution)/shard_map/all_gather | solution.py:291
  46.6 130.0 %reduce-scatter.2.cloned.1.call-start = ((), (), s32[]{:S(2)}) async-start(), calls=%async_computation.5 | async-start | bytes 7077888 | tf_op jit(solution)/shard_map/reduce_scatter | solution.py:299
  133.5 64.9 %copy-start.10 = (f32[4,256]{1,0:T(4,128)S(1)}, f32[4,256]{1,0:T(4,128)}, u32[]{:S(2)}) copy-start(f32[4,256]{1,0:T(4,128)} %refs_0_.3) | copy-start | bytes 12292
  133.5 65.0 %copy-start.38 = (u32[128]{0:T(128)S(1)}, u32[128]{0:T(128)}, u32[]{:S(2)}) copy-start(u32[128]{0:T(128)} %constant.36) | copy-start | bytes 1540
  133.5 129.0 %all-gather.8.cloned.1.call-start = ((), (), s32[]{:S(2)}) async-start(), calls=%async_computation.6 | async-start | bytes 2359296 | tf_op jit(solution)/shard_map/all_gather | solution.py:311
  198.4 58.0 %copy-start.23 = (bf16[768,256]{1,0:T(8,128)(2,1)S(1)}, bf16[768,256]{1,0:T(8,128)(2,1)}, u32[]{:S(2)}) copy-start(bf16[768,256]{1,0:T(8,128)(2,1)} %copy-done.22) | copy-start | bytes 1179652
  225.3 18.3 %copy-start.24 = (f32[4]{0:T(128)}, f32[4]{0:T(128)S(1)}, u32[]{:S(2)}) copy-start(f32[4]{0:T(128)S(1)} %get-tuple-element.66) | copy-start | bytes 52
  256.4 6.1 %copy-start.20 = (bf16[4096,256]{1,0:T(8,128)(2,1)S(1)}, bf16[4096,256]{1,0:T(8,128)(2,1)}, u32[]{:S(2)}) copy-start(bf16[4096,256]{1,0:T(8,128)(2,1)} %param.18) | copy-start | bytes 6291460
  268.0 46.5 %all-to-all-start.2 = ((bf16[16,256,256]{2,1,0:T(8,128)(2,1)}), bf16[16,256,256]{2,1,0:T(8,128)(2,1)}, u32[]{:S(2)}, u32[]{:S(2)}) async-start(bf16[16,256,256]{2,1,0:T(8,128)(2,1)} %bitcast.42), calls=%async_computation.3 | async-start | bytes 4194304 | tf_op jit(solution)/shard_map/all_to_all | solution.py:338
  272.4 6.1 %copy-start.17 = (f32[768,256]{1,0:T(8,128)S(1)}, f32[768,256]{1,0:T(8,128)}, u32[]{:S(2)}) copy-start(f32[768,256]{1,0:T(8,128)} %copy-done.16) | copy-start | bytes 2359300
  272.4 6.1 %copy-start.19 = (f32[768,256]{1,0:T(8,128)S(1)}, f32[768,256]{1,0:T(8,128)}, u32[]{:S(2)}) copy-start(f32[768,256]{1,0:T(8,128)} %copy-done.18) | copy-start | bytes 2359300
  278.5 20.5 %copy-start.25 = (f32[4]{0:T(128)S(1)}, f32[4]{0:T(128)}, u32[]{:S(2)}) copy-start(f32[4]{0:T(128)} %copy-done.24) | copy-start | bytes 52
  278.5 20.5 %copy-start.27 = (f32[4]{0:T(128)S(1)}, f32[4]{0:T(128)}, u32[]{:S(2)}) copy-start(f32[4]{0:T(128)} %copy-done.26) | copy-start | bytes 52
  278.5 20.5 %copy-start.29 = (f32[4]{0:T(128)S(1)}, f32[4]{0:T(128)}, u32[]{:S(2)}) copy-start(f32[4]{0:T(128)} %copy-done.28) | copy-start | bytes 52
  284.6 27.2 %copy-start.30 = (f32[256]{0:T(256)S(1)}, f32[256]{0:T(256)}, u32[]{:S(2)}) copy-start(f32[256]{0:T(256)} %mul.353) | copy-start | bytes 3076
  284.6 27.2 %copy-start.31 = (f32[256]{0:T(256)S(1)}, f32[256]{0:T(256)}, u32[]{:S(2)}) copy-start(f32[256]{0:T(256)} %mul.335) | copy-start | bytes 3076
  284.6 27.2 %copy-start.32 = (f32[256]{0:T(256)S(1)}, f32[256]{0:T(256)}, u32[]{:S(2)}) copy-start(f32[256]{0:T(256)} %mul.359) | copy-start | bytes 3076
  284.6 27.2 %copy-start.33 = (f32[256]{0:T(256)S(1)}, f32[256]{0:T(256)}, u32[]{:S(2)}) copy-start(f32[256]{0:T(256)} %mul.356) | copy-start | bytes 3076
  284.6 27.2 %copy-start.34 = (f32[256]{0:T(256)S(1)}, f32[256]{0:T(256)}, u32[]{:S(2)}) copy-start(f32[256]{0:T(256)} %mul.364) | copy-start | bytes 3076
  284.6 27.2 %copy-start.35 = (f32[256]{0:T(256)S(1)}, f32[256]{0:T(256)}, u32[]{:S(2)}) copy-start(f32[256]{0:T(256)} %mul.345) | copy-start | bytes 3076
  284.6 27.2 %copy-start.36 = (f32[256]{0:T(256)S(1)}, f32[256]{0:T(256)}, u32[]{:S(2)}) copy-start(f32[256]{0:T(256)} %mul.339) | copy-start | bytes 3076
  284.6 27.6 %copy-start.5 = (bf16[256,256]{1,0:T(8,128)(2,1)S(1)}, bf16[256,256]{1,0:T(8,128)(2,1)}, u32[]{:S(2)}) copy-start(bf16[256,256]{1,0:T(8,128)(2,1)} %refs_1_.3) | copy-start | bytes 393220
  284.6 27.6 %copy-start.8 = (bf16[256,128]{1,0:T(8,128)(2,1)S(1)}, bf16[256,128]{1,0:T(8,128)(2,1)}, u32[]{:S(2)}) copy-start(bf16[256,128]{1,0:T(8,128)(2,1)} %refs_2_.3) | copy-start | bytes 196612
  (19 other events, 50.6 us)
Sparse Core Ops, SparseCore 0:
  46.7 64.9 all-gather.5
  133.6 42.8 reduce-scatter.1
  198.5 22.3 all-gather.7

commit v2 on v1

--- a/solution.py
+++ b/solution.py
@@ -121,28 +121,6 @@
     return d_x, d_b, d_c, d_gate
 
 
-def prep_kernel(experts, cap, heads, ids, wts, mixed, cot, ld, x, b, c, send, hot, y, end):
-    slot = slots(ids[...], experts)
-    weights = weight_rows(ids[...], wts[...], experts)
-    tokens = slot.shape[1]
-    place = iota((cap, tokens), 0)
-    for e in range(experts):
-        mine = place == slot[e : e + 1, :]
-        one = mine.astype(BF16)
-        hot[e * cap : (e + 1) * cap, :] = one
-        send[e, 0:cap, :] = nn(one, mixed[...]).astype(BF16)
-        w = jnp.sum(jnp.where(mine, weights[e : e + 1, :], 0.0), axis=1, keepdims=True)
-        send[e, cap : 2 * cap, :] = (nn(one, cot[...]) * w).astype(BF16)
-    row, col = decays(ld[...])
-    inner, last = mix_local(x[...], b[...], c[...], row, col, heads)
-    y[...] = inner
-    end[...] = last
-
-
-def combine_kernel(hot, came, cot, out):
-    out[...] = (cot[...].astype(F32) + tn(hot[...], came[...])).astype(BF16)
-
-
 def carried_kernel(heads, ld, c, gate, y_inner, entering, out_grad, y, gated, back):
     row, col = decays(ld[...])
     tokens = y_inner.shape[0]
@@ -174,6 +152,492 @@
     db[...] = d_b.astype(BF16)
     dc[...] = d_c.astype(BF16)
     dg[...] = d_g.astype(BF16)
+
+
+MESH = pl.DeviceIdType.MESH
+GROUPS_OF = 4
+
+
+def remote(src, dst, send, recv, device):
+    return pltpu.make_async_remote_copy(
+        src_ref=src, dst_ref=dst, send_sem=send, recv_sem=recv, device_id=device, device_id_type=MESH
+    )
+
+
+def moe_kernel(
+    heads,
+    ids,
+    wts,
+    ld,
+    x_in,
+    b_in,
+    c_in,
+    mixed,
+    cot,
+    wg_hbm,
+    wu_hbm,
+    wd_hbm,
+    gm,
+    y_out,
+    end_out,
+    gg_hbm,
+    gu_hbm,
+    gd_hbm,
+    mixed_q,
+    cot_q,
+    cot_own,
+    wg,
+    wu,
+    wd,
+    slot_ref,
+    weight_ref,
+    hot,
+    sendbuf,
+    rows,
+    act,
+    dgate,
+    dup,
+    part,
+    part_in,
+    q1,
+    y1,
+    q2,
+    y2,
+    fin,
+    ret,
+    gg,
+    gu,
+    gd,
+    local,
+    a_send,
+    a_recv,
+    yr_send,
+    yr_recv,
+    ys_send,
+    ys_recv,
+    pa_send,
+    pa_recv,
+    pn_send,
+    pn_recv,
+    d_send,
+    d_recv,
+    s1_send,
+    s1_recv,
+    s2_send,
+    s2_recv,
+    c_send,
+    c_recv,
+    g_send,
+    g_recv,
+):
+    z, x, t = lax.axis_index("sp_0"), lax.axis_index("sp_1"), lax.axis_index("tp")
+    s = 4 * z + x
+    y, core = t // 2, t % 2
+    quarter = t % 4
+    beside = (quarter + 2) % 4
+    partner_q = quarter + 1 - 2 * core
+    partner_beside = (partner_q + 2) % 4
+    up, down, partner = (z, x, (t + 2) % 8), (z, x, (t + 6) % 8), (z, x, t + 1 - 2 * core)
+    tokens, width = mixed.shape
+    experts, _, cap, share = sendbuf.shape
+    own = width // 8
+
+    loads = [
+        pltpu.make_async_copy(mixed.at[:, pl.ds(quarter * share, share)], mixed_q, local.at[0]),
+        pltpu.make_async_copy(cot.at[:, pl.ds(quarter * share, share)], cot_q, local.at[1]),
+        pltpu.make_async_copy(cot.at[:, pl.ds(t * own, own)], cot_own, local.at[2]),
+        pltpu.make_async_copy(wg_hbm, wg, local.at[3]),
+        pltpu.make_async_copy(wu_hbm, wu, local.at[4]),
+        pltpu.make_async_copy(wd_hbm, wd, local.at[5]),
+    ]
+    for load in loads:
+        load.start()
+
+    barrier = pltpu.get_barrier_semaphore()
+
+    def greet(k, carry):
+        j = (s + k) % experts
+        pl.semaphore_signal(barrier, inc=1, device_id=(j // 4, j % 4, t), device_id_type=MESH)
+        return carry
+
+    lax.fori_loop(1, experts, greet, 0)
+    for device in (up, down, partner):
+        pl.semaphore_signal(barrier, inc=1, device_id=device, device_id_type=MESH)
+
+    slot_ref[...] = slots(ids[...], experts)
+    weight_ref[...] = weight_rows(ids[...], wts[...], experts)
+    loads[0].wait()
+    loads[1].wait()
+    pl.semaphore_wait(barrier, experts - 1 + 3)
+
+    def to_expert(e):
+        return remote(
+            sendbuf.at[e], rows.at[quarter, s], a_send.at[e], a_recv.at[s], (e // 4, e % 4, t)
+        )
+
+    def build(g, carry):
+        block = (z + g) % 4
+        place = iota((cap, tokens), 0)
+        ones, ws = [], []
+        for k in range(4):
+            e = 4 * block + k
+            mine = place == slot_ref[pl.ds(e, 1), :]
+            one = mine.astype(BF16)
+            hot[e] = one
+            ones.append(one)
+            w = jnp.where(mine, weight_ref[pl.ds(e, 1), :], 0.0)
+            ws.append(jnp.sum(w, axis=1, keepdims=True))
+        one = jnp.concatenate(ones, axis=0)
+        w = jnp.concatenate(ws, axis=0)
+        here = pl.ds(4 * block, 4)
+        sendbuf[here, 0] = nn(one, mixed_q[...]).astype(BF16).reshape(4, cap, share)
+        sendbuf[here, 1] = (nn(one, cot_q[...]) * w).astype(BF16).reshape(4, cap, share)
+        for j in range(4):
+            e = 4 * block + (x + j) % 4
+            if j > 0:
+                to_expert(e).start()
+            else:
+
+                @pl.when(g > 0)
+                def _():
+                    to_expert(e).start()
+
+        return carry
+
+    lax.fori_loop(0, 4, build, 0)
+    rows[quarter, s] = sendbuf[s]
+
+    row, col = decays(ld[...])
+    inner, last = mix_local(x_in[...], b_in[...], c_in[...], row, col, heads)
+    y_out[...] = inner
+    end_out[...] = last
+    for load in loads[2:]:
+        load.wait()
+
+    def source(g, j):
+        return 4 * ((z + 4 - g) % 4) + (x + 4 - j) % 4
+
+    def arrived(src):
+        return remote(sendbuf.at[src], rows.at[quarter, src], a_send.at[src], a_recv.at[src], up)
+
+    def rows_up(src, q):
+        return remote(
+            rows.at[q, src, 0], rows.at[q, src, 0], yr_send.at[src], yr_recv.at[src], up
+        )
+
+    def scaled_down(src, q):
+        return remote(
+            rows.at[q, src, 1], rows.at[q, src, 1], ys_send.at[src], ys_recv.at[src], down
+        )
+
+    def across(src, q):
+        return remote(rows.at[q, src], rows.at[q, src], pa_send.at[src], pa_recv.at[src], partner)
+
+    def across_beside(src, q):
+        return remote(rows.at[q, src], rows.at[q, src], pn_send.at[src], pn_recv.at[src], partner)
+
+    def forward_own(g):
+        for j in range(4):
+            src = source(g, j)
+            if j > 0:
+                arrived(src).wait_recv()
+            else:
+
+                @pl.when(g > 0)
+                def _():
+                    arrived(src).wait_recv()
+
+            rows_up(src, quarter).start()
+            scaled_down(src, quarter).start()
+            across(src, quarter).start()
+
+    def forward_beside(g):
+        for j in range(4):
+            src = source(g, j)
+            rows_up(src, beside).wait_recv()
+            scaled_down(src, beside).wait_recv()
+            across_beside(src, beside).start()
+
+    def halves_across(g):
+        return remote(
+            part.at[g, 1 - core], part_in.at[g], d_send.at[g], d_recv.at[g], partner
+        )
+
+    def compute(g):
+        block = (z + 4 - g) % 4
+        for j in range(4):
+            src = source(g, j)
+            across(src, partner_q).wait_recv()
+            across_beside(src, partner_beside).wait_recv()
+        here = pl.ds(4 * block, 4)
+        n = 4 * cap
+        gate_pre = up_pre = d_hidden = jnp.zeros((n, wg.shape[1]), F32)
+        for q in range(4):
+            r = rows[q, here, 0].reshape(n, share)
+            sc = rows[q, here, 1].reshape(n, share)
+            f = slice(q * share, (q + 1) * share)
+            gate_pre = gate_pre + nn(r, wg[f, :])
+            up_pre = up_pre + nn(r, wu[f, :])
+            d_hidden = d_hidden + nt(sc, wd[:, f])
+        sigma = jax.nn.sigmoid(gate_pre)
+        silu = gate_pre * sigma
+        dg = (d_hidden * up_pre * sigma * (1.0 + gate_pre * (1.0 - sigma))).astype(BF16)
+        du = (d_hidden * silu).astype(BF16)
+        act[block] = (silu * up_pre).astype(BF16)
+        dgate[block] = dg
+        dup[block] = du
+        for k in range(8):
+            f = slice(k * own, (k + 1) * own)
+            part[g, k % 2, k // 2] = (nt(dg, wg[f, :]) + nt(du, wu[f, :])).astype(BF16)
+        halves_across(g).start()
+
+    def both(g, f):
+        return part[g, core, f].astype(F32) + part_in[g, f].astype(F32)
+
+    half = 2 * cap
+
+    def first_step(g, way):
+        return remote(
+            q1.at[g, way], y1.at[g, way], s1_send.at[g, way], s1_recv.at[g, way], (up, down)[way]
+        )
+
+    def second_step(g, way):
+        return remote(
+            q2.at[g, way], y2.at[g, way], s2_send.at[g, way], s2_recv.at[g, way], (up, down)[way]
+        )
+
+    def sum_far(g):
+        halves_across(g).wait_recv()
+        far = both(g, (y + 2) % 4)
+        q1[g, 0] = far[:half].astype(BF16)
+        q1[g, 1] = far[half:].astype(BF16)
+        first_step(g, 0).start()
+        first_step(g, 1).start()
+
+    def sum_near(g):
+        first_step(g, 0).wait_recv()
+        above = both(g, (y + 1) % 4)
+        q2[g, 0, :half] = (above[:half] + y1[g, 0].astype(F32)).astype(BF16)
+        q2[g, 0, half:] = above[half:].astype(BF16)
+        second_step(g, 0).start()
+        first_step(g, 1).wait_recv()
+        below = both(g, (y + 3) % 4)
+        q2[g, 1, :half] = below[:half].astype(BF16)
+        q2[g, 1, half:] = (below[half:] + y1[g, 1].astype(F32)).astype(BF16)
+        second_step(g, 1).start()
+
+    def to_owner(g, src):
+        return remote(
+            fin.at[src], ret.at[s], c_send.at[src], c_recv.at[s], (src // 4, src % 4, t)
+        )
+
+    def from_expert(e):
+        return remote(fin.at[e], ret.at[e], c_send.at[e], c_recv.at[e], up)
+
+    def sum_own(g):
+        second_step(g, 0).wait_recv()
+        second_step(g, 1).wait_recv()
+        block = (z + 4 - g) % 4
+        total = both(g, y) + y2[g, 0].astype(F32) + y2[g, 1].astype(F32)
+        fin[pl.ds(4 * block, 4)] = total.astype(BF16).reshape(4, cap, own)
+        for j in range(4):
+            src = source(g, j)
+            if j > 0:
+                to_owner(g, src).start()
+            else:
+
+                @pl.when(g > 0)
+                def _():
+                    to_owner(g, src).start()
+
+                @pl.when(g == 0)
+                def _():
+                    ret[s] = fin[s]
+
+    def grad_rows(target, which):
+        for q in range(4):
+            r = rows[q, :, 0].reshape(experts * cap, share)
+            target[q * share : (q + 1) * share, :] = tn(
+                r, which[...].reshape(experts * cap, -1)
+            ).astype(BF16)
+
+    def grad_down():
+        hidden = act[...].reshape(experts * cap, -1)
+        for q in range(4):
+            sc = rows[q, :, 1].reshape(experts * cap, share)
+            gd[:, q * share : (q + 1) * share] = tn(hidden, sc).astype(BF16)
+
+    stores = [
+        pltpu.make_async_copy(gg, gg_hbm, local.at[6]),
+        pltpu.make_async_copy(gu, gu_hbm, local.at[7]),
+        pltpu.make_async_copy(gd, gd_hbm, local.at[8]),
+    ]
+
+    def turn(n, carry):
+        for lag, task in enumerate(
+            (forward_own, forward_beside, compute, sum_far, sum_near, sum_own)
+        ):
+
+            @pl.when((n >= lag) & (n < lag + 4))
+            def _():
+                task(n - lag)
+
+        @pl.when(n == 5)
+        def _():
+            grad_rows(gg, dgate)
+            stores[0].start()
+
+        @pl.when(n == 6)
+        def _():
+            grad_rows(gu, dup)
+            stores[1].start()
+
+        @pl.when(n == 7)
+        def _():
+            grad_down()
+            stores[2].start()
+
+        return carry
+
+    lax.fori_loop(0, 9, turn, 0)
+
+    def take(k, carry):
+        from_expert((s + k) % experts).wait_recv()
+        return carry
+
+    lax.fori_loop(1, experts, take, 0)
+    places = experts * cap
+    picked = tn(hot[...].reshape(places, tokens), ret[...].reshape(places, own))
+    gm[t] = (cot_own[...].astype(F32) + picked).astype(BF16)
+
+    low, high = pl.ds(0, tokens // 2), pl.ds(tokens // 2, tokens // 2)
+    below, above, far = (t + 6) % 8, (t + 2) % 8, (t + 4) % 8
+    mate = t + 1 - 2 * core
+    m_below, m_above, m_far = (mate + 6) % 8, (mate + 2) % 8, (mate + 4) % 8
+
+    def gather(k, src, device, part_rows=None):
+        ref = gm.at[src] if part_rows is None else gm.at[src, part_rows]
+        return remote(ref, ref, g_send.at[k], g_recv.at[k], device)
+
+    gather(1, t, up).start()
+    gather(2, t, down).start()
+    gather(0, t, partner).start()
+    gather(1, below, up).wait_recv()
+    gather(3, below, up, low).start()
+    gather(5, below, partner).start()
+    gather(2, above, down).wait_recv()
+    gather(4, above, down, high).start()
+    gather(6, above, partner).start()
+    gather(3, far, up, low).wait_recv()
+    gather(4, far, down, high).wait_recv()
+    gather(7, far, partner).start()
+    gather(0, mate, partner).wait_recv()
+    gather(5, m_below, partner).wait_recv()
+    gather(6, m_above, partner).wait_recv()
+    gather(7, m_far, partner).wait_recv()
+
+    def sent(k, carry):
+        e = (s + k) % experts
+        to_expert(e).wait_send()
+        to_owner(0, e).wait_send()
+        return carry
+
+    lax.fori_loop(1, experts, sent, 0)
+
+    def forwarded(k, carry):
+        rows_up(k, quarter).wait_send()
+        scaled_down(k, quarter).wait_send()
+        across(k, quarter).wait_send()
+        across_beside(k, beside).wait_send()
+        return carry
+
+    lax.fori_loop(0, experts, forwarded, 0)
+
+    def summed(g, carry):
+        halves_across(g).wait_send()
+        for way in range(2):
+            first_step(g, way).wait_send()
+            second_step(g, way).wait_send()
+        return carry
+
+    lax.fori_loop(0, 4, summed, 0)
+    gather(0, t, partner).wait_send()
+    gather(1, t, up).wait_send()
+    gather(2, t, down).wait_send()
+    gather(3, below, up, low).wait_send()
+    gather(4, above, down, high).wait_send()
+    gather(5, below, partner).wait_send()
+    gather(6, above, partner).wait_send()
+    gather(7, far, partner).wait_send()
+    for store in stores:
+        store.wait()
+
+
+def moe(ids, wts, ld, x, b, c, mixed, cot, wg, wu, wd, experts, cap, heads):
+    tokens, width = mixed.shape
+    hidden = wg.shape[1]
+    share, own = width // 4, width // 8
+    vmem = pl.BlockSpec(memory_space=pltpu.VMEM)
+    hbm = pl.BlockSpec(memory_space=pl.ANY)
+    dma = pltpu.SemaphoreType.DMA
+
+    def kernel(*refs):
+        moe_kernel(heads, *refs)
+
+    def buf(*shape, dtype=BF16):
+        return pltpu.VMEM(shape, dtype)
+
+    n = 4 * cap
+    return pl.pallas_call(
+        kernel,
+        out_shape=[
+            jax.ShapeDtypeStruct((8, tokens, own), BF16),
+            jax.ShapeDtypeStruct(x.shape, F32),
+            jax.ShapeDtypeStruct((x.shape[1], STATE), F32),
+            jax.ShapeDtypeStruct(wg.shape, BF16),
+            jax.ShapeDtypeStruct(wu.shape, BF16),
+            jax.ShapeDtypeStruct(wd.shape, BF16),
+        ],
+        in_specs=[vmem] * 6 + [hbm] * 5,
+        out_specs=[vmem] * 3 + [hbm] * 3,
+        scratch_shapes=[
+            buf(tokens, share),
+            buf(tokens, share),
+            buf(tokens, own),
+            buf(*wg.shape),
+            buf(*wu.shape),
+            buf(*wd.shape),
+            buf(experts, tokens, dtype=jnp.int32),
+            buf(experts, tokens, dtype=F32),
+            buf(experts, cap, tokens),
+            buf(experts, 2, cap, share),
+            buf(4, experts, 2, cap, share),
+            buf(4, n, hidden),
+            buf(4, n, hidden),
+            buf(4, n, hidden),
+            buf(4, 2, 4, n, own),
+            buf(4, 4, n, own),
+            buf(4, 2, n // 2, own),
+            buf(4, 2, n // 2, own),
+            buf(4, 2, n, own),
+            buf(4, 2, n, own),
+            buf(experts, cap, own),
+            buf(experts, cap, own),
+            buf(*wg.shape),
+            buf(*wu.shape),
+            buf(*wd.shape),
+            dma((9,)),
+        ]
+        + [dma((experts,))] * 10
+        + [dma((4,))] * 2
+        + [dma((4, 2))] * 4
+        + [dma((experts,))] * 2
+        + [dma((8,))] * 2,
+        compiler_params=pltpu.CompilerParams(
+            collective_id=0, has_side_effects=True, vmem_limit_bytes=60 * 2**20
+        ),
+        name="moe",
+    )(ids, wts, ld, x, b, c, mixed, cot, wg, wu, wd)
 
 
 def call(kernel, outs, *args, name):
@@ -223,23 +687,6 @@
     return (earlier[0] + later[0], later[1] + jnp.exp(later[0])[..., None, None] * earlier[1])
 
 
-def expert_backward(rows, scaled, gate_weight, up_weight, down_weight):
-    gate_pre = nn(rows, gate_weight)
-    up_pre = nn(rows, up_weight)
-    sigma = jax.nn.sigmoid(gate_pre)
-    hidden = (gate_pre * sigma * up_pre).astype(BF16)
-    d_hidden = nt(scaled, down_weight)
-    d_gate = (d_hidden * up_pre * sigma * (1.0 + gate_pre * (1.0 - sigma))).astype(BF16)
-    d_up = (d_hidden * (gate_pre * sigma)).astype(BF16)
-    portion = nt(d_gate, gate_weight) + nt(d_up, up_weight)
-    return (
-        tn(rows, d_gate).astype(BF16),
-        tn(rows, d_up).astype(BF16),
-        tn(hidden, scaled).astype(BF16),
-        portion.astype(BF16),
-    )
-
-
 def body(
     token_values,
     write_keys,
@@ -258,57 +705,25 @@
     tokens, width = mixed.shape
     experts = lax.axis_size(SP)
     cap = 3 * tokens // experts
-    places = experts * cap
     heads = log_decay.shape[0]
     channels = token_values.shape[1]
-    share = width // lax.axis_size("tp")
-    offset = lax.axis_index("tp") * share
-    mixed_part = lax.dynamic_slice_in_dim(mixed, offset, share, 1)
-    cot_part = lax.dynamic_slice_in_dim(cotangent, offset, share, 1)
-
-    def prep(*refs):
-        prep_kernel(experts, cap, heads, *refs)
-
-    send, hot, y_inner, local_end = call(
-        prep,
-        [
-            ((experts, 2 * cap, share), BF16),
-            ((places, tokens), BF16),
-            ((tokens, channels), F32),
-            ((channels, STATE), F32),
-        ],
+    gm, y_inner, local_end, *grads = moe(
         route_ids.T,
         route_weights.T,
-        mixed_part,
-        cot_part,
         log_decay,
         token_values,
         write_keys,
         read_keys,
-        name="prep",
-    )
-    got = lax.all_to_all(send, SP, split_axis=0, concat_axis=0, tiled=True)
-    rows = lax.all_gather(got, "tp", axis=2, tiled=True)
-    grads = expert_backward(
-        rows[:, :cap].reshape(places, width),
-        rows[:, cap:].reshape(places, width),
+        mixed,
+        cotangent,
         w_gate[0],
         w_up[0],
         w_down[0],
-    )
-    summed = lax.psum_scatter(
-        grads[3].reshape(experts, cap, width), "tp", scatter_dimension=2, tiled=True
-    )
-    came = lax.all_to_all(summed, SP, split_axis=0, concat_axis=0, tiled=True)
-    (grad_part,) = call(
-        combine_kernel,
-        [((tokens, share), BF16)],
-        hot,
-        came.reshape(places, share),
-        cot_part,
-        name="combine",
-    )
-    grad_mixed = lax.all_gather(grad_part, "tp", axis=1, tiled=True)
+        experts,
+        cap,
+        heads,
+    )
+    grad_mixed = jnp.moveaxis(gm, 0, 1).reshape(tokens, width)
     out_grad = nn(grad_mixed, out_proj)
 
     total = jnp.sum(log_decay, axis=1)

time: 324 us -> 233 us (0.72)
  waiting for transfers between devices: 108 us -> 0.01 us
  Pallas kernels: 7.02 us -> 111 us
  blocking collectives: 127 us -> 90.7 us
  matrix products: 36.3 us -> 4.51 us
  between operations: 14.9 us -> 1.56 us
  local copies, waits for them, and re-layouts: 21.5 us -> 14 us
    pallas_call x0 -> x1, Pallas kernels: none -> 108 us  [moe(): pl.pallas_call(kernel, out_shape=[jax.ShapeDtypeStruct((8, tokens, own),...]
    all_gather x2 -> x0, waiting for transfers between devices: 65 us -> none  [the longest x1 65 us: body(): rows = lax.all_gather(got, 'tp', axis=2, tiled=True)]
    all_to_all x2 -> x0, blocking collectives: 51.4 us -> none  [the longest x1 30.7 us: body(): got = lax.all_to_all(send, SP, split_axis=0, concat_axis=0, tiled=True)]
    reduce_scatter x1 -> x0, waiting for transfers between devices: 43 us -> none  [body(): lax.psum_scatter(grads[3].reshape(experts, cap, width), 'tp', scatter_dim...]
    dot_general x4 -> x1, matrix products: 20.3 us -> 2.03 us  [tn(): lax.dot_general(a, b, (((0,), (0,)), ((), ())), preferred_element_type=F32)]
    all_gather x6, blocking collectives: 67.3 us -> 80.2 us  [prefix_by_axis(): lax.all_gather(part.astype(kind), axis)]
    dot_general x3 -> x0, matrix products: 9.92 us -> none  [nt(): lax.dot_general(a, b, (((1,), (1,)), ((), ())), preferred_element_type=F32)]
    slice x1 -> x0, local copies, waits for them, and re-layouts: 5.59 us -> none  [body(): rows[:, cap:].reshape(places, width)]
  transfers between devices with their start and end apart: 4 -> 1, of which waited for: 2 -> 0; matrix products, arithmetic and copies ran while one was open for 8% -> 1% of each run, Pallas kernels for 1% -> 1%
where the time goes in v2:
time: 233 us; the launch traced here: 231 us
  Pallas kernels  111 us (48%)
  blocking collectives  90.7 us (39%)
  local copies, waits for them, and re-layouts  14 us (6%)
  other arithmetic  5.07 us (2%)
  matrix products  4.51 us (2%)
  starting transfers between devices  4.44 us (2%)
    pallas_call x1, Pallas kernels, moe(): pl.pallas_call(kernel, out_shape=[jax.ShapeDtypeStruct((8, tokens, own),...  108 us
    all_gather x6, blocking collectives, prefix_by_axis(): lax.all_gather(part.astype(kind), axis)  80.2 us
    unnamed x1, blocking collectives  10.6 us
    unnamed x30, local copies, waits for them, and re-layouts  7.55 us
  transfers between devices with their start and end apart: 1, of which 0 were waited for; matrix products, arithmetic and copies ran while one was open for 1% of the time, Pallas kernels for 1%

profile of v2, /device:TPU:0, one launch (start us, length us, event | category | flops | bytes accessed | tf_op | source)
XLA Modules:
  0.0 231.4 jit_solution(14495757790088056519)
XLA Ops:
  0.7 1.0 reduce_sum.18
  1.6 1.2 dynamic-slice
  3.8 10.6 %all-reduce = bf16[16]{0:T(256)(128)(2,1)S(1)} all-reduce(bf16[16]{0:T(256)(128)(2,1)S(1)} %dynamic-update-slice), channel_id=2, replica_groups=mesh['sp_0'=4,'sp_1'=4,'tp'=8] {'sp_1'}, use_global_device_ids=true, to_apply=%add | all-reduce | flops 16 | bytes 64
  14.5 108.0 %moe.1 = (bf16[8,256,512]{2,1,0:T(8,128)(2,1)}, f32[256,256]{1,0:T(8,128)}, f32[256,128]{1,0:T(8,128)}, bf16[4096,256]{1,0:T(8,128)(2,1)}, bf16[4096,256]{1,0:T(8,128)(2,1)}, /*index=5*/bf16[256,4096]{1,0:T(8,128)(2,1)}) custom-call(s32[2,256]{1,0:T(2,128)} %bitcast.142, f32[2,256]{1,0:T(2,128)} %bitcast.143, f32[4,256]{1,0:T(4,128)} %refs_0_.3, ...), custom_call_target="tpu_custom_call" | custom-call | tf_op jit(solution)/shard_map/moe/pallas_call | solution.py:591
  122.5 3.9 %copy.22 = bf16[256,8,512]{0,2,1:T(8,128)(2,1)} copy(bf16[256,8,512]{2,0,1:T(8,128)(2,1)} %bitcast.136) | data formatting | bytes 4194304 | tf_op jit(solution)/shard_map/transpose | solution.py:726
  126.5 12.4 %all_gather.32 = bf16[4,4,64,128]{3,2,1,0:T(8,128)(2,1)S(1)} all-gather(bf16[1,4,64,128]{3,2,1,0:T(8,128)(2,1)S(1)} %bitcast.141), channel_id=1, replica_groups=mesh['sp_0'=4,'sp_1'=4,'tp'=8] {'sp_1'}, dimensions={0}, use_global_device_ids=true | all-gather | bytes 327680 | tf_op jit(solution)/shard_map/all_gather | solution.py:667
  139.1 12.3 %all_gather.33 = bf16[4,4,64,128]{3,2,1,0:T(8,128)(2,1)S(1)} all-gather(bf16[1,4,64,128]{3,2,1,0:T(8,128)(2,1)S(1)} %add_convert_fusion.1), channel_id=1, replica_groups=mesh['sp_0'=4,'sp_1'=4,'tp'=8] {'sp_0'}, dimensions={0}, use_global_device_ids=true | all-gather | bytes 327680 | tf_op jit(solution)/shard_map/all_gather | solution.py:667
  152.0 8.8 %all-gather.1 = bf16[4,1,4]{2,1,0:T(2,128)(2,1)S(1)} all-gather(bf16[1,1,4]{2,1,0:T(2,128)(2,1)S(1)} %get-tuple-element.64), channel_id=1, replica_groups=mesh['sp_0'=4,'sp_1'=4,'tp'=8] {'sp_0'}, dimensions={0}, use_global_device_ids=true | all-gather | bytes 40 | tf_op jit(solution)/shard_map/all_gather | solution.py:667
  161.7 2.5 %fusion.47.refs_5_ = f32[256,256]{1,0:T(8,128)S(1)} fusion(bf16[256,4096]{0,1:T(8,128)(2,1)} %bitcast.131, bf16[4096,256]{1,0:T(8,128)(2,1)S(1)} %copy-done), kind=kOutput, calls=%fused_computation.104 | convolution fusion | flops 536870912 | bytes 4456448 | tf_op jit(solution)/shard_map/dot_general | solution.py:18
  164.1 0.4 fusion.14.refs_4_.refs_7_
  164.6 0.9 carried.1
  165.5 2.0 convolution_convert_fusion
  167.5 4.4 %all-to-all-start = ((bf16[16,256,256]{2,1,0:T(8,128)(2,1)}), bf16[16,256,256]{2,1,0:T(8,128)(2,1)}, u32[]{:S(2)}, u32[]{:S(2)}) async-start(bf16[16,256,256]{2,1,0:T(8,128)(2,1)} %bitcast.130), calls=%async_computation | async-start | bytes 4194304 | tf_op jit(solution)/shard_map/all_to_all | solution.py:753
  172.0 21.6 %all-gather.2 = bf16[4,1,4]{2,1,0:T(2,128)(2,1)S(1)} all-gather(bf16[1,1,4]{2,1,0:T(2,128)(2,1)S(1)} %get-tuple-element.63), channel_id=1, replica_groups=mesh['sp_0'=4,'sp_1'=4,'tp'=8] {'sp_0'}, dimensions={0}, use_global_device_ids=true | all-gather | bytes 40 | tf_op jit(solution)/shard_map/all_gather | solution.py:667
  194.8 12.8 %all_gather.34 = bf16[4,4,64,128]{3,2,1,0:T(8,128)(2,1)S(1)} all-gather(bf16[1,4,64,128]{3,2,1,0:T(8,128)(2,1)S(1)} %bitcast.140), channel_id=1, replica_groups=mesh['sp_0'=4,'sp_1'=4,'tp'=8] {'sp_1'}, dimensions={0}, use_global_device_ids=true | all-gather | bytes 327680 | tf_op jit(solution)/shard_map/all_gather | solution.py:667
  207.7 12.3 %all_gather.35 = bf16[4,4,64,128]{3,2,1,0:T(8,128)(2,1)S(1)} all-gather(bf16[1,4,64,128]{3,2,1,0:T(8,128)(2,1)S(1)} %add_convert_fusion), channel_id=1, replica_groups=mesh['sp_0'=4,'sp_1'=4,'tp'=8] {'sp_0'}, dimensions={0}, use_global_device_ids=true | all-gather | bytes 327680 | tf_op jit(solution)/shard_map/all_gather | solution.py:667
  220.0 0.4 fusion.8.refs_8_
  220.4 2.2 backward.1
  222.7 2.7 %convert_reduce_fusion = f32[256,256]{1,0:T(8,128)} fusion(bf16[16,256,256]{2,1,0:T(8,128)(2,1)} %all-to-all-done), kind=kLoop, calls=%fused_computation.1 | loop fusion | flops 2031616 | bytes 2359296 | tf_op jit(solution)/shard_map/reduce_sum | solution.py:754
  225.4 1.3 copy.27
  226.7 1.0 copy-done.9
  227.8 1.3 copy.28
  229.1 1.0 copy-done.8
  230.1 1.3 copy.29
  (70 shorter events, 3.4 us)
Async XLA Ops:
  0.6 161.0 %copy-start = (bf16[4096,256]{1,0:T(8,128)(2,1)S(1)}, bf16[4096,256]{1,0:T(8,128)(2,1)}, u32[]{:S(2)}) copy-start(bf16[4096,256]{1,0:T(8,128)(2,1)} %param.18) | copy-start | bytes 6291460
  122.5 4.0 %copy-start.11 = (f32[256,128]{1,0:T(8,128)S(1)}, f32[256,128]{1,0:T(8,128)}, u32[]{:S(2)}) copy-start(f32[256,128]{1,0:T(8,128)} %get-tuple-element.23) | copy-start | bytes 393220
  161.6 2.9 %copy-start.1 = (bf16[256,128]{1,0:T(8,128)(2,1)S(1)}, bf16[256,128]{1,0:T(8,128)(2,1)}, u32[]{:S(2)}) copy-start(bf16[256,128]{1,0:T(8,128)(2,1)} %refs_3_.3) | copy-start | bytes 196612
  161.6 2.9 %copy-start.3 = (bf16[256,256]{1,0:T(8,128)(2,1)S(1)}, bf16[256,256]{1,0:T(8,128)(2,1)}, u32[]{:S(2)}) copy-start(bf16[256,256]{1,0:T(8,128)(2,1)} %refs_4_.3) | copy-start | bytes 393220
  161.6 2.9 %copy-start.5 = (f32[256,256]{1,0:T(8,128)S(1)}, f32[256,256]{1,0:T(8,128)}, u32[]{:S(2)}) copy-start(f32[256,256]{1,0:T(8,128)} %get-tuple-element.22.refs_3_) | copy-start | bytes 786436
  161.6 2.9 %copy-start.6 = (f32[4,256]{1,0:T(4,128)S(1)}, f32[4,256]{1,0:T(4,128)}, u32[]{:S(2)}) copy-start(f32[4,256]{1,0:T(4,128)} %refs_0_.3) | copy-start | bytes 12292
  161.6 3.8 %copy-start.7 = (bf16[256,8,512]{0,2,1:T(8,128)(2,1)S(1)}, bf16[256,8,512]{0,2,1:T(8,128)(2,1)}, u32[]{:S(2)}) copy-start(bf16[256,8,512]{0,2,1:T(8,128)(2,1)} %copy.22) | copy-start | bytes 6291460
  167.5 55.1 %all-to-all-start = ((bf16[16,256,256]{2,1,0:T(8,128)(2,1)}), bf16[16,256,256]{2,1,0:T(8,128)(2,1)}, u32[]{:S(2)}, u32[]{:S(2)}) async-start(bf16[16,256,256]{2,1,0:T(8,128)(2,1)} %bitcast.130), calls=%async_computation | async-start | bytes 4194304 | tf_op jit(solution)/shard_map/all_to_all | solution.py:753
  172.0 48.5 %copy-start.2 = (bf16[256,256]{1,0:T(8,128)(2,1)S(1)}, bf16[256,256]{1,0:T(8,128)(2,1)}, u32[]{:S(2)}) copy-start(bf16[256,256]{1,0:T(8,128)(2,1)} %refs_1_.3) | copy-start | bytes 393220
  172.0 48.5 %copy-start.4 = (bf16[256,128]{1,0:T(8,128)(2,1)S(1)}, bf16[256,128]{1,0:T(8,128)(2,1)}, u32[]{:S(2)}) copy-start(bf16[256,128]{1,0:T(8,128)(2,1)} %refs_2_.5) | copy-start | bytes 196612
  222.7 2.8 %copy-start.10 = (bf16[4096,256]{1,0:T(8,128)(2,1)S(1)}, bf16[4096,256]{1,0:T(8,128)(2,1)}, u32[]{:S(2)}) copy-start(bf16[4096,256]{1,0:T(8,128)(2,1)} %get-tuple-element.31) | copy-start | bytes 6291460
  225.4 2.3 %copy-start.9 = (bf16[4096,256]{1,0:T(8,128)(2,1)S(1)}, bf16[4096,256]{1,0:T(8,128)(2,1)}, u32[]{:S(2)}) copy-start(bf16[4096,256]{1,0:T(8,128)(2,1)} %get-tuple-element.32) | copy-start | bytes 6291460
  227.8 2.3 %copy-start.8 = (bf16[256,4096]{1,0:T(8,128)(2,1)S(1)}, bf16[256,4096]{1,0:T(8,128)(2,1)}, u32[]{:S(2)}) copy-start(bf16[256,4096]{1,0:T(8,128)(2,1)} %get-tuple-element.33) | copy-start | bytes 6291460

commit v3 on v2

--- a/solution.py
+++ b/solution.py
@@ -92,12 +92,11 @@
     return jnp.concatenate(ys, axis=1), end
 
 
-def mix_backward(x, b, c, gate, out_grad, y, row, col, entering, leaving, heads):
+def mix_backward(x, b, c, gate, out_grad, y, lead_grad, entering, row, col, heads):
     tokens = x.shape[0]
     sigma = jax.nn.sigmoid(gate)
-    g = out_grad * (gate * sigma)
+    gb = (out_grad * (gate * sigma)).astype(BF16)
     d_gate = out_grad * y * sigma * (1.0 + gate * (1.0 - sigma))
-    gb = g.astype(BF16)
     scores = nt(c, b)
     first = iota((tokens, 2 * HEAD_DIM), 1) < HEAD_DIM
     d_scores = jnp.zeros((tokens, tokens), F32)
@@ -112,50 +111,12 @@
             d_scores = d_scores + w * nt(jnp.where(mine, gp, jnp.zeros_like(gp)), xp)
             pair.append(tn((scores * w).astype(BF16), gp))
         dxs.append(jnp.where(first, pair[0], pair[1]))
-    tails = by_lane(jnp.exp(col[tokens - 1 : tokens, :] - col), tokens, heads)
-    leads = by_lane(jnp.exp(col), tokens, heads)
-    d_x = jnp.concatenate(dxs, axis=1) + tails * nt(b, leaving)
     ds = d_scores.astype(BF16)
-    d_c = nn(ds, b) + nn((g * leads).astype(BF16), entering)
-    d_b = tn(ds, c) + nn((x.astype(F32) * tails).astype(BF16), leaving)
-    return d_x, d_b, d_c, d_gate
-
-
-def carried_kernel(heads, ld, c, gate, y_inner, entering, out_grad, y, gated, back):
-    row, col = decays(ld[...])
-    tokens = y_inner.shape[0]
-    leads = by_lane(jnp.exp(col), tokens, heads)
-    whole = y_inner[...] + leads * nt(c[...], entering[...])
-    g = gate[...].astype(F32)
-    silu = g * jax.nn.sigmoid(g)
-    y[...] = whole
-    gated[...] = (whole * silu).astype(BF16)
-    back[...] = tn((out_grad[...] * silu * leads).astype(BF16), c[...])
-
-
-def backward_kernel(heads, ld, x, b, c, gate, og, y, entering, leaving, dx, db, dc, dg):
-    row, col = decays(ld[...])
-    d_x, d_b, d_c, d_g = mix_backward(
-        x[...],
-        b[...],
-        c[...],
-        gate[...].astype(F32),
-        og[...],
-        y[...],
-        row,
-        col,
-        entering[...],
-        leaving[...],
-        heads,
-    )
-    dx[...] = d_x.astype(BF16)
-    db[...] = d_b.astype(BF16)
-    dc[...] = d_c.astype(BF16)
-    dg[...] = d_g.astype(BF16)
+    return jnp.concatenate(dxs, axis=1), tn(ds, c), nn(ds, b) + nn(lead_grad, entering), d_gate
 
 
 MESH = pl.DeviceIdType.MESH
-GROUPS_OF = 4
+STEP = 16
 
 
 def remote(src, dst, send, recv, device):
@@ -172,17 +133,35 @@
     x_in,
     b_in,
     c_in,
+    gate_in,
     mixed,
     cot,
     wg_hbm,
     wu_hbm,
     wd_hbm,
-    gm,
-    y_out,
-    end_out,
+    op_hbm,
+    dx_out,
+    db_out,
+    dc_out,
+    dgate_out,
+    proj_out,
     gg_hbm,
     gu_hbm,
     gd_hbm,
+    gm,
+    op,
+    y_ref,
+    gated,
+    state_send,
+    state_in,
+    enter_send,
+    enter,
+    back_send,
+    back_in,
+    leave_send,
+    leave,
+    proj_send,
+    proj_in,
     mixed_q,
     cot_q,
     cot_own,
@@ -229,6 +208,16 @@
     c_recv,
     g_send,
     g_recv,
+    e_send,
+    e_recv,
+    f_send,
+    f_recv,
+    b_send,
+    b_recv,
+    l_send,
+    l_recv,
+    p_send,
+    p_recv,
 ):
     z, x, t = lax.axis_index("sp_0"), lax.axis_index("sp_1"), lax.axis_index("tp")
     s = 4 * z + x
@@ -249,6 +238,7 @@
         pltpu.make_async_copy(wg_hbm, wg, local.at[3]),
         pltpu.make_async_copy(wu_hbm, wu, local.at[4]),
         pltpu.make_async_copy(wd_hbm, wd, local.at[5]),
+        pltpu.make_async_copy(op_hbm, op, local.at[9]),
     ]
     for load in loads:
         load.start()
@@ -309,10 +299,76 @@
 
     row, col = decays(ld[...])
     inner, last = mix_local(x_in[...], b_in[...], c_in[...], row, col, heads)
-    y_out[...] = inner
-    end_out[...] = last
+    y_ref[...] = inner
+    totals = jnp.broadcast_to(row[:, tokens - 1 : tokens], (8, STATE))
+    state_send[:, :STEP, :] = last.reshape(experts, STEP, STATE)
+    state_send[:, STEP:, :] = jnp.broadcast_to(totals[None], (experts, 8, STATE))
+    state_in[s] = state_send[s]
+
+    def peer(k):
+        j = (s + k) % experts
+        return j, (j // 4, j % 4, t)
+
+    def over_sp(source_ref, target_ref, send, recv):
+        def copy(k):
+            j, device = peer(k)
+            return remote(source_ref.at[j], target_ref.at[s], send.at[j], recv.at[s], device)
+
+        def wait(k):
+            j, device = peer(k)
+            remote(source_ref.at[j], target_ref.at[j], send.at[j], recv.at[j], device).wait_recv()
+
+        def each(action):
+            def step(k, carry):
+                action(k)
+                return carry
+
+            lax.fori_loop(1, experts, step, 0)
+
+        return (
+            lambda: each(lambda k: copy(k).start()),
+            lambda: each(wait),
+            lambda: each(lambda k: copy(k).wait_send()),
+        )
+
+    states = over_sp(state_send, state_in, e_send, e_recv)
+    enters = over_sp(enter_send, enter, f_send, f_recv)
+    backs = over_sp(back_send, back_in, b_send, b_recv)
+    leaves = over_sp(leave_send, leave, l_send, l_recv)
+    states[0]()
     for load in loads[2:]:
         load.wait()
+
+    def factor(src):
+        return jnp.exp(state_in[src, pl.ds(STEP + s // 4, 1), :])
+
+    def scan_forward():
+        states[1]()
+        held = jnp.zeros((STEP, STATE), F32)
+        for src in range(experts):
+            enter_send[src] = held.astype(BF16)
+            held = factor(src) * held + state_in[src, :STEP, :]
+        enter[s] = enter_send[s]
+        enters[0]()
+
+    def scan_back():
+        backs[1]()
+        held = jnp.zeros((STEP, STATE), F32)
+        for src in reversed(range(experts)):
+            leave_send[src] = held.astype(BF16)
+            held = factor(src) * held + back_in[src].astype(F32)
+        leave[s] = leave_send[s]
+        leaves[0]()
+
+    def finish_forward():
+        enters[1]()
+        _, col = decays(ld[...])
+        leads = by_lane(jnp.exp(col), tokens, heads)
+        entering = enter[...].reshape(x_in.shape[1], STATE)
+        whole = y_ref[...] + leads * nt(c_in[...], entering)
+        g = gate_in[...].astype(F32)
+        y_ref[...] = whole
+        gated[...] = (whole * (g * jax.nn.sigmoid(g))).astype(BF16)
 
     def source(g, j):
         return 4 * ((z + 4 - g) % 4) + (x + 4 - j) % 4
@@ -482,6 +538,14 @@
             def _():
                 task(n - lag)
 
+        @pl.when(n == 2)
+        def _():
+            scan_forward()
+
+        @pl.when(n == 4)
+        def _():
+            finish_forward()
+
         @pl.when(n == 5)
         def _():
             grad_rows(gg, dgate)
@@ -519,27 +583,91 @@
         ref = gm.at[src] if part_rows is None else gm.at[src, part_rows]
         return remote(ref, ref, g_send.at[k], g_recv.at[k], device)
 
+    def to_column(i):
+        return remote(
+            proj_send.at[i], proj_in.at[s], p_send.at[i], p_recv.at[s], (i // 4, i % 4, t)
+        )
+
+    columns = gated.shape[1]
+    gated_b = gated[...]
+
+    def project(j):
+        for k in range(own // columns):
+            i = j * (own // columns) + k
+            block = gm[j, :, k * columns : (k + 1) * columns]
+            proj_send[i] = tn(block, gated_b).astype(BF16)
+
+            @pl.when(i != s)
+            def _():
+                to_column(i).start()
+
+            @pl.when(i == s)
+            def _():
+                proj_in[s] = proj_send[s]
+
+        return nn(gm[j], op[pl.ds(j * own, own), :])
+
     gather(1, t, up).start()
     gather(2, t, down).start()
     gather(0, t, partner).start()
+    out_grad = project(t)
+    gather(0, mate, partner).wait_recv()
+    out_grad = out_grad + project(mate)
     gather(1, below, up).wait_recv()
     gather(3, below, up, low).start()
     gather(5, below, partner).start()
     gather(2, above, down).wait_recv()
     gather(4, above, down, high).start()
     gather(6, above, partner).start()
+    out_grad = out_grad + project(below) + project(above)
+    gather(5, m_below, partner).wait_recv()
+    out_grad = out_grad + project(m_below)
+    gather(6, m_above, partner).wait_recv()
+    out_grad = out_grad + project(m_above)
     gather(3, far, up, low).wait_recv()
     gather(4, far, down, high).wait_recv()
     gather(7, far, partner).start()
-    gather(0, mate, partner).wait_recv()
-    gather(5, m_below, partner).wait_recv()
-    gather(6, m_above, partner).wait_recv()
+    out_grad = out_grad + project(far)
     gather(7, m_far, partner).wait_recv()
+    out_grad = out_grad + project(m_far)
+
+    row, col = decays(ld[...])
+    leads = by_lane(jnp.exp(col), tokens, heads)
+    gate = gate_in[...].astype(F32)
+    lead_grad = (out_grad * (gate * jax.nn.sigmoid(gate)) * leads).astype(BF16)
+    back_send[...] = tn(lead_grad, c_in[...]).astype(BF16).reshape(experts, STEP, STATE)
+    back_in[s] = back_send[s]
+    backs[0]()
+    backward = mix_backward(
+        x_in[...], b_in[...], c_in[...], gate, out_grad, y_ref[...], lead_grad,
+        enter[...].reshape(x_in.shape[1], STATE), row, col, heads
+    )
+    dgate_out[...] = backward[3].astype(BF16)
+    dc_out[...] = backward[2].astype(BF16)
+    scan_back()
+    tails = by_lane(jnp.exp(col[tokens - 1 : tokens, :] - col), tokens, heads)
+    tail_values = (x_in[...].astype(F32) * tails).astype(BF16)
+    leaves[1]()
+    leaving = leave[...].reshape(x_in.shape[1], STATE)
+    dx_out[...] = (backward[0] + tails * nt(b_in[...], leaving)).astype(BF16)
+    db_out[...] = (backward[1] + nn(tail_values, leaving)).astype(BF16)
+
+    def column(k, total):
+        i = (s + k) % experts
+        remote(
+            proj_send.at[i], proj_in.at[i], p_send.at[i], p_recv.at[i], up
+        ).wait_recv()
+        return total + proj_in[i].astype(F32)
+
+    proj_out[...] = lax.fori_loop(1, experts, column, proj_in[s].astype(F32))
+    for exchange in (states, enters, backs, leaves):
+        exchange[2]()
 
     def sent(k, carry):
         e = (s + k) % experts
         to_expert(e).wait_send()
         to_owner(0, e).wait_send()
+        to_column(e).wait_send()
         return carry
 
     lax.fori_loop(1, experts, sent, 0)
@@ -573,9 +701,10 @@
         store.wait()
 
 
-def moe(ids, wts, ld, x, b, c, mixed, cot, wg, wu, wd, experts, cap, heads):
+def whole(ids, wts, ld, x, b, c, gate, mixed, cot, wg, wu, wd, op, experts, cap, heads):
     tokens, width = mixed.shape
     hidden = wg.shape[1]
+    channels = x.shape[1]
     share, own = width // 4, width // 8
     vmem = pl.BlockSpec(memory_space=pltpu.VMEM)
     hbm = pl.BlockSpec(memory_space=pl.ANY)
@@ -591,16 +720,32 @@
     return pl.pallas_call(
         kernel,
         out_shape=[
-            jax.ShapeDtypeStruct((8, tokens, own), BF16),
-            jax.ShapeDtypeStruct(x.shape, F32),
-            jax.ShapeDtypeStruct((x.shape[1], STATE), F32),
+            jax.ShapeDtypeStruct(x.shape, BF16),
+            jax.ShapeDtypeStruct(b.shape, BF16),
+            jax.ShapeDtypeStruct(c.shape, BF16),
+            jax.ShapeDtypeStruct(gate.shape, BF16),
+            jax.ShapeDtypeStruct((width // experts, channels), F32),
             jax.ShapeDtypeStruct(wg.shape, BF16),
             jax.ShapeDtypeStruct(wu.shape, BF16),
             jax.ShapeDtypeStruct(wd.shape, BF16),
         ],
-        in_specs=[vmem] * 6 + [hbm] * 5,
-        out_specs=[vmem] * 3 + [hbm] * 3,
+        in_specs=[vmem] * 7 + [hbm] * 6,
+        out_specs=[vmem] * 5 + [hbm] * 3,
         scratch_shapes=[
+            buf(8, tokens, own),
+            buf(*op.shape),
+            buf(tokens, channels, dtype=F32),
+            buf(tokens, channels),
+            buf(experts, STEP + 8, STATE, dtype=F32),
+            buf(experts, STEP + 8, STATE, dtype=F32),
+            buf(experts, STEP, STATE),
+            buf(experts, STEP, STATE),
+            buf(experts, STEP, STATE),
+            buf(experts, STEP, STATE),
+            buf(experts, STEP, STATE),
+            buf(experts, STEP, STATE),
+            buf(experts, width // experts, channels),
+            buf(experts, width // experts, channels),
             buf(tokens, share),
             buf(tokens, share),
             buf(tokens, own),
@@ -626,65 +771,19 @@
             buf(*wg.shape),
             buf(*wu.shape),
             buf(*wd.shape),
-            dma((9,)),
+            dma((10,)),
         ]
         + [dma((experts,))] * 10
         + [dma((4,))] * 2
         + [dma((4, 2))] * 4
         + [dma((experts,))] * 2
-        + [dma((8,))] * 2,
+        + [dma((8,))] * 2
+        + [dma((experts,))] * 10,
         compiler_params=pltpu.CompilerParams(
             collective_id=0, has_side_effects=True, vmem_limit_bytes=60 * 2**20
         ),
-        name="moe",
-    )(ids, wts, ld, x, b, c, mixed, cot, wg, wu, wd)
-
-
-def call(kernel, outs, *args, name):
-    vmem = pl.BlockSpec(memory_space=pltpu.VMEM)
-    return pl.pallas_call(
-        kernel,
-        out_shape=[jax.ShapeDtypeStruct(s, d) for s, d in outs],
-        in_specs=[vmem] * len(args),
-        out_specs=[vmem] * len(outs),
-        compiler_params=pltpu.CompilerParams(vmem_limit_bytes=24 * 2**20),
-        name=name,
-    )(*args)
-
-
-def nothing_yet(array, identity):
-    return jax.tree.map(
-        lambda a, e: jnp.broadcast_to(jnp.asarray(e, a.dtype), a.shape), array, identity
-    )
-
-
-def prefix_by_axis(array, axes, combine, identity, reverse):
-    before = start = nothing_yet(array, identity)
-    so_far = array
-    for axis in reversed(axes):
-        length, position = (lax.axis_size(axis), lax.axis_index(axis))
-        pieces = jax.tree.map(
-            lambda part, kind: lax.all_gather(part.astype(kind), axis),
-            so_far,
-            (BF16, BF16),
-        )
-        inside, so_far = (start, start)
-        for k in reversed(range(length)) if reverse else range(length):
-            passed = k > position if reverse else k < position
-            so_far = combine(
-                so_far, jax.tree.map(lambda part, own: part[k].astype(own.dtype), pieces, array)
-            )
-            inside = jax.tree.map(lambda new, old: jnp.where(passed, new, old), so_far, inside)
-        before = combine(inside, before)
-    return before
-
-
-def forward_join(earlier, later):
-    return (earlier[0] + later[0], jnp.exp(later[0])[..., None, None] * earlier[1] + later[1])
-
-
-def backward_join(earlier, later):
-    return (earlier[0] + later[0], later[1] + jnp.exp(later[0])[..., None, None] * earlier[1])
+        name="whole",
+    )(ids, wts, ld, x, b, c, gate, mixed, cot, wg, wu, wd, op)
 
 
 def body(
@@ -702,88 +801,26 @@
     w_up,
     w_down,
 ):
-    tokens, width = mixed.shape
     experts = lax.axis_size(SP)
-    cap = 3 * tokens // experts
-    heads = log_decay.shape[0]
-    channels = token_values.shape[1]
-    gm, y_inner, local_end, *grads = moe(
+    outs = whole(
         route_ids.T,
         route_weights.T,
         log_decay,
         token_values,
         write_keys,
         read_keys,
+        out_gate,
         mixed,
         cotangent,
         w_gate[0],
         w_up[0],
         w_down[0],
+        out_proj,
         experts,
-        cap,
-        heads,
+        3 * mixed.shape[0] // experts,
+        log_decay.shape[0],
     )
-    grad_mixed = jnp.moveaxis(gm, 0, 1).reshape(tokens, width)
-    out_grad = nn(grad_mixed, out_proj)
-
-    total = jnp.sum(log_decay, axis=1)
-    zero_total = jnp.zeros_like(total)
-    zero_state = jnp.zeros((heads, HEAD_DIM, STATE), F32)
-    shape = (heads, HEAD_DIM, STATE)
-    entering = prefix_by_axis(
-        (total, local_end.reshape(shape)), SP, forward_join, (zero_total, zero_state), False
-    )[1]
-    entering = entering.reshape(channels, STATE).astype(BF16)
-
-    def carried(*refs):
-        carried_kernel(heads, *refs)
-
-    y, gated, local_back = call(
-        carried,
-        [((tokens, channels), F32), ((tokens, channels), BF16), ((channels, STATE), F32)],
-        log_decay,
-        read_keys,
-        out_gate,
-        y_inner,
-        entering,
-        out_grad,
-        name="carried",
-    )
-    proj_part = tn(grad_mixed, gated).astype(BF16).reshape(experts, -1, channels)
-    proj_came = lax.all_to_all(proj_part, SP, split_axis=0, concat_axis=0, tiled=True)
-    proj_grad = proj_came.astype(F32).sum(axis=0)
-    leaving = prefix_by_axis(
-        (total, local_back.reshape(shape)), SP, backward_join, (zero_total, zero_state), True
-    )[1]
-    leaving = leaving.reshape(channels, STATE).astype(BF16)
-
-    def backward(*refs):
-        backward_kernel(heads, *refs)
-
-    d_values, d_writes, d_reads, d_gate = call(
-        backward,
-        [(a.shape, BF16) for a in (token_values, write_keys, read_keys, out_gate)],
-        log_decay,
-        token_values,
-        write_keys,
-        read_keys,
-        out_gate,
-        out_grad,
-        y,
-        entering,
-        leaving,
-        name="backward",
-    )
-    return (
-        d_values,
-        d_writes,
-        d_reads,
-        d_gate,
-        proj_grad,
-        grads[0][None],
-        grads[1][None],
-        grads[2][None],
-    )
+    return (*outs[:5], *(g[None] for g in outs[5:]))
 
 
 def solution(mesh):

time: 233 us -> 176 us (0.76)
  blocking collectives: 90.7 us -> 0 us
  Pallas kernels: 111 us -> 161 us
  other arithmetic: 5.07 us -> 0 us
  matrix products: 4.51 us -> 0 us
  starting transfers between devices: 4.44 us -> 0 us
    all_gather x6 -> x0, blocking collectives: 80.2 us -> none  [prefix_by_axis(): lax.all_gather(part.astype(kind), axis)]
    pallas_call x3 -> x1, Pallas kernels: 111 us -> 161 us  [whole(): pl.pallas_call(kernel, out_shape=[jax.ShapeDtypeStruct(x.shape, BF16), ja...]
    unnamed x1 -> x0, blocking collectives: 10.6 us -> none
    unnamed x30 -> x12, local copies, waits for them, and re-layouts: 7.55 us -> 14.6 us
    dot_general x2 -> x0, matrix products: 4.51 us -> none  [the longest x1 2.48 us: nn(): lax.dot_general(a, b, (((1,), (0,)), ((), ())), preferred_element_type=F32)]
    all_to_all x1 -> x0, starting transfers between devices: 4.44 us -> none  [body(): lax.all_to_all(proj_part, SP, split_axis=0, concat_axis=0, tiled=True)]
    transpose x1 -> x0, local copies, waits for them, and re-layouts: 3.95 us -> none  [body(): grad_mixed = jnp.moveaxis(gm, 0, 1).reshape(tokens, width)]
    reduce_sum x2 -> x0, other arithmetic: 3.7 us -> none  [the longest x1 2.75 us: body(): proj_grad = proj_came.astype(F32).sum(axis=0)]
  transfers between devices with their start and end apart: 1 -> 0, of which waited for: 0 -> 0; matrix products, arithmetic and copies ran while one was open for 1% -> 0% of each run, Pallas kernels for 1% -> 0%
where the time goes in v3:
time: 176 us
  Pallas kernels  161 us (91%)
  local copies, waits for them, and re-layouts  14.6 us (8%)
    pallas_call x1, Pallas kernels, whole(): pl.pallas_call(kernel, out_shape=[jax.ShapeDtypeStruct(x.shape, BF16), ja...  161 us
    unnamed x12, local copies, waits for them, and re-layouts  14.6 us

profile of v3, /device:TPU:0, one launch (start us, length us, event | category | flops | bytes accessed | tf_op | source)
XLA Modules:
  0.0 175.8 jit_solution(17495981634901801721)
XLA Ops:
  0.6 160.6 %whole.1 = (bf16[256,256]{1,0:T(8,128)(2,1)}, bf16[256,128]{1,0:T(8,128)(2,1)}, bf16[256,128]{1,0:T(8,128)(2,1)}, bf16[256,256]{1,0:T(8,128)(2,1)}, f32[256,256]...) custom-call(s32[2,256]{1,0:T(2,128)} %bitcast.14, ...), custom_call_target="tpu_custom_call" | custom-call | tf_op jit(solution)/shard_map/whole/pallas_call | solution.py:720
  161.2 1.6 copy.29
  162.8 1.5 copy.30
  164.3 1.5 copy.31
  165.7 1.6 copy.32
  167.3 1.7 copy.33
  169.0 0.0 copy-start.1
  169.0 3.2 %copy.34 = bf16[1,4096,256]{2,1,0:T(8,128)(2,1)} copy(bf16[1,4096,256]{2,1,0:T(8,128)(2,1)} %bitcast.10) | data formatting | bytes 4194304
  172.2 0.0 copy-done.1
  172.2 0.0 copy-start
  172.2 1.3 copy.35
  173.5 1.0 copy-done
  174.5 1.3 copy.36
Async XLA Ops:
  169.0 3.2 %copy-start.1 = (bf16[4096,256]{1,0:T(8,128)(2,1)S(1)}, bf16[4096,256]{1,0:T(8,128)(2,1)}, u32[]{:S(2)}) copy-start(bf16[4096,256]{1,0:T(8,128)(2,1)} %get-tuple-element.22) | copy-start | bytes 6291460
  172.2 2.3 %copy-start = (bf16[256,4096]{1,0:T(8,128)(2,1)S(1)}, bf16[256,4096]{1,0:T(8,128)(2,1)}, u32[]{:S(2)}) copy-start(bf16[256,4096]{1,0:T(8,128)(2,1)} %get-tuple-element.23) | copy-start | bytes 6291460

commit v4 on v3

--- a/solution.py
+++ b/solution.py
@@ -245,9 +245,12 @@
 
     barrier = pltpu.get_barrier_semaphore()
 
+    def peer(k):
+        to_z, to_x = (z + k % 4) % 4, (x + k % 4 + k // 4) % 4
+        return 4 * to_z + to_x, (to_z, to_x, t)
+
     def greet(k, carry):
-        j = (s + k) % experts
-        pl.semaphore_signal(barrier, inc=1, device_id=(j // 4, j % 4, t), device_id_type=MESH)
+        pl.semaphore_signal(barrier, inc=1, device_id=peer(k)[1], device_id_type=MESH)
         return carry
 
     lax.fori_loop(1, experts, greet, 0)
@@ -266,11 +269,10 @@
         )
 
     def build(g, carry):
-        block = (z + g) % 4
         place = iota((cap, tokens), 0)
         ones, ws = [], []
-        for k in range(4):
-            e = 4 * block + k
+        for j in range(4):
+            e = peer(4 * g + j)[0]
             mine = place == slot_ref[pl.ds(e, 1), :]
             one = mine.astype(BF16)
             hot[e] = one
@@ -279,11 +281,14 @@
             ws.append(jnp.sum(w, axis=1, keepdims=True))
         one = jnp.concatenate(ones, axis=0)
         w = jnp.concatenate(ws, axis=0)
-        here = pl.ds(4 * block, 4)
-        sendbuf[here, 0] = nn(one, mixed_q[...]).astype(BF16).reshape(4, cap, share)
-        sendbuf[here, 1] = (nn(one, cot_q[...]) * w).astype(BF16).reshape(4, cap, share)
+        plain = nn(one, mixed_q[...]).astype(BF16)
+        scaled = (nn(one, cot_q[...]) * w).astype(BF16)
         for j in range(4):
-            e = 4 * block + (x + j) % 4
+            e = peer(4 * g + j)[0]
+            sendbuf[e, 0] = plain[j * cap : (j + 1) * cap]
+            sendbuf[e, 1] = scaled[j * cap : (j + 1) * cap]
+        for j in range(4):
+            e = peer(4 * g + j)[0]
             if j > 0:
                 to_expert(e).start()
             else:
@@ -304,10 +309,6 @@
     state_send[:, :STEP, :] = last.reshape(experts, STEP, STATE)
     state_send[:, STEP:, :] = jnp.broadcast_to(totals[None], (experts, 8, STATE))
     state_in[s] = state_send[s]
-
-    def peer(k):
-        j = (s + k) % experts
-        return j, (j // 4, j % 4, t)
 
     def over_sp(source_ref, target_ref, send, recv):
         def copy(k):
@@ -371,7 +372,7 @@
         gated[...] = (whole * (g * jax.nn.sigmoid(g))).astype(BF16)
 
     def source(g, j):
-        return 4 * ((z + 4 - g) % 4) + (x + 4 - j) % 4
+        return 4 * ((z + 4 - j) % 4) + (x + 8 - j - g) % 4
 
     def arrived(src):
         return remote(sendbuf.at[src], rows.at[quarter, src], a_send.at[src], a_recv.at[src], up)
@@ -420,17 +421,15 @@
         )
 
     def compute(g):
-        block = (z + 4 - g) % 4
-        for j in range(4):
-            src = source(g, j)
+        sources = [source(g, j) for j in range(4)]
+        for src in sources:
             across(src, partner_q).wait_recv()
             across_beside(src, partner_beside).wait_recv()
-        here = pl.ds(4 * block, 4)
         n = 4 * cap
         gate_pre = up_pre = d_hidden = jnp.zeros((n, wg.shape[1]), F32)
         for q in range(4):
-            r = rows[q, here, 0].reshape(n, share)
-            sc = rows[q, here, 1].reshape(n, share)
+            r = jnp.concatenate([rows[q, src, 0] for src in sources], axis=0)
+            sc = jnp.concatenate([rows[q, src, 1] for src in sources], axis=0)
             f = slice(q * share, (q + 1) * share)
             gate_pre = gate_pre + nn(r, wg[f, :])
             up_pre = up_pre + nn(r, wu[f, :])
@@ -439,9 +438,12 @@
         silu = gate_pre * sigma
         dg = (d_hidden * up_pre * sigma * (1.0 + gate_pre * (1.0 - sigma))).astype(BF16)
         du = (d_hidden * silu).astype(BF16)
-        act[block] = (silu * up_pre).astype(BF16)
-        dgate[block] = dg
-        dup[block] = du
+        hidden = (silu * up_pre).astype(BF16)
+        for j, src in enumerate(sources):
+            part_rows = slice(j * cap, (j + 1) * cap)
+            act[src] = hidden[part_rows]
+            dgate[src] = dg[part_rows]
+            dup[src] = du[part_rows]
         for k in range(8):
             f = slice(k * own, (k + 1) * own)
             part[g, k % 2, k // 2] = (nt(dg, wg[f, :]) + nt(du, wu[f, :])).astype(BF16)
@@ -493,9 +495,9 @@
     def sum_own(g):
         second_step(g, 0).wait_recv()
         second_step(g, 1).wait_recv()
-        block = (z + 4 - g) % 4
-        total = both(g, y) + y2[g, 0].astype(F32) + y2[g, 1].astype(F32)
-        fin[pl.ds(4 * block, 4)] = total.astype(BF16).reshape(4, cap, own)
+        total = (both(g, y) + y2[g, 0].astype(F32) + y2[g, 1].astype(F32)).astype(BF16)
+        for j in range(4):
+            fin[source(g, j)] = total[j * cap : (j + 1) * cap]
         for j in range(4):
             src = source(g, j)
             if j > 0:
@@ -538,11 +540,11 @@
             def _():
                 task(n - lag)
 
-        @pl.when(n == 2)
+        @pl.when(n == 4)
         def _():
             scan_forward()
 
-        @pl.when(n == 4)
+        @pl.when(n == 7)
         def _():
             finish_forward()
 
@@ -566,7 +568,7 @@
     lax.fori_loop(0, 9, turn, 0)
 
     def take(k, carry):
-        from_expert((s + k) % experts).wait_recv()
+        from_expert(peer(k)[0]).wait_recv()
         return carry
 
     lax.fori_loop(1, experts, take, 0)
@@ -591,15 +593,17 @@
     columns = gated.shape[1]
     gated_b = gated[...]
 
-    def project(j):
+    def project(j, send=False):
         for k in range(own // columns):
             i = j * (own // columns) + k
             block = gm[j, :, k * columns : (k + 1) * columns]
             proj_send[i] = tn(block, gated_b).astype(BF16)
 
-            @pl.when(i != s)
-            def _():
-                to_column(i).start()
+            if send:
+
+                @pl.when(i != s)
+                def _():
+                    to_column(i).start()
 
             @pl.when(i == s)
             def _():
@@ -610,9 +614,9 @@
     gather(1, t, up).start()
     gather(2, t, down).start()
     gather(0, t, partner).start()
-    out_grad = project(t)
+    out_grad = project(t, True)
     gather(0, mate, partner).wait_recv()
-    out_grad = out_grad + project(mate)
+    out_grad = out_grad + project(mate, True)
     gather(1, below, up).wait_recv()
     gather(3, below, up, low).start()
     gather(5, below, partner).start()
@@ -631,6 +635,16 @@
     gather(7, m_far, partner).wait_recv()
     out_grad = out_grad + project(m_far)
 
+    def send_column(k, carry):
+        i, device = peer(k)
+
+        @pl.when(device[0] != y)
+        def _():
+            to_column(i).start()
+
+        return carry
+
+    lax.fori_loop(1, experts, send_column, 0)
     row, col = decays(ld[...])
     leads = by_lane(jnp.exp(col), tokens, heads)
     gate = gate_in[...].astype(F32)
@@ -653,7 +667,7 @@
     db_out[...] = (backward[1] + nn(tail_values, leaving)).astype(BF16)
 
     def column(k, total):
-        i = (s + k) % experts
+        i = peer(k)[0]
         remote(
             proj_send.at[i], proj_in.at[i], p_send.at[i], p_recv.at[i], up
         ).wait_recv()
@@ -664,7 +678,7 @@
         exchange[2]()
 
     def sent(k, carry):
-        e = (s + k) % experts
+        e = peer(k)[0]
         to_expert(e).wait_send()
         to_owner(0, e).wait_send()
         to_column(e).wait_send()
@@ -757,9 +771,9 @@
             buf(experts, cap, tokens),
             buf(experts, 2, cap, share),
             buf(4, experts, 2, cap, share),
-            buf(4, n, hidden),
-            buf(4, n, hidden),
-            buf(4, n, hidden),
+            buf(experts, cap, hidden),
+            buf(experts, cap, hidden),
+            buf(experts, cap, hidden),
             buf(4, 2, 4, n, own),
             buf(4, 4, n, own),
             buf(4, 2, n // 2, own),
@@ -786,6 +800,44 @@
     )(ids, wts, ld, x, b, c, gate, mixed, cot, wg, wu, wd, op)
 
 
+def hand_out(arrays):
+    pieces = []
+    for k, a in enumerate(arrays):
+        count = max(1, a.size * a.dtype.itemsize // 2**19)
+        step = a.shape[0] // count
+        pieces += [(k, pl.ds(m * step, step)) for m in range(count)]
+
+    def kernel(*refs):
+        n = len(arrays)
+        ins, outs, held, (come, go) = refs[:n], refs[n : 2 * n], refs[2 * n : 3 * n], refs[3 * n :]
+        fetch = [
+            pltpu.make_async_copy(ins[k].at[at], held[k].at[at], come.at[m])
+            for m, (k, at) in enumerate(pieces)
+        ]
+        store = [
+            pltpu.make_async_copy(held[k].at[at], outs[k].at[at], go.at[m])
+            for m, (k, at) in enumerate(pieces)
+        ]
+        for f in fetch:
+            f.start()
+        for f, g in zip(fetch, store):
+            f.wait()
+            g.start()
+        for g in store:
+            g.wait()
+
+    hbm = pl.BlockSpec(memory_space=pl.ANY)
+    return pl.pallas_call(
+        kernel,
+        out_shape=[jax.ShapeDtypeStruct(a.shape, a.dtype) for a in arrays],
+        in_specs=[hbm] * len(arrays),
+        out_specs=[hbm] * len(arrays),
+        scratch_shapes=[pltpu.VMEM(a.shape, a.dtype) for a in arrays]
+        + [pltpu.SemaphoreType.DMA((len(pieces),))] * 2,
+        name="hand_out",
+    )(*arrays)
+
+
 def body(
     token_values,
     write_keys,
@@ -802,7 +854,7 @@
     w_down,
 ):
     experts = lax.axis_size(SP)
-    outs = whole(
+    outs = hand_out(whole(
         route_ids.T,
         route_weights.T,
         log_decay,
@@ -819,7 +871,7 @@
         experts,
         3 * mixed.shape[0] // experts,
         log_decay.shape[0],
-    )
+    ))
     return (*outs[:5], *(g[None] for g in outs[5:]))
 
 

time: 176 us -> 155 us (0.88); the launches traced: 176 us -> 153 us
  local copies, waits for them, and re-layouts: 14.6 us -> 0 us
  Pallas kernels: 161 us -> 152 us
    unnamed x12 -> x0, local copies, waits for them, and re-layouts: 14.6 us -> none
    pallas_call x1, Pallas kernels: 161 us -> 146 us  [whole(): pl.pallas_call(kernel, out_shape=[jax.ShapeDtypeStruct(x.shape, BF16), ja...]
    pallas_call x0 -> x1, Pallas kernels: none -> 5.71 us  [hand_out(): pl.pallas_call(kernel, out_shape=[jax.ShapeDtypeStruct(a.shape, a.dtype)...]
where the time goes in v4:
time: 155 us; the launch traced here: 153 us
  Pallas kernels  152 us (98%)
    pallas_call x1, Pallas kernels, whole(): pl.pallas_call(kernel, out_shape=[jax.ShapeDtypeStruct(x.shape, BF16), ja...  146 us
    pallas_call x1, Pallas kernels, hand_out(): pl.pallas_call(kernel, out_shape=[jax.ShapeDtypeStruct(a.shape, a.dtype)...  5.71 us

profile of v4, /device:TPU:0, one launch (start us, length us, event | category | flops | bytes accessed | tf_op | source)
XLA Modules:
  0.0 152.9 jit_solution(5677056940443384307)
XLA Ops:
  0.6 146.4 %whole.1 = (bf16[256,256]{1,0:T(8,128)(2,1)}, bf16[256,128]{1,0:T(8,128)(2,1)}, bf16[256,128]{1,0:T(8,128)(2,1)}, bf16[256,256]{1,0:T(8,128)(2,1)}, f32[256,256]...) custom-call(s32[2,256]{1,0:T(2,128)} %bitcast.11, ...), custom_call_target="tpu_custom_call" | custom-call | tf_op jit(solution)/shard_map/whole/pallas_call | solution.py:734
  147.0 5.7 %hand_out.1 = (bf16[256,256]{1,0:T(8,128)(2,1)}, bf16[256,128]{1,0:T(8,128)(2,1)}, bf16[256,128]{1,0:T(8,128)(2,1)}, bf16[256,256]{1,0:T(8,128)(2,1)}, f32[256,2...) custom-call(bf16[256,256]{1,0:T(8,128)(2,1)} %get-tuple-element.24.refs_0_, ...), custom_call_target="tpu_custom_call" | custom-call | tf_op jit(solution)/shard_map/hand_out/pallas_call | solution.py:830

commit v5 on v4

--- a/solution.py
+++ b/solution.py
@@ -161,7 +161,9 @@
     leave_send,
     leave,
     proj_send,
-    proj_in,
+    row_in,
+    column_send,
+    column_in,
     mixed_q,
     cot_q,
     cot_own,
@@ -218,6 +220,8 @@
     l_recv,
     p_send,
     p_recv,
+    q_send,
+    q_recv,
 ):
     z, x, t = lax.axis_index("sp_0"), lax.axis_index("sp_1"), lax.axis_index("tp")
     s = 4 * z + x
@@ -415,9 +419,9 @@
             scaled_down(src, beside).wait_recv()
             across_beside(src, beside).start()
 
-    def halves_across(g):
+    def halves_across(g, f):
         return remote(
-            part.at[g, 1 - core], part_in.at[g], d_send.at[g], d_recv.at[g], partner
+            part.at[g, 1 - core, f], part_in.at[g, f], d_send.at[g, f], d_recv.at[g, f], partner
         )
 
     def compute(g):
@@ -444,10 +448,13 @@
             act[src] = hidden[part_rows]
             dgate[src] = dg[part_rows]
             dup[src] = du[part_rows]
-        for k in range(8):
-            f = slice(k * own, (k + 1) * own)
-            part[g, k % 2, k // 2] = (nt(dg, wg[f, :]) + nt(du, wu[f, :])).astype(BF16)
-        halves_across(g).start()
+        for step in (2, 1, 3, 0):
+            f = (y + step) % 4
+            for k in range(2):
+                cols = pl.ds(f * share + k * own, own)
+                part[g, k, f] = (nt(dg, wg[cols, :]) + nt(du, wu[cols, :])).astype(BF16)
+            halves_across(g, f).start()
+        sum_far(g)
 
     def both(g, f):
         return part[g, core, f].astype(F32) + part_in[g, f].astype(F32)
@@ -465,7 +472,7 @@
         )
 
     def sum_far(g):
-        halves_across(g).wait_recv()
+        halves_across(g, (y + 2) % 4).wait_recv()
         far = both(g, (y + 2) % 4)
         q1[g, 0] = far[:half].astype(BF16)
         q1[g, 1] = far[half:].astype(BF16)
@@ -474,11 +481,13 @@
 
     def sum_near(g):
         first_step(g, 0).wait_recv()
+        halves_across(g, (y + 1) % 4).wait_recv()
         above = both(g, (y + 1) % 4)
         q2[g, 0, :half] = (above[:half] + y1[g, 0].astype(F32)).astype(BF16)
         q2[g, 0, half:] = above[half:].astype(BF16)
         second_step(g, 0).start()
         first_step(g, 1).wait_recv()
+        halves_across(g, (y + 3) % 4).wait_recv()
         below = both(g, (y + 3) % 4)
         q2[g, 1, :half] = below[:half].astype(BF16)
         q2[g, 1, half:] = (below[half:] + y1[g, 1].astype(F32)).astype(BF16)
@@ -495,6 +504,7 @@
     def sum_own(g):
         second_step(g, 0).wait_recv()
         second_step(g, 1).wait_recv()
+        halves_across(g, y).wait_recv()
         total = (both(g, y) + y2[g, 0].astype(F32) + y2[g, 1].astype(F32)).astype(BF16)
         for j in range(4):
             fin[source(g, j)] = total[j * cap : (j + 1) * cap]
@@ -532,8 +542,12 @@
     ]
 
     def turn(n, carry):
-        for lag, task in enumerate(
-            (forward_own, forward_beside, compute, sum_far, sum_near, sum_own)
+        for lag, task in (
+            (0, forward_own),
+            (2, compute),
+            (1, forward_beside),
+            (3, sum_near),
+            (4, sum_own),
         ):
 
             @pl.when((n >= lag) & (n < lag + 4))
@@ -544,7 +558,7 @@
         def _():
             scan_forward()
 
-        @pl.when(n == 7)
+        @pl.when(n == 6)
         def _():
             finish_forward()
 
@@ -558,14 +572,14 @@
             grad_rows(gu, dup)
             stores[1].start()
 
-        @pl.when(n == 7)
+        @pl.when(n == 6)
         def _():
             grad_down()
             stores[2].start()
 
         return carry
 
-    lax.fori_loop(0, 9, turn, 0)
+    lax.fori_loop(0, 8, turn, 0)
 
     def take(k, carry):
         from_expert(peer(k)[0]).wait_recv()
@@ -585,66 +599,97 @@
         ref = gm.at[src] if part_rows is None else gm.at[src, part_rows]
         return remote(ref, ref, g_send.at[k], g_recv.at[k], device)
 
-    def to_column(i):
+    def to_row(i, to_x):
         return remote(
-            proj_send.at[i], proj_in.at[s], p_send.at[i], p_recv.at[s], (i // 4, i % 4, t)
+            proj_send.at[i], row_in.at[i // 4, x], p_send.at[i], p_recv.at[i // 4, x], (z, to_x, t)
         )
 
     columns = gated.shape[1]
     gated_b = gated[...]
 
-    def project(j, send=False):
-        for k in range(own // columns):
-            i = j * (own // columns) + k
+    def send_rows(j):
+        for k in range(2):
+            to_x = 2 * (j % 2) + k
+
+            @pl.when(to_x != x)
+            def _():
+                to_row(2 * j + k, to_x).start()
+
+    def project(j):
+        for k in range(2):
             block = gm[j, :, k * columns : (k + 1) * columns]
-            proj_send[i] = tn(block, gated_b).astype(BF16)
-
-            if send:
-
-                @pl.when(i != s)
-                def _():
-                    to_column(i).start()
-
-            @pl.when(i == s)
-            def _():
-                proj_in[s] = proj_send[s]
-
+            proj_send[2 * j + k] = tn(block, gated_b).astype(BF16)
         return nn(gm[j], op[pl.ds(j * own, own), :])
 
-    gather(1, t, up).start()
-    gather(2, t, down).start()
-    gather(0, t, partner).start()
-    out_grad = project(t, True)
+    def to_column(f):
+        return remote(
+            column_send.at[f], column_in.at[z], q_send.at[f], q_recv.at[z], (f, x, t)
+        )
+
+    def sum_row(f):
+        total = proj_send[4 * f + x].astype(F32)
+        for k in range(1, 4):
+            j = (x + k) % 4
+            remote(
+                proj_send.at[j], row_in.at[f, j], p_send.at[j], p_recv.at[f, j], up
+            ).wait_recv()
+            total = total + row_in[f, j].astype(F32)
+        column_send[f] = total.astype(BF16)
+
+        @pl.when(f != z)
+        def _():
+            to_column(f).start()
+
+        @pl.when(f == z)
+        def _():
+            proj_out[...] = total
+
+    moves = (
+        (1, t, up, low),
+        (2, t, up, high),
+        (3, t, down, high),
+        (4, t, down, low),
+        (0, t, partner, None),
+        (5, below, up, low),
+        (6, above, down, high),
+        (7, below, partner, None),
+        (8, above, partner, None),
+        (9, far, partner, None),
+    )
+
+    def start(k):
+        gather(*[m for m in moves if m[0] == k][0]).start()
+
+    for k in (1, 3, 2, 4, 0):
+        start(k)
+    out_grad = project(t)
+    send_rows(t)
     gather(0, mate, partner).wait_recv()
-    out_grad = out_grad + project(mate, True)
-    gather(1, below, up).wait_recv()
-    gather(3, below, up, low).start()
-    gather(5, below, partner).start()
-    gather(2, above, down).wait_recv()
-    gather(4, above, down, high).start()
-    gather(6, above, partner).start()
-    out_grad = out_grad + project(below) + project(above)
-    gather(5, m_below, partner).wait_recv()
+    out_grad = out_grad + project(mate)
+    send_rows(mate)
+    gather(1, below, up, low).wait_recv()
+    start(5)
+    gather(3, above, down, high).wait_recv()
+    start(6)
+    gather(2, below, up, high).wait_recv()
+    start(7)
+    gather(4, above, down, low).wait_recv()
+    start(8)
+    out_grad = out_grad + project(above)
+    send_rows(above)
+    out_grad = out_grad + project(below)
+    gather(8, m_above, partner).wait_recv()
+    out_grad = out_grad + project(m_above)
+    send_rows(m_above)
+    gather(7, m_below, partner).wait_recv()
     out_grad = out_grad + project(m_below)
-    gather(6, m_above, partner).wait_recv()
-    out_grad = out_grad + project(m_above)
-    gather(3, far, up, low).wait_recv()
-    gather(4, far, down, high).wait_recv()
-    gather(7, far, partner).start()
+    gather(5, far, up, low).wait_recv()
+    gather(6, far, down, high).wait_recv()
+    start(9)
     out_grad = out_grad + project(far)
-    gather(7, m_far, partner).wait_recv()
+    gather(9, m_far, partner).wait_recv()
     out_grad = out_grad + project(m_far)
 
-    def send_column(k, carry):
-        i, device = peer(k)
-
-        @pl.when(device[0] != y)
-        def _():
-            to_column(i).start()
-
-        return carry
-
-    lax.fori_loop(1, experts, send_column, 0)
     row, col = decays(ld[...])
     leads = by_lane(jnp.exp(col), tokens, heads)
     gate = gate_in[...].astype(F32)
@@ -652,6 +697,8 @@
     back_send[...] = tn(lead_grad, c_in[...]).astype(BF16).reshape(experts, STEP, STATE)
     back_in[s] = back_send[s]
     backs[0]()
+    for j in (below, m_below, far, m_far):
+        send_rows(j)
     backward = mix_backward(
         x_in[...], b_in[...], c_in[...], gate, out_grad, y_ref[...], lead_grad,
         enter[...].reshape(x_in.shape[1], STATE), row, col, heads
@@ -661,19 +708,23 @@
     scan_back()
     tails = by_lane(jnp.exp(col[tokens - 1 : tokens, :] - col), tokens, heads)
     tail_values = (x_in[...].astype(F32) * tails).astype(BF16)
+    sum_row(y)
+    sum_row((y + 1) % 4)
     leaves[1]()
     leaving = leave[...].reshape(x_in.shape[1], STATE)
     dx_out[...] = (backward[0] + tails * nt(b_in[...], leaving)).astype(BF16)
     db_out[...] = (backward[1] + nn(tail_values, leaving)).astype(BF16)
-
-    def column(k, total):
-        i = peer(k)[0]
+    sum_row((y + 3) % 4)
+    sum_row((y + 2) % 4)
+    for k in range(1, 4):
+        j = (z + k) % 4
         remote(
-            proj_send.at[i], proj_in.at[i], p_send.at[i], p_recv.at[i], up
+            column_send.at[j], column_in.at[j], q_send.at[j], q_recv.at[j], up
         ).wait_recv()
-        return total + proj_in[i].astype(F32)
-
-    proj_out[...] = lax.fori_loop(1, experts, column, proj_in[s].astype(F32))
+        proj_out[...] += column_in[j].astype(F32)
+        to_column(j).wait_send()
+        for f in range(4):
+            to_row(4 * f + (x + k) % 4, x).wait_send()
     for exchange in (states, enters, backs, leaves):
         exchange[2]()
 
@@ -681,7 +732,6 @@
         e = peer(k)[0]
         to_expert(e).wait_send()
         to_owner(0, e).wait_send()
-        to_column(e).wait_send()
         return carry
 
     lax.fori_loop(1, experts, sent, 0)
@@ -696,21 +746,16 @@
     lax.fori_loop(0, experts, forwarded, 0)
 
     def summed(g, carry):
-        halves_across(g).wait_send()
+        for f in range(4):
+            halves_across(g, f).wait_send()
         for way in range(2):
             first_step(g, way).wait_send()
             second_step(g, way).wait_send()
         return carry
 
     lax.fori_loop(0, 4, summed, 0)
-    gather(0, t, partner).wait_send()
-    gather(1, t, up).wait_send()
-    gather(2, t, down).wait_send()
-    gather(3, below, up, low).wait_send()
-    gather(4, above, down, high).wait_send()
-    gather(5, below, partner).wait_send()
-    gather(6, above, partner).wait_send()
-    gather(7, far, partner).wait_send()
+    for move in moves:
+        gather(*move).wait_send()
     for store in stores:
         store.wait()
 
@@ -759,7 +804,9 @@
             buf(experts, STEP, STATE),
             buf(experts, STEP, STATE),
             buf(experts, width // experts, channels),
-            buf(experts, width // experts, channels),
+            buf(4, 4, width // experts, channels),
+            buf(4, width // experts, channels),
+            buf(4, width // experts, channels),
             buf(tokens, share),
             buf(tokens, share),
             buf(tokens, own),
@@ -788,11 +835,13 @@
             dma((10,)),
         ]
         + [dma((experts,))] * 10
-        + [dma((4,))] * 2
+        + [dma((4, 4))] * 2
         + [dma((4, 2))] * 4
         + [dma((experts,))] * 2
-        + [dma((8,))] * 2
-        + [dma((experts,))] * 10,
+        + [dma((10,))] * 2
+        + [dma((experts,))] * 9
+        + [dma((4, 4))]
+        + [dma((4,))] * 2,
         compiler_params=pltpu.CompilerParams(
             collective_id=0, has_side_effects=True, vmem_limit_bytes=60 * 2**20
         ),

time: 155 us -> 144 us (0.929)
  Pallas kernels: 152 us -> 141 us
    pallas_call x1, Pallas kernels: 146 us -> 135 us  [whole(): pl.pallas_call(kernel, out_shape=[jax.ShapeDtypeStruct(x.shape, BF16), ja...]
where the time goes in v5:
time: 144 us; the launch traced here: 142 us
  Pallas kernels  141 us (98%)
    pallas_call x1, Pallas kernels, whole(): pl.pallas_call(kernel, out_shape=[jax.ShapeDtypeStruct(x.shape, BF16), ja...  135 us
    pallas_call x1, Pallas kernels, hand_out(): pl.pallas_call(kernel, out_shape=[jax.ShapeDtypeStruct(a.shape, a.dtype)...  5.71 us

profile of v5, /device:TPU:0, one launch (start us, length us, event | category | flops | bytes accessed | tf_op | source)
XLA Modules:
  0.0 142.0 jit_solution(15018098611801547350)
XLA Ops:
  0.6 135.5 %whole.1 = (bf16[256,256]{1,0:T(8,128)(2,1)}, bf16[256,128]{1,0:T(8,128)(2,1)}, bf16[256,128]{1,0:T(8,128)(2,1)}, bf16[256,256]{1,0:T(8,128)(2,1)}, f32[256,256]...) custom-call(s32[2,256]{1,0:T(2,128)} %bitcast.11, ...), custom_call_target="tpu_custom_call" | custom-call | tf_op jit(solution)/shard_map/whole/pallas_call | solution.py:779
  136.1 5.7 %hand_out.1 = (bf16[256,256]{1,0:T(8,128)(2,1)}, bf16[256,128]{1,0:T(8,128)(2,1)}, bf16[256,128]{1,0:T(8,128)(2,1)}, bf16[256,256]{1,0:T(8,128)(2,1)}, f32[256,2...) custom-call(bf16[256,256]{1,0:T(8,128)(2,1)} %get-tuple-element.24.refs_0_, ...), custom_call_target="tpu_custom_call" | custom-call | tf_op jit(solution)/shard_map/hand_out/pallas_call | solution.py:879

commit v6 on v5

--- a/solution.py
+++ b/solution.py
@@ -160,10 +160,7 @@
     back_in,
     leave_send,
     leave,
-    proj_send,
-    row_in,
-    column_send,
-    column_in,
+    features,
     mixed_q,
     cot_q,
     cot_own,
@@ -186,6 +183,7 @@
     y2,
     fin,
     ret,
+    sums,
     gg,
     gu,
     gd,
@@ -222,6 +220,8 @@
     p_recv,
     q_send,
     q_recv,
+    r_send,
+    r_recv,
 ):
     z, x, t = lax.axis_index("sp_0"), lax.axis_index("sp_1"), lax.axis_index("tp")
     s = 4 * z + x
@@ -232,7 +232,8 @@
     partner_beside = (partner_q + 2) % 4
     up, down, partner = (z, x, (t + 2) % 8), (z, x, (t + 6) % 8), (z, x, t + 1 - 2 * core)
     tokens, width = mixed.shape
-    experts, _, cap, share = sendbuf.shape
+    experts, _, _, cap, chunk = sendbuf.shape
+    share = 2 * chunk
     own = width // 8
 
     loads = [
@@ -263,13 +264,73 @@
 
     slot_ref[...] = slots(ids[...], experts)
     weight_ref[...] = weight_rows(ids[...], wts[...], experts)
+    row, col = decays(ld[...])
+    inner, last = mix_local(x_in[...], b_in[...], c_in[...], row, col, heads)
+    y_ref[...] = inner
+    totals = jnp.broadcast_to(row[:, tokens - 1 : tokens], (8, STATE))
+    state_send[:, :STEP, :] = last.reshape(experts, STEP, STATE)
+    state_send[:, STEP:, :] = jnp.broadcast_to(totals[None], (experts, 8, STATE))
+    state_in[s] = state_send[s]
+
+    def over_sp(source_ref, target_ref, send, recv):
+        def copy(k):
+            j, device = peer(k)
+            return remote(source_ref.at[j], target_ref.at[s], send.at[j], recv.at[s], device)
+
+        def wait(k):
+            j, device = peer(k)
+            remote(source_ref.at[j], target_ref.at[j], send.at[j], recv.at[j], device).wait_recv()
+
+        def each(action):
+            def step(k, carry):
+                action(k)
+                return carry
+
+            lax.fori_loop(1, experts, step, 0)
+
+        return (
+            lambda: each(lambda k: copy(k).start()),
+            lambda: each(wait),
+            lambda: each(lambda k: copy(k).wait_send()),
+        )
+
+    def gated_to(k):
+        j, device = peer(k)
+        return remote(gated.at[s], gated.at[s], q_send.at[j], q_recv.at[s], device)
+
+    def gated_from(k):
+        j, device = peer(k)
+        return remote(gated.at[j], gated.at[j], q_send.at[j], q_recv.at[j], device)
+
+    def every(action):
+        def step(k, carry):
+            action(k)
+            return carry
+
+        lax.fori_loop(1, experts, step, 0)
+
+    gates = (
+        lambda: every(lambda k: gated_to(k).start()),
+        lambda: every(lambda k: gated_from(k).wait_recv()),
+        lambda: every(lambda k: gated_to(k).wait_send()),
+    )
+    states = over_sp(state_send, state_in, e_send, e_recv)
+    enters = over_sp(enter_send, enter, f_send, f_recv)
+    backs = over_sp(back_send, back_in, b_send, b_recv)
+    leaves = over_sp(leave_send, leave, l_send, l_recv)
+
     loads[0].wait()
     loads[1].wait()
     pl.semaphore_wait(barrier, experts - 1 + 3)
-
-    def to_expert(e):
+    states[0]()
+
+    def to_expert(e, h):
         return remote(
-            sendbuf.at[e], rows.at[quarter, s], a_send.at[e], a_recv.at[s], (e // 4, e % 4, t)
+            sendbuf.at[e, h],
+            rows.at[quarter, s, h],
+            a_send.at[e, h],
+            a_recv.at[s, h],
+            (e // 4, e % 4, t),
         )
 
     def build(g, carry):
@@ -289,58 +350,25 @@
         scaled = (nn(one, cot_q[...]) * w).astype(BF16)
         for j in range(4):
             e = peer(4 * g + j)[0]
-            sendbuf[e, 0] = plain[j * cap : (j + 1) * cap]
-            sendbuf[e, 1] = scaled[j * cap : (j + 1) * cap]
-        for j in range(4):
-            e = peer(4 * g + j)[0]
-            if j > 0:
-                to_expert(e).start()
-            else:
-
-                @pl.when(g > 0)
-                def _():
-                    to_expert(e).start()
+            for h in range(2):
+                part_rows, f = slice(j * cap, (j + 1) * cap), slice(h * chunk, (h + 1) * chunk)
+                sendbuf[e, h, 0] = plain[part_rows, f]
+                sendbuf[e, h, 1] = scaled[part_rows, f]
+        for h in range(2):
+            for j in range(4):
+                e = peer(4 * g + j)[0]
+                if j > 0:
+                    to_expert(e, h).start()
+                else:
+
+                    @pl.when(g > 0)
+                    def _():
+                        to_expert(e, h).start()
 
         return carry
 
     lax.fori_loop(0, 4, build, 0)
     rows[quarter, s] = sendbuf[s]
-
-    row, col = decays(ld[...])
-    inner, last = mix_local(x_in[...], b_in[...], c_in[...], row, col, heads)
-    y_ref[...] = inner
-    totals = jnp.broadcast_to(row[:, tokens - 1 : tokens], (8, STATE))
-    state_send[:, :STEP, :] = last.reshape(experts, STEP, STATE)
-    state_send[:, STEP:, :] = jnp.broadcast_to(totals[None], (experts, 8, STATE))
-    state_in[s] = state_send[s]
-
-    def over_sp(source_ref, target_ref, send, recv):
-        def copy(k):
-            j, device = peer(k)
-            return remote(source_ref.at[j], target_ref.at[s], send.at[j], recv.at[s], device)
-
-        def wait(k):
-            j, device = peer(k)
-            remote(source_ref.at[j], target_ref.at[j], send.at[j], recv.at[j], device).wait_recv()
-
-        def each(action):
-            def step(k, carry):
-                action(k)
-                return carry
-
-            lax.fori_loop(1, experts, step, 0)
-
-        return (
-            lambda: each(lambda k: copy(k).start()),
-            lambda: each(wait),
-            lambda: each(lambda k: copy(k).wait_send()),
-        )
-
-    states = over_sp(state_send, state_in, e_send, e_recv)
-    enters = over_sp(enter_send, enter, f_send, f_recv)
-    backs = over_sp(back_send, back_in, b_send, b_recv)
-    leaves = over_sp(leave_send, leave, l_send, l_recv)
-    states[0]()
     for load in loads[2:]:
         load.wait()
 
@@ -373,71 +401,81 @@
         whole = y_ref[...] + leads * nt(c_in[...], entering)
         g = gate_in[...].astype(F32)
         y_ref[...] = whole
-        gated[...] = (whole * (g * jax.nn.sigmoid(g))).astype(BF16)
+        gated[s] = (whole * (g * jax.nn.sigmoid(g))).astype(BF16)
+        gates[0]()
 
     def source(g, j):
         return 4 * ((z + 4 - j) % 4) + (x + 8 - j - g) % 4
 
-    def arrived(src):
-        return remote(sendbuf.at[src], rows.at[quarter, src], a_send.at[src], a_recv.at[src], up)
-
-    def rows_up(src, q):
+    def arrived(src, h):
         return remote(
-            rows.at[q, src, 0], rows.at[q, src, 0], yr_send.at[src], yr_recv.at[src], up
+            sendbuf.at[src, h], rows.at[quarter, src, h], a_send.at[src, h], a_recv.at[src, h], up
         )
 
-    def scaled_down(src, q):
-        return remote(
-            rows.at[q, src, 1], rows.at[q, src, 1], ys_send.at[src], ys_recv.at[src], down
-        )
-
-    def across(src, q):
-        return remote(rows.at[q, src], rows.at[q, src], pa_send.at[src], pa_recv.at[src], partner)
-
-    def across_beside(src, q):
-        return remote(rows.at[q, src], rows.at[q, src], pn_send.at[src], pn_recv.at[src], partner)
-
-    def forward_own(g):
-        for j in range(4):
-            src = source(g, j)
-            if j > 0:
-                arrived(src).wait_recv()
-            else:
-
-                @pl.when(g > 0)
-                def _():
-                    arrived(src).wait_recv()
-
-            rows_up(src, quarter).start()
-            scaled_down(src, quarter).start()
-            across(src, quarter).start()
-
-    def forward_beside(g):
-        for j in range(4):
-            src = source(g, j)
-            rows_up(src, beside).wait_recv()
-            scaled_down(src, beside).wait_recv()
-            across_beside(src, beside).start()
+    def rows_up(src, h, q):
+        ref = rows.at[q, src, h, 0]
+        return remote(ref, ref, yr_send.at[src, h], yr_recv.at[src, h], up)
+
+    def scaled_down(src, h, q):
+        ref = rows.at[q, src, h, 1]
+        return remote(ref, ref, ys_send.at[src, h], ys_recv.at[src, h], down)
+
+    def across(src, h, q):
+        ref = rows.at[q, src, h]
+        return remote(ref, ref, pa_send.at[src, h], pa_recv.at[src, h], partner)
+
+    def across_beside(src, h, q):
+        ref = rows.at[q, src, h]
+        return remote(ref, ref, pn_send.at[src, h], pn_recv.at[src, h], partner)
+
+    def unit(u):
+        g, h, j = u // 8, u // 4 % 2, u % 4
+        return source(g, j), h
+
+    def forward_own(u):
+        src, h = unit(u)
+
+        @pl.when(src != s)
+        def _():
+            arrived(src, h).wait_recv()
+
+        rows_up(src, h, quarter).start()
+        scaled_down(src, h, quarter).start()
+        across(src, h, quarter).start()
+
+    def forward_beside(u):
+        src, h = unit(u)
+        rows_up(src, h, beside).wait_recv()
+        scaled_down(src, h, beside).wait_recv()
+        across_beside(src, h, beside).start()
 
     def halves_across(g, f):
         return remote(
             part.at[g, 1 - core, f], part_in.at[g, f], d_send.at[g, f], d_recv.at[g, f], partner
         )
 
-    def compute(g):
+    def multiply(g, q):
         sources = [source(g, j) for j in range(4)]
-        for src in sources:
-            across(src, partner_q).wait_recv()
-            across_beside(src, partner_beside).wait_recv()
-        n = 4 * cap
-        gate_pre = up_pre = d_hidden = jnp.zeros((n, wg.shape[1]), F32)
-        for q in range(4):
-            r = jnp.concatenate([rows[q, src, 0] for src in sources], axis=0)
-            sc = jnp.concatenate([rows[q, src, 1] for src in sources], axis=0)
-            f = slice(q * share, (q + 1) * share)
-            gate_pre = gate_pre + nn(r, wg[f, :])
-            up_pre = up_pre + nn(r, wu[f, :])
-            d_hidden = d_hidden + nt(sc, wd[:, f])
+
+        @pl.when(q == 0)
+        def _():
+            for src in sources:
+                for h in range(2):
+                    across(src, h, partner_q).wait_recv()
+                    across_beside(src, h, partner_beside).wait_recv()
+            sums[...] = jnp.zeros_like(sums)
+
+        for h in range(2):
+            r = jnp.concatenate([rows[q, src, h, 0] for src in sources], axis=0)
+            sc = jnp.concatenate([rows[q, src, h, 1] for src in sources], axis=0)
+            f = pl.ds(pl.multiple_of(q * share + h * chunk, chunk), chunk)
+            sums[0] += nn(r, wg[f, :])
+            sums[1] += nn(r, wu[f, :])
+            sums[2] += nt(sc, wd[:, f])
+
+    def activate(g):
+        sources = [source(g, j) for j in range(4)]
+        gate_pre, up_pre, d_hidden = sums[0], sums[1], sums[2]
         sigma = jax.nn.sigmoid(gate_pre)
         silu = gate_pre * sigma
         dg = (d_hidden * up_pre * sigma * (1.0 + gate_pre * (1.0 - sigma))).astype(BF16)
@@ -448,13 +486,16 @@
             act[src] = hidden[part_rows]
             dgate[src] = dg[part_rows]
             dup[src] = du[part_rows]
-        for step in (2, 1, 3, 0):
-            f = (y + step) % 4
-            for k in range(2):
-                cols = pl.ds(f * share + k * own, own)
-                part[g, k, f] = (nt(dg, wg[cols, :]) + nt(du, wu[cols, :])).astype(BF16)
-            halves_across(g, f).start()
-        sum_far(g)
+
+    def back(g, k):
+        sources = [source(g, j) for j in range(4)]
+        dg = jnp.concatenate([dgate[src] for src in sources], axis=0)
+        du = jnp.concatenate([dup[src] for src in sources], axis=0)
+        f = (y + 2 + 3 * k) % 4
+        for m in range(2):
+            cols = pl.ds(pl.multiple_of(f * share + m * own, own), own)
+            part[g, m, f] = (nt(dg, wg[cols, :]) + nt(du, wu[cols, :])).astype(BF16)
+        halves_across(g, f).start()
 
     def both(g, f):
         return part[g, core, f].astype(F32) + part_in[g, f].astype(F32)
@@ -523,17 +564,17 @@
                     ret[s] = fin[s]
 
     def grad_rows(target, which):
-        for q in range(4):
-            r = rows[q, :, 0].reshape(experts * cap, share)
-            target[q * share : (q + 1) * share, :] = tn(
+        for k in range(8):
+            r = rows[k // 2, :, k % 2, 0].reshape(experts * cap, chunk)
+            target[k * chunk : (k + 1) * chunk, :] = tn(
                 r, which[...].reshape(experts * cap, -1)
             ).astype(BF16)
 
     def grad_down():
         hidden = act[...].reshape(experts * cap, -1)
-        for q in range(4):
-            sc = rows[q, :, 1].reshape(experts * cap, share)
-            gd[:, q * share : (q + 1) * share] = tn(hidden, sc).astype(BF16)
+        for k in range(8):
+            sc = rows[k // 2, :, k % 2, 1].reshape(experts * cap, chunk)
+            gd[:, k * chunk : (k + 1) * chunk] = tn(hidden, sc).astype(BF16)
 
     stores = [
         pltpu.make_async_copy(gg, gg_hbm, local.at[6]),
@@ -541,45 +582,98 @@
         pltpu.make_async_copy(gd, gd_hbm, local.at[8]),
     ]
 
-    def turn(n, carry):
-        for lag, task in (
-            (0, forward_own),
-            (2, compute),
-            (1, forward_beside),
-            (3, sum_near),
-            (4, sum_own),
-        ):
-
-            @pl.when((n >= lag) & (n < lag + 4))
+    def turn(u, carry):
+        @pl.when(u < 32)
+        def _():
+            forward_own(u)
+
+        v = u - 5
+
+        @pl.when((v >= 0) & (v < 32))
+        def _():
+            forward_beside(v)
+
+        m = u - 14
+        g, k = (m + 64) // 8 - 8, (m + 64) % 8
+        active = (m >= 0) & (m < 32)
+
+        @pl.when(active & (k < 4))
+        def _():
+            multiply(g, k)
+
+        @pl.when(active & (k == 3))
+        def _():
+            activate(g)
+
+        @pl.when(active & (k >= 4))
+        def _():
+            back(g, k - 4)
+
+        @pl.when(active & (k == 5))
+        def _():
+            sum_far(g)
+
+        for late, task in ((11, sum_near), (17, sum_own)):
+            w = m - late
+
+            @pl.when((w >= 0) & (w < 32) & ((w + 64) % 8 == 0))
             def _():
-                task(n - lag)
-
-        @pl.when(n == 4)
+                task((w + 64) // 8 - 8)
+
+        @pl.when(u == 20)
         def _():
             scan_forward()
 
-        @pl.when(n == 6)
+        @pl.when(u == 33)
         def _():
             finish_forward()
 
-        @pl.when(n == 5)
+        @pl.when(m == 32)
         def _():
             grad_rows(gg, dgate)
             stores[0].start()
 
-        @pl.when(n == 6)
+        @pl.when(m == 24 + 11)
         def _():
             grad_rows(gu, dup)
             stores[1].start()
-
-        @pl.when(n == 6)
-        def _():
             grad_down()
             stores[2].start()
 
         return carry
 
-    lax.fori_loop(0, 8, turn, 0)
+    lax.fori_loop(0, 14 + 24 + 17 + 1, turn, 0)
+
+    def sent(k, carry):
+        e = peer(k)[0]
+        to_expert(e, 0).wait_send()
+        to_expert(e, 1).wait_send()
+        to_owner(0, e).wait_send()
+        return carry
+
+    lax.fori_loop(1, experts, sent, 0)
+
+    def forwarded(k, carry):
+        for h in range(2):
+            rows_up(k, h, quarter).wait_send()
+            scaled_down(k, h, quarter).wait_send()
+            across(k, h, quarter).wait_send()
+            across_beside(k, h, beside).wait_send()
+        return carry
+
+    lax.fori_loop(0, experts, forwarded, 0)
+
+    def summed(g, carry):
+        for f in range(4):
+            halves_across(g, f).wait_send()
+        for way in range(2):
+            first_step(g, way).wait_send()
+            second_step(g, way).wait_send()
+        return carry
+
+    lax.fori_loop(0, 4, summed, 0)
+    for exchange in (states, enters):
+        exchange[2]()
 
     def take(k, carry):
         from_expert(peer(k)[0]).wait_recv()
@@ -599,50 +693,49 @@
         ref = gm.at[src] if part_rows is None else gm.at[src, part_rows]
         return remote(ref, ref, g_send.at[k], g_recv.at[k], device)
 
-    def to_row(i, to_x):
+    columns = gated.shape[2]
+    my_half = pl.ds(core * (tokens // 2), tokens // 2)
+    mate_half = pl.ds((1 - core) * (tokens // 2), tokens // 2)
+
+    def to_features(i, k):
         return remote(
-            proj_send.at[i], row_in.at[i // 4, x], p_send.at[i], p_recv.at[i // 4, x], (z, to_x, t)
+            gm.at[i // 2, my_half, k * columns : (k + 1) * columns],
+            features.at[s, my_half],
+            p_send.at[i],
+            p_recv.at[s],
+            (i // 4, i % 4, t),
         )
 
-    columns = gated.shape[1]
-    gated_b = gated[...]
+    def share_half(src, half_rows):
+        ref = features.at[src, half_rows]
+        return remote(ref, ref, r_send.at[src], r_recv.at[src], partner)
 
     def send_rows(j):
         for k in range(2):
-            to_x = 2 * (j % 2) + k
-
-            @pl.when(to_x != x)
+            i = 2 * j + k
+
+            @pl.when(i != s)
             def _():
-                to_row(2 * j + k, to_x).start()
+                to_features(i, k).start()
+
+            @pl.when(i == s)
+            def _():
+                features[s] = gm[j, :, k * columns : (k + 1) * columns]
 
     def project(j):
-        for k in range(2):
-            block = gm[j, :, k * columns : (k + 1) * columns]
-            proj_send[2 * j + k] = tn(block, gated_b).astype(BF16)
         return nn(gm[j], op[pl.ds(j * own, own), :])
 
-    def to_column(f):
-        return remote(
-            column_send.at[f], column_in.at[z], q_send.at[f], q_recv.at[z], (f, x, t)
-        )
-
-    def sum_row(f):
-        total = proj_send[4 * f + x].astype(F32)
-        for k in range(1, 4):
-            j = (x + k) % 4
-            remote(
-                proj_send.at[j], row_in.at[f, j], p_send.at[j], p_recv.at[f, j], up
-            ).wait_recv()
-            total = total + row_in[f, j].astype(F32)
-        column_send[f] = total.astype(BF16)
-
-        @pl.when(f != z)
-        def _():
-            to_column(f).start()
-
-        @pl.when(f == z)
-        def _():
-            proj_out[...] = total
+    def take_features(k):
+        src = peer(k)[0]
+        remote(
+            features.at[src, my_half], features.at[src, my_half], p_send.at[src], p_recv.at[src], up
+        ).wait_recv()
+        share_half(src, my_half).start()
+
+    def multiply_features(k):
+        src = peer(k)[0]
+        share_half(src, mate_half).wait_recv()
+        proj_out[...] += tn(features[src], gated[src])
 
     moves = (
         (1, t, up, low),
@@ -678,11 +771,13 @@
     out_grad = out_grad + project(above)
     send_rows(above)
     out_grad = out_grad + project(below)
+    send_rows(below)
     gather(8, m_above, partner).wait_recv()
     out_grad = out_grad + project(m_above)
     send_rows(m_above)
     gather(7, m_below, partner).wait_recv()
     out_grad = out_grad + project(m_below)
+    send_rows(m_below)
     gather(5, far, up, low).wait_recv()
     gather(6, far, down, high).wait_recv()
     start(9)
@@ -697,7 +792,7 @@
     back_send[...] = tn(lead_grad, c_in[...]).astype(BF16).reshape(experts, STEP, STATE)
     back_in[s] = back_send[s]
     backs[0]()
-    for j in (below, m_below, far, m_far):
+    for j in (far, m_far):
         send_rows(j)
     backward = mix_backward(
         x_in[...], b_in[...], c_in[...], gate, out_grad, y_ref[...], lead_grad,
@@ -708,56 +803,29 @@
     scan_back()
     tails = by_lane(jnp.exp(col[tokens - 1 : tokens, :] - col), tokens, heads)
     tail_values = (x_in[...].astype(F32) * tails).astype(BF16)
-    sum_row(y)
-    sum_row((y + 1) % 4)
+    every(take_features)
+    gates[1]()
+    proj_out[...] = tn(features[s], gated[s])
+    every(multiply_features)
+    def features_sent(k):
+        i = peer(k)[0]
+        to_features(i, 0).wait_send()
+        share_half(i, my_half).wait_send()
+
+    every(features_sent)
+    gates[2]()
+    backs[2]()
+    for move in moves:
+        gather(*move).wait_send()
+    for store in stores:
+        store.wait()
+
     leaves[1]()
     leaving = leave[...].reshape(x_in.shape[1], STATE)
     dx_out[...] = (backward[0] + tails * nt(b_in[...], leaving)).astype(BF16)
     db_out[...] = (backward[1] + nn(tail_values, leaving)).astype(BF16)
-    sum_row((y + 3) % 4)
-    sum_row((y + 2) % 4)
-    for k in range(1, 4):
-        j = (z + k) % 4
-        remote(
-            column_send.at[j], column_in.at[j], q_send.at[j], q_recv.at[j], up
-        ).wait_recv()
-        proj_out[...] += column_in[j].astype(F32)
-        to_column(j).wait_send()
-        for f in range(4):
-            to_row(4 * f + (x + k) % 4, x).wait_send()
-    for exchange in (states, enters, backs, leaves):
-        exchange[2]()
-
-    def sent(k, carry):
-        e = peer(k)[0]
-        to_expert(e).wait_send()
-        to_owner(0, e).wait_send()
-        return carry
-
-    lax.fori_loop(1, experts, sent, 0)
-
-    def forwarded(k, carry):
-        rows_up(k, quarter).wait_send()
-        scaled_down(k, quarter).wait_send()
-        across(k, quarter).wait_send()
-        across_beside(k, beside).wait_send()
-        return carry
-
-    lax.fori_loop(0, experts, forwarded, 0)
-
-    def summed(g, carry):
-        for f in range(4):
-            halves_across(g, f).wait_send()
-        for way in range(2):
-            first_step(g, way).wait_send()
-            second_step(g, way).wait_send()
-        return carry
-
-    lax.fori_loop(0, 4, summed, 0)
-    for move in moves:
-        gather(*move).wait_send()
-    for store in stores:
-        store.wait()
+
+    leaves[2]()
 
 
 def whole(ids, wts, ld, x, b, c, gate, mixed, cot, wg, wu, wd, op, experts, cap, heads):
@@ -794,7 +862,7 @@
             buf(8, tokens, own),
             buf(*op.shape),
             buf(tokens, channels, dtype=F32),
-            buf(tokens, channels),
+            buf(experts, tokens, channels),
             buf(experts, STEP + 8, STATE, dtype=F32),
             buf(experts, STEP + 8, STATE, dtype=F32),
             buf(experts, STEP, STATE),
@@ -803,10 +871,7 @@
             buf(experts, STEP, STATE),
             buf(experts, STEP, STATE),
             buf(experts, STEP, STATE),
-            buf(experts, width // experts, channels),
-            buf(4, 4, width // experts, channels),
-            buf(4, width // experts, channels),
-            buf(4, width // experts, channels),
+            buf(experts, tokens, width // experts),
             buf(tokens, share),
             buf(tokens, share),
             buf(tokens, own),
@@ -816,8 +881,8 @@
             buf(experts, tokens, dtype=jnp.int32),
             buf(experts, tokens, dtype=F32),
             buf(experts, cap, tokens),
-            buf(experts, 2, cap, share),
-            buf(4, experts, 2, cap, share),
+            buf(experts, 2, 2, cap, own),
+            buf(4, experts, 2, 2, cap, own),
             buf(experts, cap, hidden),
             buf(experts, cap, hidden),
             buf(experts, cap, hidden),
@@ -829,19 +894,18 @@
             buf(4, 2, n, own),
             buf(experts, cap, own),
             buf(experts, cap, own),
+            buf(3, n, hidden, dtype=F32),
             buf(*wg.shape),
             buf(*wu.shape),
             buf(*wd.shape),
             dma((10,)),
         ]
-        + [dma((experts,))] * 10
+        + [dma((experts, 2))] * 10
         + [dma((4, 4))] * 2
         + [dma((4, 2))] * 4
         + [dma((experts,))] * 2
         + [dma((10,))] * 2
-        + [dma((experts,))] * 9
-        + [dma((4, 4))]
-        + [dma((4,))] * 2,
+        + [dma((experts,))] * 14,
         compiler_params=pltpu.CompilerParams(
             collective_id=0, has_side_effects=True, vmem_limit_bytes=60 * 2**20
         ),

time: 144 us -> 141 us (0.979)
  Pallas kernels: 141 us -> 139 us
    pallas_call x1, Pallas kernels: 135 us -> 133 us  [whole(): pl.pallas_call(kernel, out_shape=[jax.ShapeDtypeStruct(x.shape, BF16), ja...]
where the time goes in v6:
time: 141 us; the launch traced here: 140 us
  Pallas kernels  139 us (99%)
    pallas_call x1, Pallas kernels, whole(): pl.pallas_call(kernel, out_shape=[jax.ShapeDtypeStruct(x.shape, BF16), ja...  133 us
    pallas_call x1, Pallas kernels, hand_out(): pl.pallas_call(kernel, out_shape=[jax.ShapeDtypeStruct(a.shape, a.dtype)...  5.71 us

profile of v6, /device:TPU:0, one launch (start us, length us, event | category | flops | bytes accessed | tf_op | source)
XLA Modules:
  0.0 139.6 jit_solution(10384226413895061742)
XLA Ops:
  0.6 133.1 %whole.1 = (bf16[256,256]{1,0:T(8,128)(2,1)}, bf16[256,128]{1,0:T(8,128)(2,1)}, bf16[256,128]{1,0:T(8,128)(2,1)}, bf16[256,256]{1,0:T(8,128)(2,1)}, f32[256,256]...) custom-call(s32[2,256]{1,0:T(2,128)} %bitcast.11, ...), custom_call_target="tpu_custom_call" | custom-call | tf_op jit(solution)/shard_map/whole/pallas_call | solution.py:847
  133.7 5.7 %hand_out.1 = (bf16[256,256]{1,0:T(8,128)(2,1)}, bf16[256,128]{1,0:T(8,128)(2,1)}, bf16[256,128]{1,0:T(8,128)(2,1)}, bf16[256,256]{1,0:T(8,128)(2,1)}, f32[256,2...) custom-call(bf16[256,256]{1,0:T(8,128)(2,1)} %get-tuple-element.24.refs_0_, ...), custom_call_target="tpu_custom_call" | custom-call | tf_op jit(solution)/shard_map/hand_out/pallas_call | solution.py:943

commit v7 on v6

--- a/solution.py
+++ b/solution.py
@@ -140,14 +140,19 @@
     wu_hbm,
     wd_hbm,
     op_hbm,
+    dx_hbm,
+    db_hbm,
+    dc_hbm,
+    dgate_hbm,
+    proj_hbm,
+    gg_hbm,
+    gu_hbm,
+    gd_hbm,
     dx_out,
     db_out,
     dc_out,
     dgate_out,
     proj_out,
-    gg_hbm,
-    gu_hbm,
-    gd_hbm,
     gm,
     op,
     y_ref,
@@ -191,9 +196,8 @@
     a_send,
     a_recv,
     yr_send,
-    yr_recv,
+    n_recv,
     ys_send,
-    ys_recv,
     pa_send,
     pa_recv,
     pn_send,
@@ -272,35 +276,7 @@
     state_send[:, STEP:, :] = jnp.broadcast_to(totals[None], (experts, 8, STATE))
     state_in[s] = state_send[s]
 
-    def over_sp(source_ref, target_ref, send, recv):
-        def copy(k):
-            j, device = peer(k)
-            return remote(source_ref.at[j], target_ref.at[s], send.at[j], recv.at[s], device)
-
-        def wait(k):
-            j, device = peer(k)
-            remote(source_ref.at[j], target_ref.at[j], send.at[j], recv.at[j], device).wait_recv()
-
-        def each(action):
-            def step(k, carry):
-                action(k)
-                return carry
-
-            lax.fori_loop(1, experts, step, 0)
-
-        return (
-            lambda: each(lambda k: copy(k).start()),
-            lambda: each(wait),
-            lambda: each(lambda k: copy(k).wait_send()),
-        )
-
-    def gated_to(k):
-        j, device = peer(k)
-        return remote(gated.at[s], gated.at[s], q_send.at[j], q_recv.at[s], device)
-
-    def gated_from(k):
-        j, device = peer(k)
-        return remote(gated.at[j], gated.at[j], q_send.at[j], q_recv.at[j], device)
+    others = pl.ds(0, experts - 1)
 
     def every(action):
         def step(k, carry):
@@ -309,10 +285,27 @@
 
         lax.fori_loop(1, experts, step, 0)
 
+    def over_sp(source_ref, target_ref, send, recv):
+        def copy(k):
+            j, device = peer(k)
+            return remote(source_ref.at[j], target_ref.at[s], send, recv, device)
+
+        return (
+            lambda: every(lambda k: copy(k).start()),
+            lambda: remote(source_ref.at[others], target_ref.at[others], send, recv, up).wait_recv(),
+            lambda: remote(source_ref.at[others], target_ref.at[others], send, recv, up).wait_send(),
+        )
+
+    def gated_to(k):
+        return remote(gated.at[s], gated.at[s], q_send, q_recv, peer(k)[1])
+
+    def gated_all():
+        return remote(gated.at[others], gated.at[others], q_send, q_recv, up)
+
     gates = (
         lambda: every(lambda k: gated_to(k).start()),
-        lambda: every(lambda k: gated_from(k).wait_recv()),
-        lambda: every(lambda k: gated_to(k).wait_send()),
+        lambda: gated_all().wait_recv(),
+        lambda: gated_all().wait_send(),
     )
     states = over_sp(state_send, state_in, e_send, e_recv)
     enters = over_sp(enter_send, enter, f_send, f_recv)
@@ -326,11 +319,7 @@
 
     def to_expert(e, h):
         return remote(
-            sendbuf.at[e, h],
-            rows.at[quarter, s, h],
-            a_send.at[e, h],
-            a_recv.at[s, h],
-            (e // 4, e % 4, t),
+            sendbuf.at[e, h], rows.at[quarter, s, h], a_send, a_recv.at[s, h], (e // 4, e % 4, t)
         )
 
     def build(g, carry):
@@ -409,24 +398,24 @@
 
     def arrived(src, h):
         return remote(
-            sendbuf.at[src, h], rows.at[quarter, src, h], a_send.at[src, h], a_recv.at[src, h], up
+            sendbuf.at[src, h], rows.at[quarter, src, h], a_send, a_recv.at[src, h], up
         )
 
     def rows_up(src, h, q):
         ref = rows.at[q, src, h, 0]
-        return remote(ref, ref, yr_send.at[src, h], yr_recv.at[src, h], up)
+        return remote(ref, ref, yr_send, n_recv.at[src, h], up)
 
     def scaled_down(src, h, q):
         ref = rows.at[q, src, h, 1]
-        return remote(ref, ref, ys_send.at[src, h], ys_recv.at[src, h], down)
-
-    def across(src, h, q):
+        return remote(ref, ref, ys_send, n_recv.at[src, h], down)
+
+    def across(src, h, q, g):
         ref = rows.at[q, src, h]
-        return remote(ref, ref, pa_send.at[src, h], pa_recv.at[src, h], partner)
-
-    def across_beside(src, h, q):
+        return remote(ref, ref, pa_send, pa_recv.at[g], partner)
+
+    def across_beside(src, h, q, g):
         ref = rows.at[q, src, h]
-        return remote(ref, ref, pn_send.at[src, h], pn_recv.at[src, h], partner)
+        return remote(ref, ref, pn_send, pn_recv.at[g], partner)
 
     def unit(u):
         g, h, j = u // 8, u // 4 % 2, u % 4
@@ -441,17 +430,17 @@
 
         rows_up(src, h, quarter).start()
         scaled_down(src, h, quarter).start()
-        across(src, h, quarter).start()
+        across(src, h, quarter, u // 8).start()
 
     def forward_beside(u):
         src, h = unit(u)
-        rows_up(src, h, beside).wait_recv()
-        scaled_down(src, h, beside).wait_recv()
-        across_beside(src, h, beside).start()
+        ref = rows.at[beside, src, h]
+        remote(ref, ref, yr_send, n_recv.at[src, h], up).wait_recv()
+        across_beside(src, h, beside, u // 8).start()
 
     def halves_across(g, f):
         return remote(
-            part.at[g, 1 - core, f], part_in.at[g, f], d_send.at[g, f], d_recv.at[g, f], partner
+            part.at[g, 1 - core, f], part_in.at[g, f], d_send, d_recv.at[g, f], partner
         )
 
     def multiply(g, q):
@@ -459,10 +448,9 @@
 
         @pl.when(q == 0)
         def _():
-            for src in sources:
-                for h in range(2):
-                    across(src, h, partner_q).wait_recv()
-                    across_beside(src, h, partner_beside).wait_recv()
+            four = rows.at[partner_q, pl.ds(0, 4)]
+            remote(four, four, pa_send, pa_recv.at[g], partner).wait_recv()
+            remote(four, four, pn_send, pn_recv.at[g], partner).wait_recv()
             sums[...] = jnp.zeros_like(sums)
 
         for h in range(2):
@@ -504,12 +492,12 @@
 
     def first_step(g, way):
         return remote(
-            q1.at[g, way], y1.at[g, way], s1_send.at[g, way], s1_recv.at[g, way], (up, down)[way]
+            q1.at[g, way], y1.at[g, way], s1_send, s1_recv.at[g, way], (up, down)[way]
         )
 
     def second_step(g, way):
         return remote(
-            q2.at[g, way], y2.at[g, way], s2_send.at[g, way], s2_recv.at[g, way], (up, down)[way]
+            q2.at[g, way], y2.at[g, way], s2_send, s2_recv.at[g, way], (up, down)[way]
         )
 
     def sum_far(g):
@@ -536,11 +524,8 @@
 
     def to_owner(g, src):
         return remote(
-            fin.at[src], ret.at[s], c_send.at[src], c_recv.at[s], (src // 4, src % 4, t)
+            fin.at[src], ret.at[s], c_send, c_recv, (src // 4, src % 4, t)
         )
-
-    def from_expert(e):
-        return remote(fin.at[e], ret.at[e], c_send.at[e], c_recv.at[e], up)
 
     def sum_own(g):
         second_step(g, 0).wait_recv()
@@ -580,6 +565,11 @@
         pltpu.make_async_copy(gg, gg_hbm, local.at[6]),
         pltpu.make_async_copy(gu, gu_hbm, local.at[7]),
         pltpu.make_async_copy(gd, gd_hbm, local.at[8]),
+        pltpu.make_async_copy(dgate_out, dgate_hbm, local.at[10]),
+        pltpu.make_async_copy(dc_out, dc_hbm, local.at[11]),
+        pltpu.make_async_copy(proj_out, proj_hbm, local.at[12]),
+        pltpu.make_async_copy(dx_out, dx_hbm, local.at[13]),
+        pltpu.make_async_copy(db_out, db_hbm, local.at[14]),
     ]
 
     def turn(u, carry):
@@ -628,58 +618,33 @@
         def _():
             finish_forward()
 
-        @pl.when(m == 32)
-        def _():
-            grad_rows(gg, dgate)
-            stores[0].start()
-
-        @pl.when(m == 24 + 11)
-        def _():
-            grad_rows(gu, dup)
-            stores[1].start()
-            grad_down()
-            stores[2].start()
-
         return carry
 
     lax.fori_loop(0, 14 + 24 + 17 + 1, turn, 0)
 
-    def sent(k, carry):
-        e = peer(k)[0]
-        to_expert(e, 0).wait_send()
-        to_expert(e, 1).wait_send()
-        to_owner(0, e).wait_send()
-        return carry
-
-    lax.fori_loop(1, experts, sent, 0)
-
-    def forwarded(k, carry):
-        for h in range(2):
-            rows_up(k, h, quarter).wait_send()
-            scaled_down(k, h, quarter).wait_send()
-            across(k, h, quarter).wait_send()
-            across_beside(k, h, beside).wait_send()
-        return carry
-
-    lax.fori_loop(0, experts, forwarded, 0)
-
-    def summed(g, carry):
-        for f in range(4):
-            halves_across(g, f).wait_send()
-        for way in range(2):
-            first_step(g, way).wait_send()
-            second_step(g, way).wait_send()
-        return carry
-
-    lax.fori_loop(0, 4, summed, 0)
+    grad_rows(gg, dgate)
+    stores[0].start()
+    grad_rows(gu, dup)
+    stores[1].start()
+    grad_down()
+    stores[2].start()
+
+    for ref, send in (
+        (sendbuf.at[others], a_send),
+        (rows.at[0, :, :, 0], yr_send),
+        (rows.at[0, :, :, 1], ys_send),
+        (rows.at[0], pa_send),
+        (rows.at[0], pn_send),
+        (part.at[:, 0], d_send),
+        (q1, s1_send),
+        (q2, s2_send),
+        (fin.at[others], c_send),
+    ):
+        remote(ref, ref, send, c_recv, up).wait_send()
     for exchange in (states, enters):
         exchange[2]()
 
-    def take(k, carry):
-        from_expert(peer(k)[0]).wait_recv()
-        return carry
-
-    lax.fori_loop(1, experts, take, 0)
+    remote(fin.at[others], ret.at[others], c_send, c_recv, up).wait_recv()
     places = experts * cap
     picked = tn(hot[...].reshape(places, tokens), ret[...].reshape(places, own))
     gm[t] = (cot_own[...].astype(F32) + picked).astype(BF16)
@@ -701,14 +666,14 @@
         return remote(
             gm.at[i // 2, my_half, k * columns : (k + 1) * columns],
             features.at[s, my_half],
-            p_send.at[i],
-            p_recv.at[s],
+            p_send,
+            p_recv,
             (i // 4, i % 4, t),
         )
 
-    def share_half(src, half_rows):
-        ref = features.at[src, half_rows]
-        return remote(ref, ref, r_send.at[src], r_recv.at[src], partner)
+    def share_half(half_rows):
+        ref = features.at[:, half_rows]
+        return remote(ref, ref, r_send, r_recv, partner)
 
     def send_rows(j):
         for k in range(2):
@@ -720,22 +685,17 @@
 
             @pl.when(i == s)
             def _():
-                features[s] = gm[j, :, k * columns : (k + 1) * columns]
+                features[s, my_half] = gm[j, my_half, k * columns : (k + 1) * columns]
 
     def project(j):
         return nn(gm[j], op[pl.ds(j * own, own), :])
 
-    def take_features(k):
-        src = peer(k)[0]
-        remote(
-            features.at[src, my_half], features.at[src, my_half], p_send.at[src], p_recv.at[src], up
-        ).wait_recv()
-        share_half(src, my_half).start()
-
-    def multiply_features(k):
-        src = peer(k)[0]
-        share_half(src, mate_half).wait_recv()
-        proj_out[...] += tn(features[src], gated[src])
+    def features_all():
+        ref = features.at[others, my_half]
+        return remote(ref, ref, p_send, p_recv, up)
+
+    def multiply_features(src, total):
+        return total + tn(features[src], gated[src])
 
     moves = (
         (1, t, up, low),
@@ -800,32 +760,38 @@
     )
     dgate_out[...] = backward[3].astype(BF16)
     dc_out[...] = backward[2].astype(BF16)
+    stores[3].start()
+    stores[4].start()
     scan_back()
     tails = by_lane(jnp.exp(col[tokens - 1 : tokens, :] - col), tokens, heads)
     tail_values = (x_in[...].astype(F32) * tails).astype(BF16)
-    every(take_features)
+    features_all().wait_recv()
+    share_half(my_half).start()
     gates[1]()
-    proj_out[...] = tn(features[s], gated[s])
-    every(multiply_features)
-    def features_sent(k):
-        i = peer(k)[0]
-        to_features(i, 0).wait_send()
-        share_half(i, my_half).wait_send()
-
-    every(features_sent)
+    share_half(mate_half).wait_recv()
+    proj_out[...] = lax.fori_loop(
+        0, experts, multiply_features, jnp.zeros(proj_out.shape, F32)
+    )
+    stores[5].start()
+    features_all().wait_send()
+    share_half(my_half).wait_send()
     gates[2]()
     backs[2]()
     for move in moves:
         gather(*move).wait_send()
-    for store in stores:
+    for store in stores[:6]:
         store.wait()
 
     leaves[1]()
     leaving = leave[...].reshape(x_in.shape[1], STATE)
     dx_out[...] = (backward[0] + tails * nt(b_in[...], leaving)).astype(BF16)
+    stores[6].start()
     db_out[...] = (backward[1] + nn(tail_values, leaving)).astype(BF16)
+    stores[7].start()
 
     leaves[2]()
+    stores[6].wait()
+    stores[7].wait()
 
 
 def whole(ids, wts, ld, x, b, c, gate, mixed, cot, wg, wu, wd, op, experts, cap, heads):
@@ -857,8 +823,13 @@
             jax.ShapeDtypeStruct(wd.shape, BF16),
         ],
         in_specs=[vmem] * 7 + [hbm] * 6,
-        out_specs=[vmem] * 5 + [hbm] * 3,
+        out_specs=[hbm] * 8,
         scratch_shapes=[
+            buf(*x.shape),
+            buf(*b.shape),
+            buf(*c.shape),
+            buf(*gate.shape),
+            buf(width // experts, channels, dtype=F32),
             buf(8, tokens, own),
             buf(*op.shape),
             buf(tokens, channels, dtype=F32),
@@ -898,14 +869,16 @@
             buf(*wg.shape),
             buf(*wu.shape),
             buf(*wd.shape),
-            dma((10,)),
+            dma((15,)),
         ]
-        + [dma((experts, 2))] * 10
-        + [dma((4, 4))] * 2
-        + [dma((4, 2))] * 4
-        + [dma((experts,))] * 2
+        + [dma(()), dma((experts, 2))] * 2
+        + [dma(())]
+        + [dma(()), dma((4,))] * 2
+        + [dma(()), dma((4, 4))]
+        + [dma(()), dma((4, 2))] * 2
+        + [dma(())] * 2
         + [dma((10,))] * 2
-        + [dma((experts,))] * 14,
+        + [dma(())] * 14,
         compiler_params=pltpu.CompilerParams(
             collective_id=0, has_side_effects=True, vmem_limit_bytes=60 * 2**20
         ),

time: 141 us -> 138 us (0.979)
  the two profiles are of different devices: /device:TPU:0 before, /device:TPU:19 now
where the time goes in v7:
time: 138 us
  Pallas kernels  137 us (99%)
    pallas_call x1, Pallas kernels, whole(): pl.pallas_call(kernel, out_shape=[jax.ShapeDtypeStruct(x.shape, BF16), ja...  131 us
    pallas_call x1, Pallas kernels, hand_out(): pl.pallas_call(kernel, out_shape=[jax.ShapeDtypeStruct(a.shape, a.dtype)...  5.71 us

profile of v7, /device:TPU:19, one launch (start us, length us, event | category | flops | bytes accessed | tf_op | source)
XLA Modules:
  0.0 137.6 jit_solution(15582261944507455830)
XLA Ops:
  0.6 131.2 %whole.1 = (bf16[256,256]{1,0:T(8,128)(2,1)}, bf16[256,128]{1,0:T(8,128)(2,1)}, bf16[256,128]{1,0:T(8,128)(2,1)}, bf16[256,256]{1,0:T(8,128)(2,1)}, f32[256,256]...) custom-call(s32[2,256]{1,0:T(2,128)} %bitcast.11, ...), custom_call_target="tpu_custom_call" | custom-call | tf_op jit(solution)/shard_map/whole/pallas_call | solution.py:813
  131.9 5.7 %hand_out.1 = (bf16[256,256]{1,0:T(8,128)(2,1)}, bf16[256,128]{1,0:T(8,128)(2,1)}, bf16[256,128]{1,0:T(8,128)(2,1)}, bf16[256,256]{1,0:T(8,128)(2,1)}, f32[256,2...) custom-call(bf16[256,256]{1,0:T(8,128)(2,1)} %get-tuple-element.24.refs_0_, ...), custom_call_target="tpu_custom_call" | custom-call | tf_op jit(solution)/shard_map/hand_out/pallas_call | solution.py:916

commit v8 on v7

--- a/solution.py
+++ b/solution.py
@@ -296,17 +296,39 @@
             lambda: remote(source_ref.at[others], target_ref.at[others], send, recv, up).wait_send(),
         )
 
-    def gated_to(k):
-        return remote(gated.at[s], gated.at[s], q_send, q_recv, peer(k)[1])
-
-    def gated_all():
-        return remote(gated.at[others], gated.at[others], q_send, q_recv, up)
-
-    gates = (
-        lambda: every(lambda k: gated_to(k).start()),
-        lambda: gated_all().wait_recv(),
-        lambda: gated_all().wait_send(),
-    )
+    first_half, second_half = pl.ds(0, tokens // 2), pl.ds(tokens // 2, tokens // 2)
+
+    def gated_one(k):
+        ref, other = gated.at[z, x, first_half], gated.at[z, x, second_half]
+        to_z, to_x = (z + k) % 4, (x + k) % 4
+        return (
+            remote(ref, ref, q_send.at[0], q_recv.at[0], (z, to_x, t)),
+            remote(other, other, q_send.at[1], q_recv.at[1], (to_z, x, t)),
+        )
+
+    def gated_four(k):
+        ref, other = gated.at[z, :, first_half], gated.at[:, x, second_half]
+        to_z, to_x = (z + k) % 4, (x + k) % 4
+        return (
+            remote(ref, ref, q_send.at[2], q_recv.at[2], (to_z, x, t)),
+            remote(other, other, q_send.at[3], q_recv.at[3], (z, to_x, t)),
+        )
+
+    def gated_came(k):
+        three = pl.ds(0, 3)
+        ref = gated.at[three, :, first_half] if k > 1 else gated.at[z, three, first_half]
+        return remote(ref, ref, q_send.at[k], q_recv.at[k], up)
+
+    def gated_start(step):
+        for k in range(1, 4):
+            for copy in step(k):
+                copy.start()
+
+    def gated_second():
+        gated_came(0).wait_recv()
+        gated_came(1).wait_recv()
+        gated_start(gated_four)
+
     states = over_sp(state_send, state_in, e_send, e_recv)
     enters = over_sp(enter_send, enter, f_send, f_recv)
     backs = over_sp(back_send, back_in, b_send, b_recv)
@@ -390,8 +412,8 @@
         whole = y_ref[...] + leads * nt(c_in[...], entering)
         g = gate_in[...].astype(F32)
         y_ref[...] = whole
-        gated[s] = (whole * (g * jax.nn.sigmoid(g))).astype(BF16)
-        gates[0]()
+        gated[z, x] = (whole * (g * jax.nn.sigmoid(g))).astype(BF16)
+        gated_start(gated_one)
 
     def source(g, j):
         return 4 * ((z + 4 - j) % 4) + (x + 8 - j - g) % 4
@@ -617,6 +639,10 @@
         @pl.when(u == 33)
         def _():
             finish_forward()
+
+        @pl.when(u == 38)
+        def _():
+            gated_second()
 
         return carry
 
@@ -658,9 +684,10 @@
         ref = gm.at[src] if part_rows is None else gm.at[src, part_rows]
         return remote(ref, ref, g_send.at[k], g_recv.at[k], device)
 
-    columns = gated.shape[2]
-    my_half = pl.ds(core * (tokens // 2), tokens // 2)
-    mate_half = pl.ds((1 - core) * (tokens // 2), tokens // 2)
+    columns = gated.shape[3]
+    half_size = tokens // 2
+    my_half = pl.ds(pl.multiple_of(core * half_size, half_size), half_size)
+    mate_half = pl.ds(pl.multiple_of((1 - core) * half_size, half_size), half_size)
 
     def to_features(i, k):
         return remote(
@@ -694,8 +721,9 @@
         ref = features.at[others, my_half]
         return remote(ref, ref, p_send, p_recv, up)
 
-    def multiply_features(src, total):
-        return total + tn(features[src], gated[src])
+    def multiply_features(half_rows):
+        long = (experts * tokens // 2, columns)
+        return tn(features[:, half_rows].reshape(long), gated[:, :, half_rows].reshape(long))
 
     moves = (
         (1, t, up, low),
@@ -767,15 +795,16 @@
     tail_values = (x_in[...].astype(F32) * tails).astype(BF16)
     features_all().wait_recv()
     share_half(my_half).start()
-    gates[1]()
+    gated_came(2).wait_recv()
+    gated_came(3).wait_recv()
+    proj_out[...] = multiply_features(my_half)
     share_half(mate_half).wait_recv()
-    proj_out[...] = lax.fori_loop(
-        0, experts, multiply_features, jnp.zeros(proj_out.shape, F32)
-    )
+    proj_out[...] += multiply_features(mate_half)
     stores[5].start()
     features_all().wait_send()
     share_half(my_half).wait_send()
-    gates[2]()
+    for k in range(4):
+        gated_came(k).wait_send()
     backs[2]()
     for move in moves:
         gather(*move).wait_send()
@@ -833,7 +862,7 @@
             buf(8, tokens, own),
             buf(*op.shape),
             buf(tokens, channels, dtype=F32),
-            buf(experts, tokens, channels),
+            buf(4, 4, tokens, channels),
             buf(experts, STEP + 8, STATE, dtype=F32),
             buf(experts, STEP + 8, STATE, dtype=F32),
             buf(experts, STEP, STATE),
@@ -878,7 +907,9 @@
         + [dma(()), dma((4, 2))] * 2
         + [dma(())] * 2
         + [dma((10,))] * 2
-        + [dma(())] * 14,
+        + [dma(())] * 10
+        + [dma((4,))] * 2
+        + [dma(())] * 2,
         compiler_params=pltpu.CompilerParams(
             collective_id=0, has_side_effects=True, vmem_limit_bytes=60 * 2**20
         ),

time: 138 us -> 129 us (0.935)
  the two profiles are of different devices: /device:TPU:19 before, /device:TPU:0 now
where the time goes in v8:
time: 129 us; the launch traced here: 128 us
  Pallas kernels  127 us (98%)
    pallas_call x1, Pallas kernels, whole(): pl.pallas_call(kernel, out_shape=[jax.ShapeDtypeStruct(x.shape, BF16), ja...  121 us
    pallas_call x1, Pallas kernels, hand_out(): pl.pallas_call(kernel, out_shape=[jax.ShapeDtypeStruct(a.shape, a.dtype)...  5.71 us

profile of v8, /device:TPU:0, one launch (start us, length us, event | category | flops | bytes accessed | tf_op | source)
XLA Modules:
  0.0 127.9 jit_solution(12335908696338432194)
XLA Ops:
  0.6 121.3 %whole.1 = (bf16[256,256]{1,0:T(8,128)(2,1)}, bf16[256,128]{1,0:T(8,128)(2,1)}, bf16[256,128]{1,0:T(8,128)(2,1)}, bf16[256,256]{1,0:T(8,128)(2,1)}, f32[256,256]...) custom-call(s32[2,256]{1,0:T(2,128)} %bitcast.11, ...), custom_call_target="tpu_custom_call" | custom-call | tf_op jit(solution)/shard_map/whole/pallas_call | solution.py:842
  122.0 5.7 %hand_out.1 = (bf16[256,256]{1,0:T(8,128)(2,1)}, bf16[256,128]{1,0:T(8,128)(2,1)}, bf16[256,128]{1,0:T(8,128)(2,1)}, bf16[256,256]{1,0:T(8,128)(2,1)}, f32[256,2...) custom-call(bf16[256,256]{1,0:T(8,128)(2,1)} %get-tuple-element.24.refs_0_, ...), custom_call_target="tpu_custom_call" | custom-call | tf_op jit(solution)/shard_map/hand_out/pallas_call | solution.py:947

commit v9 on v8

--- a/solution.py
+++ b/solution.py
@@ -671,10 +671,6 @@
         exchange[2]()
 
     remote(fin.at[others], ret.at[others], c_send, c_recv, up).wait_recv()
-    places = experts * cap
-    picked = tn(hot[...].reshape(places, tokens), ret[...].reshape(places, own))
-    gm[t] = (cot_own[...].astype(F32) + picked).astype(BF16)
-
     low, high = pl.ds(0, tokens // 2), pl.ds(tokens // 2, tokens // 2)
     below, above, far = (t + 6) % 8, (t + 2) % 8, (t + 4) % 8
     mate = t + 1 - 2 * core
@@ -741,7 +737,15 @@
     def start(k):
         gather(*[m for m in moves if m[0] == k][0]).start()
 
-    for k in (1, 3, 2, 4, 0):
+    def combine(at):
+        there = hot[:, :, at].reshape(experts * cap, -1)
+        picked = tn(there, ret[...].reshape(experts * cap, own))
+        gm[t, at] = (cot_own[at].astype(F32) + picked).astype(BF16)
+
+    combine(slice(0, tokens // 2))
+    start(1)
+    combine(slice(tokens // 2, tokens))
+    for k in (3, 2, 4, 0):
         start(k)
     out_grad = project(t)
     send_rows(t)
@@ -920,7 +924,7 @@
 def hand_out(arrays):
     pieces = []
     for k, a in enumerate(arrays):
-        count = max(1, a.size * a.dtype.itemsize // 2**19)
+        count = max(1, a.size * a.dtype.itemsize // 2**20)
         step = a.shape[0] // count
         pieces += [(k, pl.ds(m * step, step)) for m in range(count)]
 

time: 129 us -> 129 us (level)
  no operation moved by 1% of the time
where the time goes in v9:
time: 129 us; the launch traced here: 128 us
  Pallas kernels  127 us (98%)
    pallas_call x1, Pallas kernels, whole(): pl.pallas_call(kernel, out_shape=[jax.ShapeDtypeStruct(x.shape, BF16), ja...  121 us
    pallas_call x1, Pallas kernels, hand_out(): pl.pallas_call(kernel, out_shape=[jax.ShapeDtypeStruct(a.shape, a.dtype)...  6 us

profile of v9, /device:TPU:0, one launch (start us, length us, event | category | flops | bytes accessed | tf_op | source)
XLA Modules:
  0.0 127.9 jit_solution(11520545089721982825)
XLA Ops:
  0.6 121.1 %whole.1 = (bf16[256,256]{1,0:T(8,128)(2,1)}, bf16[256,128]{1,0:T(8,128)(2,1)}, bf16[256,128]{1,0:T(8,128)(2,1)}, bf16[256,256]{1,0:T(8,128)(2,1)}, f32[256,256]...) custom-call(s32[2,256]{1,0:T(2,128)} %bitcast.11, ...), custom_call_target="tpu_custom_call" | custom-call | tf_op jit(solution)/shard_map/whole/pallas_call | solution.py:846
  121.7 6.0 %hand_out.1 = (bf16[256,256]{1,0:T(8,128)(2,1)}, bf16[256,128]{1,0:T(8,128)(2,1)}, bf16[256,128]{1,0:T(8,128)(2,1)}, bf16[256,256]{1,0:T(8,128)(2,1)}, f32[256,2...) custom-call(bf16[256,256]{1,0:T(8,128)(2,1)} %get-tuple-element.24.refs_0_, ...), custom_call_target="tpu_custom_call" | custom-call | tf_op jit(solution)/shard_map/hand_out/pallas_call | solution.py:951
